TPU v7x, 512 devices: a whole 4x4x16 slice. The times are simulated.
512 devices in a mesh: ep: 128 (over z, x, core), tp: 4 (over y).
Axes of the slice: x: 4, y: 4, z: 16, core: 2. Of those that a mesh axis runs over, the one named last changes fastest.
Arguments:
- tokens: bfloat16 [6144, 2048], P('ep', 'tp'), may hold values from -6 to 6
- conv_state: bfloat16 [6144, 3, 1024], P('ep', None, 'tp'), may hold values from -6 to 6
- lru_state: float32 [6144, 1024], P('ep', 'tp'), may hold values from -6 to 6
- mix_gain: float32 [2048], replicated, may hold values from 0.1 to 1.9
- input_weight: bfloat16 [2048, 1024], P(None, 'tp'), may hold values from -0.125 to 0.125
- branch_weight: bfloat16 [2048, 1024], P(None, 'tp'), may hold values from -0.125 to 0.125
- conv_taps: float32 [4, 1024], P(None, 'tp'), may hold values from -3 to 3
- conv_bias: float32 [1024], P('tp'), may hold values from -3 to 3
- recur_weight: bfloat16 [8, 128, 128], P('tp'), may hold values from -0.5 to 0.5
- recur_bias: float32 [1024], P('tp'), may hold values from -4 to 4
- inject_weight: bfloat16 [8, 128, 128], P('tp'), may hold values from -0.5 to 0.5
- inject_bias: float32 [1024], P('tp'), may hold values from -4 to 4
- decay_param: float32 [1024], P('tp'), may hold values from -1 to 4
- output_weight: bfloat16 [1024, 2048], P(None, 'tp'), may hold values from -0.1875 to 0.1875
- moe_gain: float32 [2048], replicated, may hold values from 0.1 to 1.9
- route_ids: int32 [6144, 2], P('ep'), may hold values from 0 to 127, as said below
- route_logits: float32 [6144, 2], P('ep'), may hold values from -6 to 6
- group_weight: float32 [6144], P('ep'), may hold values from 0.25 to 1
- expert_gate: bfloat16 [128, 2048, 512], P('ep', None, 'tp'), may hold values from -0.125 to 0.125
- expert_up: bfloat16 [128, 2048, 512], P('ep', None, 'tp'), may hold values from -0.125 to 0.125
- expert_down: bfloat16 [128, 512, 2048], P('ep', 'tp'), may hold values from -0.25 to 0.25
Outputs:
- result: bfloat16 [6144, 2048], P('ep', 'tp')
- new_state: float32 [6144, 1024], P('ep', 'tp')
- new_conv: bfloat16 [6144, 3, 1024], P('ep', None, 'tp')
Inputs may be any that keep to these rules, and one draw needn't show every extreme that they name: `route_ids`: each row names 2 different experts of one group of 4 consecutive experts (the group of expert e is e // 4). In each aligned block of 48 rows no expert is named by more than 2 rows, and in every draw some expert is named by exactly 2 rows of every block.
All inputs are finite; a program needn't handle non-finite values.
Results may differ from a plain program's by a relative error of at most 0.013.
Values may be sent and summed in bfloat16 or wider, within the bound.
No kernel may reach another device: no remote copies, remote signals or barrier semaphores. Data moves between devices by JAX's collectives and lax.ppermute only.
A program may use at most 64 MiB of HBM per device.

v0:
```python
import jax
import jax.numpy as jnp
from jax import lax
from jax.sharding import PartitionSpec as P

PER_GROUP = 4


EPS = 1e-06
RATE = 8.0


def copy_for_each(value, axis):
    size = lax.axis_size(axis)
    return lax.all_to_all(
        jnp.broadcast_to(value[None], (size, *value.shape)), axis, 0, 0, tiled=True
    )


def laid_out(parts, dim):
    parts = jnp.moveaxis(parts, 0, dim)
    dims = parts.shape
    return parts.reshape(*dims[:dim], dims[dim] * dims[dim + 1], *dims[dim + 2 :])


def collect(value, axis, dim):
    parts = copy_for_each(value, axis)
    return laid_out(parts, dim)


def cut_along(value, dim, size):
    before, after = (value.shape[:dim], value.shape[dim + 1 :])
    return jnp.moveaxis(value.reshape(*before, size, -1, *after), dim, 0)


def summed_on_arrival(value, axis, dim):
    size = lax.axis_size(axis)
    parts = lax.all_to_all(cut_along(value, dim, size), axis, 0, 0, tiled=True)
    return jnp.sum(parts.astype(jnp.float32), axis=0)


def of_everyone(value, axis):
    return copy_for_each(value, axis).sum(axis=0)


def rms_norm(values, scales):
    wide = values.astype(jnp.float32)
    return wide * lax.rsqrt(jnp.mean(wide * wide, axis=-1, keepdims=True) + EPS) * scales


def block_gate(signal, weight, bias):
    blocks = weight.shape[0]
    grouped = signal.reshape(signal.shape[0], blocks, -1)
    mixed_out = jnp.einsum("sbi,bij->sbj", grouped, weight, preferred_element_type=jnp.float32)
    return jax.nn.sigmoid(mixed_out.reshape(signal.shape[0], -1) + bias)


def body(
    tokens,
    conv_state,
    lru_state,
    mix_gain,
    input_weight,
    branch_weight,
    conv_taps,
    conv_bias,
    recur_weight,
    recur_bias,
    inject_weight,
    inject_bias,
    decay_param,
    output_weight,
    moe_gain,
    route_ids,
    route_logits,
    group_weight,
    expert_gate,
    expert_up,
    expert_down,
):
    seq_count = tokens.shape[0]
    quarter = tokens.shape[1]
    member = lax.axis_index("tp")
    full_tokens = collect(tokens, "tp", 1)
    model_width = full_tokens.shape[1]
    normed = rms_norm(full_tokens, mix_gain).astype(jnp.bfloat16)
    branch_x = jnp.dot(normed, input_weight, preferred_element_type=jnp.float32).astype(
        jnp.bfloat16
    )
    branch_g = jnp.dot(normed, branch_weight, preferred_element_type=jnp.float32).astype(
        jnp.bfloat16
    )
    window = jnp.concatenate([conv_state, branch_x[:, None, :]], axis=1)
    conv_sum = conv_bias + jnp.sum(window.astype(jnp.float32) * conv_taps[None], axis=1)
    conv_out = conv_sum.astype(jnp.bfloat16)
    recur_gate = block_gate(conv_out, recur_weight, recur_bias)
    inject_gate = block_gate(conv_out, inject_weight, inject_bias)
    log_rate = -RATE * recur_gate * jax.nn.softplus(-decay_param)
    new_state = jnp.exp(log_rate) * lru_state + jnp.sqrt(
        -jnp.expm1(2.0 * log_rate)
    ) * inject_gate * conv_out.astype(jnp.float32)
    mixer_out = (new_state * jax.nn.gelu(branch_g.astype(jnp.float32))).astype(jnp.bfloat16)
    mixed_out = jnp.dot(
        collect(mixer_out, "tp", 1), output_weight, preferred_element_type=jnp.float32
    )
    stream = (tokens.astype(jnp.float32) + mixed_out).astype(jnp.bfloat16)
    top_count = route_ids.shape[1]
    experts = lax.axis_size("ep")
    capacity = max(
        2, min((seq_count - 2) * top_count // PER_GROUP, 2 * seq_count * top_count // experts)
    )
    flat_ids = route_ids.reshape(-1)
    one_hot = (flat_ids[:, None] == jnp.arange(experts, dtype=jnp.int32)[None, :]).astype(jnp.int32)
    earlier = jnp.cumsum(one_hot, axis=0) - one_hot
    slot_rank = jnp.sum(one_hot * earlier, axis=1).reshape(seq_count, top_count)
    slot_index = route_ids * capacity + slot_rank
    targets = jnp.arange(experts * capacity, dtype=jnp.int32)
    dispatch = jnp.sum(
        (targets[:, None, None] == slot_index[None]).astype(jnp.float32), axis=2
    ).astype(jnp.bfloat16)
    raised = jnp.exp(route_logits)
    route_weight = group_weight[:, None] * raised / jnp.sum(raised, axis=1, keepdims=True)
    stream_wide = stream.astype(jnp.float32)
    squares = jnp.sum(stream_wide * stream_wide, axis=1)
    total_sq = of_everyone(squares, "tp")
    gain_part = lax.dynamic_slice_in_dim(moe_gain, member * quarter, quarter, 0)
    moe_part = (stream_wide * lax.rsqrt(total_sq / model_width + EPS)[:, None] * gain_part).astype(
        jnp.bfloat16
    )
    outgoing = jnp.dot(dispatch, moe_part, preferred_element_type=jnp.float32).astype(jnp.bfloat16)
    outgoing = outgoing.reshape(experts, capacity, quarter)
    arrived = collect(
        lax.all_to_all(outgoing, "ep", split_axis=0, concat_axis=0, tiled=True), "tp", 2
    )
    senders, slot_count, unused = arrived.shape
    flat_rows = arrived.reshape(senders * slot_count, model_width)
    gate_act = jnp.dot(flat_rows, expert_gate[0], preferred_element_type=jnp.float32)
    up_act = jnp.dot(flat_rows, expert_up[0], preferred_element_type=jnp.float32)
    hidden = (jax.nn.silu(gate_act) * up_act).astype(jnp.bfloat16)
    partial_value = jnp.dot(hidden, expert_down[0], preferred_element_type=jnp.float32)
    partial_value = partial_value.reshape(senders, slot_count, model_width)
    summed = summed_on_arrival(partial_value.astype(jnp.bfloat16), "tp", 2)
    answer = summed.astype(jnp.bfloat16)
    returned = lax.all_to_all(answer, "ep", split_axis=0, concat_axis=0, tiled=True)
    flat_back = returned.reshape(experts * capacity, quarter)
    picked = jnp.take(flat_back, slot_index, axis=0).astype(jnp.float32)
    routed = jnp.sum(route_weight[:, :, None] * picked, axis=1)
    result = (stream.astype(jnp.float32) + routed).astype(jnp.bfloat16)
    return (result, new_state, window[:, 1:])


def solution(mesh):
    in_specs = (
        P("ep", "tp"),
        P("ep", None, "tp"),
        P("ep", "tp"),
        P(),
        P(None, "tp"),
        P(None, "tp"),
        P(None, "tp"),
        P("tp"),
        P("tp", None, None),
        P("tp"),
        P("tp", None, None),
        P("tp"),
        P("tp"),
        P(None, "tp"),
        P(),
        P("ep", None),
        P("ep", None),
        P("ep"),
        P("ep", None, "tp"),
        P("ep", None, "tp"),
        P("ep", "tp", None),
    )
    out_specs = (P("ep", "tp"), P("ep", "tp"), P("ep", None, "tp"))
    return jax.shard_map(body, mesh=mesh, in_specs=in_specs, out_specs=out_specs, check_vma=False)
```

profile of v0, /device:TPU:33, one launch (start us, length us, event | category | flops | bytes accessed | tf_op | source)
XLA Modules:
  0.0 148.3 jit_solution(1740164918627735072)
XLA Ops:
  0.6 1.6 %broadcast_in_dim.19 = bf16[4,48,512]{2,1,0:T(8,128)(2,1)} broadcast(bf16[48,512]{1,0:T(8,128)(2,1)} %param.21), dimensions={1,2} | broadcast | bytes 245760 | tf_op jit(solution)/shard_map/broadcast_in_dim | solution.py:16
  2.2 4.3 %all-to-all-start = ((bf16[4,48,512]{2,1,0:T(8,128)(2,1)}), bf16[4,48,512]{2,1,0:T(8,128)(2,1)S(1)}, u32[]{:S(2)}, u32[]{:S(2)}) async-start(bf16[4,48,512]{2,1,0:T(8,128)(2,1)} %broadcast_in_dim.19), calls=%async_computation | async-start | bytes 393216 | tf_op jit(solution)/shard_map/all_to_all | solution.py:15
  6.5 0.8 copy.103
  7.3 0.1 eq.28
  7.5 0.1 reduce_window_sum.11
  7.7 0.2 select_reduce_fusion
  7.8 0.1 reshape.82
  8.0 0.7 compare_and_fusion
  8.7 0.7 fusion.40
  9.4 2.3 %all-to-all-done = bf16[4,48,512]{2,1,0:T(8,128)(2,1)S(1)} async-done(((bf16[4,48,512]{2,1,0:T(8,128)(2,1)}), bf16[4,48,512]{2,1,0:T(8,128)(2,1)S(1)}, u32[]{:S(2)}, u32[]{:S(2)}) %all-to-all-start) | async-done | bytes 196640 | tf_op jit(solution)/shard_map/all_to_all | solution.py:15
  11.9 0.1 fusion.9
  12.1 0.3 fusion.4
  12.4 0.2 copy-done.5
  12.7 0.1 convolution_bitcast_fusion
  12.8 0.1 convolution_bitcast_fusion.1
  13.1 0.2 copy-done.2
  13.3 0.3 fusion.20
  13.7 0.6 broadcast_in_dim.21
  14.3 3.3 %all-to-all-start.1 = ((bf16[4,48,256]{2,1,0:T(8,128)(2,1)}), bf16[4,48,256]{2,1,0:T(8,128)(2,1)S(1)}, u32[]{:S(2)}, u32[]{:S(2)}) async-start(bf16[4,48,256]{2,1,0:T(8,128)(2,1)} %broadcast_in_dim.21), calls=%async_computation.1 | async-start | bytes 196608 | tf_op jit(solution)/shard_map/all_to_all | solution.py:15
  17.7 4.5 %all-to-all-done.1 = bf16[4,48,256]{2,1,0:T(8,128)(2,1)S(1)} async-done(((bf16[4,48,256]{2,1,0:T(8,128)(2,1)}), bf16[4,48,256]{2,1,0:T(8,128)(2,1)S(1)}, u32[]{:S(2)}, u32[]{:S(2)}) %all-to-all-start.1) | async-done | bytes 98336 | tf_op jit(solution)/shard_map/all_to_all | solution.py:15
  22.3 0.4 multiply_reduce_fusion.2
  22.7 0.6 broadcast_in_dim.23
  23.3 3.2 %all-to-all-start.2 = ((f32[4,1,48]{2,1,0:T(1,128)}), f32[4,1,48]{2,1,0:T(1,128)S(1)}, u32[]{:S(2)}, u32[]{:S(2)}) async-start(f32[4,1,48]{2,1,0:T(1,128)} %broadcast_in_dim.23), calls=%async_computation.2 | async-start | bytes 4096 | tf_op jit(solution)/shard_map/all_to_all | solution.py:15
  26.5 0.8 dynamic_slice.3
  27.3 3.3 %all-to-all-done.2 = f32[4,1,48]{2,1,0:T(1,128)S(1)} async-done(((f32[4,1,48]{2,1,0:T(1,128)}), f32[4,1,48]{2,1,0:T(1,128)S(1)}, u32[]{:S(2)}, u32[]{:S(2)}) %all-to-all-start.2) | async-done | bytes 800 | tf_op jit(solution)/shard_map/all_to_all | solution.py:15
  30.5 0.3 convolution_convert_fusion.1
  30.8 0.1 reshape.83
  30.9 45.4 %all_to_all.36 = bf16[128,2,512]{2,1,0:T(2,128)(2,1)S(1)} all-to-all(bf16[128,2,512]{2,1,0:T(2,128)(2,1)S(1)} %reshape.83), channel_id=1, replica_groups=mesh['ep'=128,'tp'=4] {'ep'}, dimensions={0} | all-to-all | bytes 524288 | tf_op jit(solution)/shard_map/all_to_all | solution.py:133
  76.3 0.5 broadcast_in_dim.24
  76.9 17.3 %all_to_all.37 = bf16[4,128,2,512]{3,2,1,0:T(2,128)(2,1)S(1)} all-to-all(bf16[4,128,2,512]{3,2,1,0:T(2,128)(2,1)S(1)} %broadcast_in_dim.24), channel_id=1, replica_groups=mesh['ep'=128,'tp'=4] {'tp'}, dimensions={0} | all-to-all | bytes 2097152 | tf_op jit(solution)/shard_map/all_to_all | solution.py:15
  94.2 1.4 copy.107
  95.5 0.3 copy.120
  95.8 0.7 copy-done.4
  96.6 0.4 fusion.7
  97.0 0.4 fusion
  97.4 0.6 copy-done.3
  98.0 0.4 convolution_convert_fusion
  98.6 16.4 %all_to_all.38 = bf16[4,128,2,512]{3,1,2,0:T(8,128)(2,1)S(1)} all-to-all(bf16[4,128,2,512]{3,1,2,0:T(8,128)(2,1)S(1)} %bitcast.94), channel_id=1, replica_groups=mesh['ep'=128,'tp'=4] {'tp'}, dimensions={0} | all-to-all | bytes 2097152 | tf_op jit(solution)/shard_map/all_to_all | solution.py:38
  115.0 0.3 reduce_sum.94
  115.3 1.0 copy.111
  116.2 7.5 %all-to-all-start.6 = ((bf16[128,2,512]{2,1,0:T(2,128)(2,1)}), bf16[128,2,512]{2,1,0:T(2,128)(2,1)S(1)}, u32[]{:S(2)}, u32[]{:S(2)}) async-start(bf16[128,2,512]{2,1,0:T(2,128)(2,1)} %copy.111), calls=%async_computation.6 | async-start | bytes 524288 | tf_op jit(solution)/shard_map/all_to_all | solution.py:144
  123.9 0.1 reshape.89
  124.0 0.1 copy.105
  124.2 0.6 fusion.10
  124.9 21.4 %all-to-all-done.6 = bf16[128,2,512]{2,1,0:T(2,128)(2,1)S(1)} async-done(((bf16[128,2,512]{2,1,0:T(2,128)(2,1)}), bf16[128,2,512]{2,1,0:T(2,128)(2,1)S(1)}, u32[]{:S(2)}, u32[]{:S(2)}) %all-to-all-start.6) | async-done | bytes 262176 | tf_op jit(solution)/shard_map/all_to_all | solution.py:144
  146.4 0.8 gather_fusion
  147.3 0.4 multiply_reduce_fusion
  147.6 0.6 add_convert_fusion
  (54 shorter events, 1.0 us)
Async XLA Ops:
  0.6 21.6 %copy-start = (bf16[1024,512]{1,0:T(8,128)(2,1)S(1)}, bf16[1024,512]{1,0:T(8,128)(2,1)}, u32[]{:S(2)}) copy-start(bf16[1024,512]{1,0:T(8,128)(2,1)} %param.34) | copy-start | bytes 3145732
  2.2 9.8 %copy-start.1 = (bf16[2048,256]{1,0:T(8,128)(2,1)S(1)}, bf16[2048,256]{1,0:T(8,128)(2,1)}, u32[]{:S(2)}) copy-start(bf16[2048,256]{1,0:T(8,128)(2,1)} %param.25) | copy-start | bytes 3145732
  2.2 9.8 %copy-start.11 = (f32[2048]{0:T(1024)S(1)}, f32[2048]{0:T(1024)}, u32[]{:S(2)}) copy-start(f32[2048]{0:T(1024)} %param.24) | copy-start | bytes 24580
  2.2 9.5 %all-to-all-start = ((bf16[4,48,512]{2,1,0:T(8,128)(2,1)}), bf16[4,48,512]{2,1,0:T(8,128)(2,1)S(1)}, u32[]{:S(2)}, u32[]{:S(2)}) async-start(bf16[4,48,512]{2,1,0:T(8,128)(2,1)} %broadcast_in_dim.19), calls=%async_computation | async-start | bytes 393216 | tf_op jit(solution)/shard_map/all_to_all | solution.py:15
  11.8 0.9 copy-start.5
  11.8 0.9 copy-start.13
  11.8 0.9 copy-start.8
  11.8 0.9 copy-start.12
  11.8 1.0 copy-start.9
  11.9 1.1 copy-start.10
  11.9 1.1 copy-start.14
  11.9 1.1 copy-start.15
  12.1 1.3 copy-start.2
  13.3 9.3 %copy-start.7 = (f32[48,256]{1,0:T(8,128)}, f32[48,256]{1,0:T(8,128)S(1)}, u32[]{:S(2)}) copy-start(f32[48,256]{1,0:T(8,128)S(1)} %fusion.27) | copy-start | bytes 147460
  13.3 8.9 %copy-start.6 = (bf16[48,512]{1,0:T(8,128)(2,1)S(1)}, bf16[48,512]{1,0:T(8,128)(2,1)}, u32[]{:S(2)}) copy-start(bf16[48,512]{1,0:T(8,128)(2,1)} %param.21) | copy-start | bytes 147460
  14.3 7.9 %all-to-all-start.1 = ((bf16[4,48,256]{2,1,0:T(8,128)(2,1)}), bf16[4,48,256]{2,1,0:T(8,128)(2,1)S(1)}, u32[]{:S(2)}, u32[]{:S(2)}) async-start(bf16[4,48,256]{2,1,0:T(8,128)(2,1)} %broadcast_in_dim.21), calls=%async_computation.1 | async-start | bytes 196608 | tf_op jit(solution)/shard_map/all_to_all | solution.py:15
  23.3 7.3 %all-to-all-start.2 = ((f32[4,1,48]{2,1,0:T(1,128)}), f32[4,1,48]{2,1,0:T(1,128)S(1)}, u32[]{:S(2)}, u32[]{:S(2)}) async-start(f32[4,1,48]{2,1,0:T(1,128)} %broadcast_in_dim.23), calls=%async_computation.2 | async-start | bytes 4096 | tf_op jit(solution)/shard_map/all_to_all | solution.py:15
  95.5 1.0 copy-start.4
  95.8 1.2 copy-start.18
  97.0 1.0 copy-start.3
  115.0 9.1 %copy-start.16 = (f32[48,2]{0,1:T(2,128)S(1)}, f32[48,2]{0,1:T(2,128)}, u32[]{:S(2)}) copy-start(f32[48,2]{0,1:T(2,128)} %param.37) | copy-start | bytes 1156
  115.0 9.1 %copy-start.17 = (f32[48]{0:T(128)S(1)}, f32[48]{0:T(128)}, u32[]{:S(2)}) copy-start(f32[48]{0:T(128)} %param.38) | copy-start | bytes 580
  116.2 30.1 %all-to-all-start.6 = ((bf16[128,2,512]{2,1,0:T(2,128)(2,1)}), bf16[128,2,512]{2,1,0:T(2,128)(2,1)S(1)}, u32[]{:S(2)}, u32[]{:S(2)}) async-start(bf16[128,2,512]{2,1,0:T(2,128)(2,1)} %copy.111), calls=%async_computation.6 | async-start | bytes 524288 | tf_op jit(solution)/shard_map/all_to_all | solution.py:144
where the time goes:
time: 149 us; the launch traced here: 148 us
  blocking collectives  79.1 us (53%)
  waiting for transfers between devices  31.5 us (21%)
  starting transfers between devices  18.4 us (12%)
  local copies, waits for them, and re-layouts  11.2 us (8%)
  other arithmetic  4.12 us (3%)
  matrix products  2.89 us (2%)
    all_to_all x1, blocking collectives, body(): lax.all_to_all(outgoing, 'ep', split_axis=0, concat_axis=0, tiled=True)  45.4 us
    all_to_all x1, waiting for transfers between devices, body(): lax.all_to_all(answer, 'ep', split_axis=0, concat_axis=0, tiled=True)  21.4 us
    all_to_all x1, blocking collectives, copy_for_each(): lax.all_to_all(jnp.broadcast_to(value[None], (size, *value.shape)), axis,...  17.3 us
    all_to_all x1, blocking collectives, summed_on_arrival(): parts = lax.all_to_all(cut_along(value, dim, size), axis, 0, 0, tiled=True)  16.4 us
    all_to_all x3, starting transfers between devices, copy_for_each(): lax.all_to_all(jnp.broadcast_to(value[None], (size, *value.shape)), axis,...  10.8 us
    all_to_all x3, waiting for transfers between devices, copy_for_each(): lax.all_to_all(jnp.broadcast_to(value[None], (size, *value.shape)), axis,...  10.1 us
    all_to_all x1, starting transfers between devices, body(): lax.all_to_all(answer, 'ep', split_axis=0, concat_axis=0, tiled=True)  7.51 us
    broadcast_in_dim x4, local copies, waits for them, and re-layouts, copy_for_each(): jnp.broadcast_to(value[None], (size, *value.shape))  3.33 us
  transfers between devices with their start and end apart: 4, of which 4 were waited for; matrix products, arithmetic and copies ran while one was open for 3% of the time, Pallas kernels for 0%

commit v1 on v0

v1 whole, which is shorter than its diff:
```python
import jax
import jax.numpy as jnp
from jax import lax
from jax.sharding import PartitionSpec as P

PER_GROUP = 4
EPS = 1e-06
RATE = 8.0
F32 = jnp.float32
BF16 = jnp.bfloat16


def to_each(value, axis):
    size = lax.axis_size(axis)
    return lax.all_to_all(
        jnp.broadcast_to(value[None], (size, *value.shape)), axis, 0, 0, tiled=True
    )


def side_by_side(parts):
    size, rows, width = parts.shape
    return jnp.swapaxes(parts, 0, 1).reshape(rows, size * width)


def dot(a, b):
    return jnp.dot(a, b, preferred_element_type=F32)


def block_gate(signal, weight, bias):
    blocks = weight.shape[0]
    grouped = signal.reshape(signal.shape[0], blocks, -1)
    mixed_out = jnp.einsum("sbi,bij->sbj", grouped, weight, preferred_element_type=F32)
    return jax.nn.sigmoid(mixed_out.reshape(signal.shape[0], -1) + bias)


def body(
    tokens,
    conv_state,
    lru_state,
    mix_gain,
    input_weight,
    branch_weight,
    conv_taps,
    conv_bias,
    recur_weight,
    recur_bias,
    inject_weight,
    inject_bias,
    decay_param,
    output_weight,
    moe_gain,
    route_ids,
    route_logits,
    group_weight,
    expert_gate,
    expert_up,
    expert_down,
):
    seq_count, quarter = tokens.shape
    members = lax.axis_size("tp")
    model_width = members * quarter
    experts = lax.axis_size("ep")
    top_count = route_ids.shape[1]
    capacity = 2

    flat_ids = route_ids.reshape(-1)
    one_hot = (flat_ids[:, None] == jnp.arange(experts, dtype=jnp.int32)[None, :]).astype(jnp.int32)
    earlier = jnp.cumsum(one_hot, axis=0) - one_hot
    slot_rank = jnp.sum(one_hot * earlier, axis=1).reshape(seq_count, top_count)
    slot_index = route_ids * capacity + slot_rank
    slots = experts * capacity
    targets = jnp.arange(slots, dtype=jnp.int32)
    hits = (targets[None, None, :] == slot_index[:, :, None])
    dispatch = jnp.any(targets[:, None, None] == slot_index[None], axis=2).astype(BF16)
    raised = jnp.exp(route_logits)
    route_weight = group_weight[:, None] * raised / jnp.sum(raised, axis=1, keepdims=True)
    combine = jnp.sum(jnp.where(hits, route_weight[:, :, None], 0.0), axis=1)
    combine_high = combine.astype(BF16)
    combine_low = (combine - combine_high.astype(F32)).astype(BF16)

    wide = to_each(tokens, "tp").astype(F32)
    scale = lax.rsqrt(jnp.sum(wide * wide, axis=(0, 2)) / model_width + EPS)
    normed = (
        wide * scale[None, :, None] * mix_gain.reshape(members, 1, quarter)
    ).astype(BF16)
    normed = side_by_side(normed)
    branch_x = dot(normed, input_weight).astype(BF16)
    branch_g = dot(normed, branch_weight).astype(BF16)
    window = jnp.concatenate([conv_state, branch_x[:, None, :]], axis=1)
    conv_sum = conv_bias + jnp.sum(window.astype(F32) * conv_taps[None], axis=1)
    conv_out = conv_sum.astype(BF16)
    recur_gate = block_gate(conv_out, recur_weight, recur_bias)
    inject_gate = block_gate(conv_out, inject_weight, inject_bias)
    log_rate = -RATE * recur_gate * jax.nn.softplus(-decay_param)
    new_state = jnp.exp(log_rate) * lru_state + jnp.sqrt(
        -jnp.expm1(2.0 * log_rate)
    ) * inject_gate * conv_out.astype(F32)
    mixer_out = (new_state * jax.nn.gelu(branch_g.astype(F32))).astype(BF16)
    mixed_out = dot(side_by_side(to_each(mixer_out, "tp")), output_weight)
    stream = (tokens.astype(F32) + mixed_out).astype(BF16)

    outgoing = dot(dispatch, stream).astype(BF16)
    arrived = lax.all_to_all(outgoing, "ep", 0, 0, tiled=True)
    rows = to_each(arrived, "tp").astype(F32)
    row_scale = lax.rsqrt(jnp.sum(rows * rows, axis=(0, 2)) / model_width + EPS)
    moe_in = (
        rows * row_scale[None, :, None] * moe_gain.reshape(members, 1, quarter)
    ).astype(BF16)
    moe_in = side_by_side(moe_in)
    gate_act = dot(moe_in, expert_gate[0])
    up_act = dot(moe_in, expert_up[0])
    hidden = (jax.nn.silu(gate_act) * up_act).astype(BF16)
    down = expert_down[0]
    partial_out = jnp.concatenate(
        [
            dot(hidden, down[:, m * quarter : (m + 1) * quarter]).astype(BF16)
            for m in range(members)
        ],
        axis=0,
    )
    partial_in = lax.all_to_all(partial_out, "tp", 0, 0, tiled=True)
    answer = jnp.sum(partial_in.reshape(members, slots, quarter).astype(F32), axis=0).astype(BF16)
    returned = lax.all_to_all(answer, "ep", 0, 0, tiled=True)
    routed = dot(combine_high, returned) + dot(combine_low, returned)
    result = (stream.astype(F32) + routed).astype(BF16)
    return (result, new_state, window[:, 1:])


def solution(mesh):
    in_specs = (
        P("ep", "tp"),
        P("ep", None, "tp"),
        P("ep", "tp"),
        P(),
        P(None, "tp"),
        P(None, "tp"),
        P(None, "tp"),
        P("tp"),
        P("tp", None, None),
        P("tp"),
        P("tp", None, None),
        P("tp"),
        P("tp"),
        P(None, "tp"),
        P(),
        P("ep", None),
        P("ep", None),
        P("ep"),
        P("ep", None, "tp"),
        P("ep", None, "tp"),
        P("ep", "tp", None),
    )
    out_specs = (P("ep", "tp"), P("ep", "tp"), P("ep", None, "tp"))
    return jax.shard_map(body, mesh=mesh, in_specs=in_specs, out_specs=out_specs, check_vma=False)
```

time: 149 us -> 140 us (0.940)
  blocking collectives: 79.1 us -> 60.7 us
  waiting for transfers between devices: 31.5 us -> 42.7 us
  local copies, waits for them, and re-layouts: 11.2 us -> 8.2 us
    all_to_all x3 -> x2, blocking collectives: 79.1 us -> 60.7 us  [the longest x1 44.2 us: body(): arrived = lax.all_to_all(outgoing, 'ep', 0, 0, tiled=True)]
    all_to_all x4, waiting for transfers between devices: 31.5 us -> 42.7 us  [the longest x1 21.8 us: body(): returned = lax.all_to_all(answer, 'ep', 0, 0, tiled=True)]
    dot_general x9 -> x14, matrix products: 2.89 us -> 4.17 us  [the longest x12 3.9 us: dot(): return jnp.dot(a, b, preferred_element_type=F32)]
where the time goes in v1:
time: 140 us
  blocking collectives  60.7 us (43%)
  waiting for transfers between devices  42.7 us (30%)
  starting transfers between devices  18.9 us (13%)
  local copies, waits for them, and re-layouts  8.2 us (6%)
  matrix products  4.17 us (3%)
  other arithmetic  3.97 us (3%)
    all_to_all x1, blocking collectives, body(): arrived = lax.all_to_all(outgoing, 'ep', 0, 0, tiled=True)  44.2 us
    all_to_all x1, waiting for transfers between devices, body(): returned = lax.all_to_all(answer, 'ep', 0, 0, tiled=True)  21.8 us
    all_to_all x3, waiting for transfers between devices, to_each(): lax.all_to_all(jnp.broadcast_to(value[None], (size, *value.shape)), axis,...  20.9 us
    all_to_all x1, blocking collectives, body(): partial_in = lax.all_to_all(partial_out, 'tp', 0, 0, tiled=True)  16.4 us
    all_to_all x3, starting transfers between devices, to_each(): lax.all_to_all(jnp.broadcast_to(value[None], (size, *value.shape)), axis,...  11.1 us
    all_to_all x1, starting transfers between devices, body(): returned = lax.all_to_all(answer, 'ep', 0, 0, tiled=True)  7.72 us
    dot_general x12, matrix products, dot(): return jnp.dot(a, b, preferred_element_type=F32)  3.9 us
    broadcast_in_dim x5, local copies, waits for them, and re-layouts, to_each(): jnp.broadcast_to(value[None], (size, *value.shape))  3.57 us
  transfers between devices with their start and end apart: 4, of which 4 were waited for; matrix products, arithmetic and copies ran while one was open for 3% of the time, Pallas kernels for 0%

profile of v1, /device:TPU:33, one launch (start us, length us, event | category | flops | bytes accessed | tf_op | source)
XLA Modules:
  0.0 139.6 jit_solution(16232884044620684058)
XLA Ops:
  0.7 1.6 %broadcast_in_dim.22 = bf16[4,48,512]{2,1,0:T(8,128)(2,1)} broadcast(bf16[48,512]{1,0:T(8,128)(2,1)} %param.21), dimensions={1,2} | broadcast | bytes 245760 | tf_op jit(solution)/shard_map/broadcast_in_dim | solution.py:16
  2.3 4.2 %all-to-all-start = ((bf16[4,48,512]{2,1,0:T(8,128)(2,1)}), bf16[4,48,512]{2,1,0:T(8,128)(2,1)S(1)}, u32[]{:S(2)}, u32[]{:S(2)}) async-start(bf16[4,48,512]{2,1,0:T(8,128)(2,1)} %broadcast_in_dim.22), calls=%async_computation | async-start | bytes 393216 | tf_op jit(solution)/shard_map/all_to_all | solution.py:15
  6.5 0.7 mul.130
  7.2 0.8 copy.63
  7.9 0.1 eq.42
  8.2 0.1 reduce_window_sum.11
  8.3 0.2 select_reduce_fusion.1
  8.5 0.1 reshape.73
  8.7 0.7 multiply_add_fusion
  9.4 0.7 fusion.50
  10.1 1.6 %all-to-all-done = bf16[4,48,512]{2,1,0:T(8,128)(2,1)S(1)} async-done(((bf16[4,48,512]{2,1,0:T(8,128)(2,1)}), bf16[4,48,512]{2,1,0:T(8,128)(2,1)S(1)}, u32[]{:S(2)}, u32[]{:S(2)}) %all-to-all-start) | async-done | bytes 196640 | tf_op jit(solution)/shard_map/all_to_all | solution.py:15
  11.7 0.1 fusion.12
  11.9 0.1 fusion.15
  12.1 0.3 fusion.8
  12.4 0.3 copy-done.5
  12.7 0.1 convolution_bitcast_fusion
  12.9 0.1 convolution_bitcast_fusion.1
  13.2 0.2 copy-done.1
  13.3 0.3 fusion.30
  13.6 0.6 broadcast_in_dim.24
  14.3 3.3 %all-to-all-start.1 = ((bf16[4,48,256]{2,1,0:T(8,128)(2,1)}), bf16[4,48,256]{2,1,0:T(8,128)(2,1)S(1)}, u32[]{:S(2)}, u32[]{:S(2)}) async-start(bf16[4,48,256]{2,1,0:T(8,128)(2,1)} %broadcast_in_dim.24), calls=%async_computation.1 | async-start | bytes 196608 | tf_op jit(solution)/shard_map/all_to_all | solution.py:15
  17.7 4.5 %all-to-all-done.1 = bf16[4,48,256]{2,1,0:T(8,128)(2,1)S(1)} async-done(((bf16[4,48,256]{2,1,0:T(8,128)(2,1)}), bf16[4,48,256]{2,1,0:T(8,128)(2,1)S(1)}, u32[]{:S(2)}, u32[]{:S(2)}) %all-to-all-start.1) | async-done | bytes 98336 | tf_op jit(solution)/shard_map/all_to_all | solution.py:15
  22.2 0.3 fusion.5
  22.5 0.3 convolution_convert_fusion
  22.8 0.1 all_to_all.31
  22.9 44.2 %all_to_all.45 = bf16[128,2,512]{2,1,0:T(2,128)(2,1)S(1)} all-to-all(bf16[128,2,512]{2,1,0:T(2,128)(2,1)S(1)} %all_to_all.31), channel_id=1, replica_groups=mesh['ep'=128,'tp'=4] {'ep'}, dimensions={0} | all-to-all | bytes 524288 | tf_op jit(solution)/shard_map/all_to_all | solution.py:103
  67.3 0.1 copy.65
  67.4 1.1 broadcast_in_dim.28
  68.5 3.6 %all-to-all-start.3 = ((bf16[4,256,512]{1,2,0:T(8,128)(2,1)}), bf16[4,256,512]{1,2,0:T(8,128)(2,1)S(1)}, u32[]{:S(2)}, u32[]{:S(2)}) async-start(bf16[4,256,512]{1,2,0:T(8,128)(2,1)} %broadcast_in_dim.28), calls=%async_computation.3 | async-start | bytes 2097152 | tf_op jit(solution)/shard_map/all_to_all | solution.py:15
  72.1 14.8 %all-to-all-done.3 = bf16[4,256,512]{1,2,0:T(8,128)(2,1)S(1)} async-done(((bf16[4,256,512]{1,2,0:T(8,128)(2,1)}), bf16[4,256,512]{1,2,0:T(8,128)(2,1)S(1)}, u32[]{:S(2)}, u32[]{:S(2)}) %all-to-all-start.3) | async-done | bytes 1048608 | tf_op jit(solution)/shard_map/all_to_all | solution.py:15
  87.0 0.3 fusion
  87.3 0.3 fusion.2
  87.6 0.7 copy-done.4
  88.3 0.5 fusion.10
  88.8 0.5 fusion.3
  89.3 0.5 copy-done.3
  89.9 0.2 convolution_convert_fusion.1
  90.1 0.2 convolution_convert_fusion.2
  90.3 0.2 convolution_convert_fusion.3
  90.5 0.2 convolution_convert_fusion.4
  90.8 16.4 %all_to_all.46 = bf16[4,256,512]{2,1,0:T(8,128)(2,1)S(1)} all-to-all(bf16[4,256,512]{2,1,0:T(8,128)(2,1)S(1)} %bitcast.88), channel_id=1, replica_groups=mesh['ep'=128,'tp'=4] {'tp'}, dimensions={0} | all-to-all | bytes 2097152 | tf_op jit(solution)/shard_map/all_to_all | solution.py:121
  107.3 0.2 reduce_sum.75
  107.5 0.8 all_to_all.36
  108.3 7.7 %all-to-all-start.5 = ((bf16[128,2,512]{2,1,0:T(2,128)(2,1)}), bf16[128,2,512]{2,1,0:T(2,128)(2,1)S(1)}, u32[]{:S(2)}, u32[]{:S(2)}) async-start(bf16[128,2,512]{2,1,0:T(2,128)(2,1)} %all_to_all.36), calls=%async_computation.5 | async-start | bytes 524288 | tf_op jit(solution)/shard_map/all_to_all | solution.py:123
  116.2 0.6 fusion.21
  116.8 21.8 %all-to-all-done.5 = bf16[128,2,512]{2,1,0:T(2,128)(2,1)S(1)} async-done(((bf16[128,2,512]{2,1,0:T(2,128)(2,1)}), bf16[128,2,512]{2,1,0:T(2,128)(2,1)S(1)}, u32[]{:S(2)}, u32[]{:S(2)}) %all-to-all-start.5) | async-done | bytes 262176 | tf_op jit(solution)/shard_map/all_to_all | solution.py:123
  138.7 0.1 fusion.46
  138.8 0.8 fusion.6
  (50 shorter events, 0.9 us)
Async XLA Ops:
  0.6 21.6 %copy-start = (bf16[1024,512]{1,0:T(8,128)(2,1)S(1)}, bf16[1024,512]{1,0:T(8,128)(2,1)}, u32[]{:S(2)}) copy-start(bf16[1024,512]{1,0:T(8,128)(2,1)} %param.34) | copy-start | bytes 3145732
  0.6 11.4 %copy-start.2 = (bf16[2048,256]{1,0:T(8,128)(2,1)S(1)}, bf16[2048,256]{1,0:T(8,128)(2,1)}, u32[]{:S(2)}) copy-start(bf16[2048,256]{1,0:T(8,128)(2,1)} %param.25) | copy-start | bytes 3145732
  2.3 9.4 %all-to-all-start = ((bf16[4,48,512]{2,1,0:T(8,128)(2,1)}), bf16[4,48,512]{2,1,0:T(8,128)(2,1)S(1)}, u32[]{:S(2)}, u32[]{:S(2)}) async-start(bf16[4,48,512]{2,1,0:T(8,128)(2,1)} %broadcast_in_dim.22), calls=%async_computation | async-start | bytes 393216 | tf_op jit(solution)/shard_map/all_to_all | solution.py:15
  11.8 0.9 copy-start.5
  11.8 0.9 copy-start.13
  11.8 0.9 copy-start.8
  11.8 0.9 copy-start.11
  12.0 0.9 copy-start.9
  12.0 1.0 copy-start.10
  12.0 1.0 copy-start.14
  12.0 1.0 copy-start.15
  12.0 1.3 copy-start.1
  13.0 9.2 %copy-start.6 = (bf16[48,512]{1,0:T(8,128)(2,1)S(1)}, bf16[48,512]{1,0:T(8,128)(2,1)}, u32[]{:S(2)}) copy-start(bf16[48,512]{1,0:T(8,128)(2,1)} %param.21) | copy-start | bytes 147460
  13.3 9.2 %copy-start.7 = (f32[48,256]{1,0:T(8,128)}, f32[48,256]{1,0:T(8,128)S(1)}, u32[]{:S(2)}) copy-start(f32[48,256]{1,0:T(8,128)S(1)} %fusion.37) | copy-start | bytes 147460
  14.3 7.9 %all-to-all-start.1 = ((bf16[4,48,256]{2,1,0:T(8,128)(2,1)}), bf16[4,48,256]{2,1,0:T(8,128)(2,1)S(1)}, u32[]{:S(2)}, u32[]{:S(2)}) async-start(bf16[4,48,256]{2,1,0:T(8,128)(2,1)} %broadcast_in_dim.24), calls=%async_computation.1 | async-start | bytes 196608 | tf_op jit(solution)/shard_map/all_to_all | solution.py:15
  68.5 3.7 %copy-start.12 = (f32[2048]{0:T(1024)S(1)}, f32[2048]{0:T(1024)}, u32[]{:S(2)}) copy-start(f32[2048]{0:T(1024)} %param.35) | copy-start | bytes 24580
  68.5 18.5 %all-to-all-start.3 = ((bf16[4,256,512]{1,2,0:T(8,128)(2,1)}), bf16[4,256,512]{1,2,0:T(8,128)(2,1)S(1)}, u32[]{:S(2)}, u32[]{:S(2)}) async-start(bf16[4,256,512]{1,2,0:T(8,128)(2,1)} %broadcast_in_dim.28), calls=%async_computation.3 | async-start | bytes 2097152 | tf_op jit(solution)/shard_map/all_to_all | solution.py:15
  87.3 1.0 copy-start.4
  87.6 1.2 copy-start.18
  88.8 1.0 copy-start.3
  107.2 8.8 %copy-start.16 = (f32[48,2]{0,1:T(2,128)S(1)}, f32[48,2]{0,1:T(2,128)}, u32[]{:S(2)}) copy-start(f32[48,2]{0,1:T(2,128)} %param.37) | copy-start | bytes 1156
  107.3 8.8 %copy-start.17 = (f32[48]{0:T(128)S(1)}, f32[48]{0:T(128)}, u32[]{:S(2)}) copy-start(f32[48]{0:T(128)} %param.38) | copy-start | bytes 580
  108.3 30.3 %all-to-all-start.5 = ((bf16[128,2,512]{2,1,0:T(2,128)(2,1)}), bf16[128,2,512]{2,1,0:T(2,128)(2,1)S(1)}, u32[]{:S(2)}, u32[]{:S(2)}) async-start(bf16[128,2,512]{2,1,0:T(2,128)(2,1)} %all_to_all.36), calls=%async_computation.5 | async-start | bytes 524288 | tf_op jit(solution)/shard_map/all_to_all | solution.py:123

commit v2 on v1

--- a/solution.py
+++ b/solution.py
@@ -1,9 +1,10 @@
 import jax
 import jax.numpy as jnp
 from jax import lax
+from jax.experimental import pallas as pl
+from jax.experimental.pallas import tpu as pltpu
 from jax.sharding import PartitionSpec as P
 
-PER_GROUP = 4
 EPS = 1e-06
 RATE = 8.0
 F32 = jnp.float32
@@ -24,6 +25,83 @@
 
 def dot(a, b):
     return jnp.dot(a, b, preferred_element_type=F32)
+
+
+VMEM = pl.BlockSpec(memory_space=pltpu.VMEM)
+SUM_ROWS = 16
+
+
+def call(kernel, shape, count):
+    return pl.pallas_call(
+        kernel,
+        out_shape=pltpu.VMEM(shape, BF16),
+        in_specs=[pl.BlockSpec(memory_space=pltpu.SMEM)] + [VMEM] * count,
+        out_specs=VMEM,
+    )
+
+
+def near(value):
+    return pltpu.with_memory_space_constraint(value, pltpu.VMEM)
+
+
+def first_products(member_ref, rows_ref, gain_ref, *refs):
+    *weight_refs, out_ref = refs
+    members = len(weight_refs)
+    rows = rows_ref[...].astype(F32)
+    count, width = rows.shape
+    half = width // 2
+    scaled = (rows * gain_ref[...]).astype(BF16)
+    for k, weight_ref in enumerate(weight_refs):
+        product = dot(scaled[:, :half], weight_ref[:half, :half]) + dot(
+            scaled[:, half:], weight_ref[:half, half:]
+        )
+        owner = lax.rem(member_ref[0] + (members - k), members)
+        out_ref[owner, :count, :] = product.astype(BF16)
+    squares = rows * rows
+    high = squares.astype(BF16)
+    low = (squares - high.astype(F32)).astype(BF16)
+    ones = jnp.ones((SUM_ROWS, width), BF16)
+    across = (((1,), (1,)), ((), ()))
+    sums = lax.dot_general(ones, high, across, preferred_element_type=F32) + lax.dot_general(
+        ones, low, across, preferred_element_type=F32
+    )
+    sums_high = sums.astype(BF16)
+    sums_low = (sums - sums_high.astype(F32)).astype(BF16)
+    place = lax.broadcasted_iota(jnp.int32, sums.shape, 0)
+    mixed = jnp.where(
+        place == 0,
+        sums_high.astype(F32),
+        jnp.where(place == 1, sums_low.astype(F32), 0.0),
+    ).astype(BF16)
+    for k in range(members):
+        out_ref[k, count:, :] = mixed
+
+
+def hidden_units(member_ref, parts_ref, out_ref):
+    members, total, width = parts_ref.shape
+    count = total - SUM_ROWS
+    half = width // 2
+    product = parts_ref[0, :count, :].astype(F32)
+    sums = parts_ref[0, count:, :].astype(F32)
+    for k in range(1, members):
+        product = product + parts_ref[k, :count, :].astype(F32)
+        sums = sums + parts_ref[k, count:, :].astype(F32)
+    row_sum = jnp.sum(jnp.transpose(sums), axis=1, keepdims=True)
+    product = product * lax.rsqrt(row_sum / (members * 512) + EPS)
+    gate = product[:, :half]
+    hidden = (gate * jax.nn.sigmoid(gate) * product[:, half:]).astype(BF16)
+    for k in range(members):
+        out_ref[k] = hidden
+
+
+def last_product(member_ref, hidden_ref, *refs):
+    *weight_refs, out_ref = refs
+    members, _, width = hidden_ref.shape
+    total = jnp.zeros(out_ref.shape, F32)
+    for k, weight_ref in enumerate(weight_refs):
+        owner = lax.rem(member_ref[0] + (members - k), members)
+        total = total + dot(hidden_ref[owner], weight_ref[weight_ref.shape[0] - width :, :])
+    out_ref[...] = total.astype(BF16)
 
 
 def block_gate(signal, weight, bias):
@@ -60,6 +138,7 @@
     members = lax.axis_size("tp")
     model_width = members * quarter
     experts = lax.axis_size("ep")
+    member = lax.axis_index("tp")
     top_count = route_ids.shape[1]
     capacity = 2
 
@@ -96,30 +175,48 @@
         -jnp.expm1(2.0 * log_rate)
     ) * inject_gate * conv_out.astype(F32)
     mixer_out = (new_state * jax.nn.gelu(branch_g.astype(F32))).astype(BF16)
-    mixed_out = dot(side_by_side(to_each(mixer_out, "tp")), output_weight)
+    mixer_copies = jnp.broadcast_to(mixer_out[None], (members, *mixer_out.shape))
+
+    gate_cut = expert_gate[0].reshape(members, 2, quarter // 2, -1)
+    up_cut = expert_up[0].reshape(members, 2, quarter // 2, -1)
+    down = expert_down[0]
+    down_cut = jnp.stack([down[:, m * quarter : (m + 1) * quarter] for m in range(members)])
+    cut = jnp.concatenate(
+        [
+            jnp.concatenate(
+                [gate_cut[:, 0], up_cut[:, 0], gate_cut[:, 1], up_cut[:, 1]], axis=2
+            ),
+            down_cut,
+        ],
+        axis=1,
+    )
+    gain_part = lax.dynamic_slice_in_dim(moe_gain, member * quarter, quarter, 0)[None]
+    cuts = [
+        lax.dynamic_index_in_dim(cut, lax.rem(member + k, members), 0, keepdims=False)
+        for k in range(members)
+    ]
+    mixer_copies, cuts, combine_high, combine_low, dispatch = lax.optimization_barrier(
+        (mixer_copies, cuts, combine_high, combine_low, dispatch)
+    )
+    mixer_parts = lax.all_to_all(mixer_copies, "tp", 0, 0, tiled=True)
+    weights = [cuts[0]]
+    for k in range(1, members):
+        ring = [(m, (m + k) % members) for m in range(members)]
+        weights.append(lax.ppermute(cuts[k], "tp", ring))
+    mixed_out = dot(side_by_side(mixer_parts), output_weight)
     stream = (tokens.astype(F32) + mixed_out).astype(BF16)
 
     outgoing = dot(dispatch, stream).astype(BF16)
     arrived = lax.all_to_all(outgoing, "ep", 0, 0, tiled=True)
-    rows = to_each(arrived, "tp").astype(F32)
-    row_scale = lax.rsqrt(jnp.sum(rows * rows, axis=(0, 2)) / model_width + EPS)
-    moe_in = (
-        rows * row_scale[None, :, None] * moe_gain.reshape(members, 1, quarter)
-    ).astype(BF16)
-    moe_in = side_by_side(moe_in)
-    gate_act = dot(moe_in, expert_gate[0])
-    up_act = dot(moe_in, expert_up[0])
-    hidden = (jax.nn.silu(gate_act) * up_act).astype(BF16)
-    down = expert_down[0]
-    partial_out = jnp.concatenate(
-        [
-            dot(hidden, down[:, m * quarter : (m + 1) * quarter]).astype(BF16)
-            for m in range(members)
-        ],
-        axis=0,
-    )
-    partial_in = lax.all_to_all(partial_out, "tp", 0, 0, tiled=True)
-    answer = jnp.sum(partial_in.reshape(members, slots, quarter).astype(F32), axis=0).astype(BF16)
+    weights = [near(w) for w in weights]
+    place = member.astype(jnp.int32)[None]
+    products = call(first_products, (members, slots + SUM_ROWS, 256), members + 2)(
+        place, near(arrived), near(gain_part), *weights
+    )
+    products = lax.all_to_all(products, "tp", 0, 0, tiled=True)
+    hidden = call(hidden_units, (members, slots, 128), 1)(place, near(products))
+    hidden = lax.all_to_all(hidden, "tp", 0, 0, tiled=True)
+    answer = call(last_product, (slots, quarter), members + 1)(place, near(hidden), *weights)
     returned = lax.all_to_all(answer, "ep", 0, 0, tiled=True)
     routed = dot(combine_high, returned) + dot(combine_low, returned)
     result = (stream.astype(F32) + routed).astype(BF16)

time: 140 us -> 143 us (1.021)
  starting transfers between devices: 18.9 us -> 52.6 us
  blocking collectives: 60.7 us -> 29.9 us
  waiting for transfers between devices: 42.7 us -> 36.9 us
  local copies, waits for them, and re-layouts: 8.2 us -> 12.7 us
    all_to_all x2 -> x3, blocking collectives: 60.7 us -> 29.9 us  [the longest x1 13.3 us: body(): products = lax.all_to_all(products, 'tp', 0, 0, tiled=True)]
    all_to_all x0 -> x1, starting transfers between devices: none -> 21.3 us  [body(): arrived = lax.all_to_all(outgoing, 'ep', 0, 0, tiled=True)]
    all_to_all x3 -> x1, waiting for transfers between devices: 20.9 us -> 0.01 us  [to_each(): lax.all_to_all(jnp.broadcast_to(value[None], (size, *value.shape)), axis,...]
    all_to_all x0 -> x1, waiting for transfers between devices: none -> 13.4 us  [body(): arrived = lax.all_to_all(outgoing, 'ep', 0, 0, tiled=True)]
    all_to_all x1, starting transfers between devices: 7.72 us -> 18.8 us  [body(): returned = lax.all_to_all(answer, 'ep', 0, 0, tiled=True)]
    ppermute x0 -> x3, starting transfers between devices: none -> 8.42 us  [body(): weights.append(lax.ppermute(cuts[k], 'tp', ring))]
    all_to_all x3 -> x1, starting transfers between devices: 11.1 us -> 4.18 us  [to_each(): lax.all_to_all(jnp.broadcast_to(value[None], (size, *value.shape)), axis,...]
    unnamed x39 -> x65, local copies, waits for them, and re-layouts: 2.57 us -> 5.13 us
  transfers between devices with their start and end apart: 4 -> 6, of which waited for: 4 -> 3; matrix products, arithmetic and copies ran while one was open for 3% -> 5% of each run, Pallas kernels for 0% -> 0%
where the time goes in v2:
time: 143 us; the launch traced here: 142 us
  starting transfers between devices  52.6 us (37%)
  waiting for transfers between devices  36.9 us (26%)
  blocking collectives  29.9 us (21%)
  local copies, waits for them, and re-layouts  12.7 us (9%)
  matrix products  3.8 us (3%)
  other arithmetic  3.63 us (3%)
    all_to_all x1, waiting for transfers between devices, body(): returned = lax.all_to_all(answer, 'ep', 0, 0, tiled=True)  21.9 us
    all_to_all x1, starting transfers between devices, body(): arrived = lax.all_to_all(outgoing, 'ep', 0, 0, tiled=True)  21.3 us
    all_to_all x1, starting transfers between devices, body(): returned = lax.all_to_all(answer, 'ep', 0, 0, tiled=True)  18.8 us
    all_to_all x1, waiting for transfers between devices, body(): arrived = lax.all_to_all(outgoing, 'ep', 0, 0, tiled=True)  13.4 us
    all_to_all x1, blocking collectives, body(): products = lax.all_to_all(products, 'tp', 0, 0, tiled=True)  13.3 us
    all_to_all x1, blocking collectives, body(): mixer_parts = lax.all_to_all(mixer_copies, 'tp', 0, 0, tiled=True)  8.69 us
    ppermute x3, starting transfers between devices, body(): weights.append(lax.ppermute(cuts[k], 'tp', ring))  8.42 us
    all_to_all x1, blocking collectives, body(): hidden = lax.all_to_all(hidden, 'tp', 0, 0, tiled=True)  7.92 us
  transfers between devices with their start and end apart: 6, of which 3 were waited for; matrix products, arithmetic and copies ran while one was open for 5% of the time, Pallas kernels for 0%

profile of v2, /device:TPU:33, one launch (start us, length us, event | category | flops | bytes accessed | tf_op | source)
XLA Modules:
  0.0 141.9 jit_solution(16882558286879175647)
XLA Ops:
  0.7 1.6 %broadcast_in_dim.22 = bf16[4,48,512]{2,1,0:T(8,128)(2,1)} broadcast(bf16[48,512]{1,0:T(8,128)(2,1)} %param.21), dimensions={1,2} | broadcast | bytes 245760 | tf_op jit(solution)/shard_map/broadcast_in_dim | solution.py:17
  2.3 4.2 %all-to-all-start = ((bf16[4,48,512]{2,1,0:T(8,128)(2,1)}), bf16[4,48,512]{2,1,0:T(8,128)(2,1)S(1)}, u32[]{:S(2)}, u32[]{:S(2)}) async-start(bf16[4,48,512]{2,1,0:T(8,128)(2,1)} %broadcast_in_dim.22), calls=%async_computation | async-start | bytes 393216 | tf_op jit(solution)/shard_map/all_to_all | solution.py:16
  6.5 1.9 %slice_bitcast_fusion.7 = (bf16[1,128,512]{2,1,0:T(8,128)(2,1)S(1)}, bf16[1,128,512]{2,1,0:T(8,128)(2,1)}, bf16[1,128,512]{2,1,0:T(8,128)(2,1)}, bf16[1,128,512]{2,1,0:T(8,128)(2,1)}) fusion(bf16[128,2048]{1,0:T(8,128)(2,1)} %bitcast.113), kind=kLoop, calls=%fused_computation.31 | loop fusion | bytes 1048576 | tf_op jit(solution)/shard_map/stack | solution.py:183
  8.4 0.1 copy.79
  8.5 0.1 eq.42
  8.7 0.1 reduce_window_sum.11
  8.9 0.2 select_reduce_fusion.1
  9.0 0.1 reshape.56
  9.3 0.1 fusion.9
  9.4 0.1 select_reduce_fusion
  9.5 0.6 subtract_convert_fusion
  10.2 0.8 copy-done.12
  11.2 1.4 maximum_maximum_fusion
  12.5 1.1 dynamic-slice_bitcast_fusion
  13.7 0.1 fusion.5
  13.8 0.1 fusion.8
  14.0 1.8 %fusion.4 = bf16[48,1,256]{2,0,1:T(8,128)(2,1)S(1)} fusion(bf16[48,2048]{1,0:T(8,128)(2,1)S(1)} %bitcast.111, bf16[2048,256]{1,0:T(8,128)(2,1)} %param.25), kind=kOutput, calls=%fused_computation.12 | convolution fusion | flops 50343936 | bytes 1269760 | tf_op jit(solution)/shard_map/dot_general | solution.py:27
  15.8 0.1 convolution_bitcast_fusion
  16.0 0.1 convolution_bitcast_fusion.1
  16.3 0.3 fusion.19
  16.6 8.7 %all_to_all.43 = bf16[4,48,256]{2,1,0:T(8,128)(2,1)S(1)} all-to-all(bf16[4,48,256]{2,1,0:T(8,128)(2,1)S(1)} %broadcast_in_dim.24), channel_id=1, replica_groups=mesh['ep'=128,'tp'=4] {'tp'}, dimensions={0} | all-to-all | bytes 196608 | tf_op jit(solution)/shard_map/all_to_all | solution.py:201
  25.3 0.3 fusion.1
  25.6 0.2 convolution_convert_fusion
  25.9 0.8 all_to_all.29
  26.7 21.3 %all-to-all-start.2 = ((bf16[128,2,512]{2,1,0:T(2,128)(2,1)}), bf16[128,2,512]{2,1,0:T(2,128)(2,1)S(1)}, u32[]{:S(2)}, u32[]{:S(2)}) async-start(bf16[128,2,512]{2,1,0:T(2,128)(2,1)} %all_to_all.29), calls=%async_computation.2 | async-start | bytes 524288 | tf_op jit(solution)/shard_map/all_to_all | solution.py:210
  48.0 2.2 %collective-permute-start = (bf16[384,512]{1,0:T(8,128)(2,1)}, bf16[384,512]{1,0:T(8,128)(2,1)S(1)}, u32[]{:S(2)}, u32[]{:S(2)}) collective-permute-start(bf16[384,512]{1,0:T(8,128)(2,1)} %get-tuple-element.15), channel_id=1, source_target_pairs={{0,1},{1,2},{2,3},{3,0},{4,5},{5,6},{6,7},{7,4},{8,9},{9,10},{10,1... | collective-permute-start | bytes 1179656 | tf_op jit(solution)/shard_map/ppermute | solution.py:205
  50.2 3.7 %collective-permute-start.1 = (bf16[384,512]{1,0:T(8,128)(2,1)}, bf16[384,512]{1,0:T(8,128)(2,1)S(1)}, u32[]{:S(2)}, u32[]{:S(2)}) collective-permute-start(bf16[384,512]{1,0:T(8,128)(2,1)} %get-tuple-element.16), channel_id=1, source_target_pairs={{0,2},{1,3},{2,0},{3,1},{4,6},{5,7},{6,4},{7,5},{8,10},{9,11},{10,... | collective-permute-start | bytes 1179656 | tf_op jit(solution)/shard_map/ppermute | solution.py:205
  53.9 2.5 %collective-permute-start.2 = (bf16[384,512]{1,0:T(8,128)(2,1)}, bf16[384,512]{1,0:T(8,128)(2,1)S(1)}, u32[]{:S(2)}, u32[]{:S(2)}) collective-permute-start(bf16[384,512]{1,0:T(8,128)(2,1)} %get-tuple-element.17), channel_id=1, source_target_pairs={{0,3},{1,0},{2,1},{3,2},{4,7},{5,4},{6,5},{7,6},{8,11},{9,8},{10,9... | collective-permute-start | bytes 1179656 | tf_op jit(solution)/shard_map/ppermute | solution.py:205
  56.4 0.8 dynamic_slice.20
  57.2 13.4 %all-to-all-done.2 = bf16[128,2,512]{2,1,0:T(2,128)(2,1)S(1)} async-done(((bf16[128,2,512]{2,1,0:T(2,128)(2,1)}), bf16[128,2,512]{2,1,0:T(2,128)(2,1)S(1)}, u32[]{:S(2)}, u32[]{:S(2)}) %all-to-all-start.2) | async-done | bytes 262176 | tf_op jit(solution)/shard_map/all_to_all | solution.py:210
  70.5 0.1 all_to_all.31.rows_ref
  70.7 1.6 %collective-permute-done.2.refs_3_ = bf16[384,512]{1,0:T(8,128)(2,1)S(1)} collective-permute-done((bf16[384,512]{1,0:T(8,128)(2,1)}, bf16[384,512]{1,0:T(8,128)(2,1)S(1)}, u32[]{:S(2)}, u32[]{:S(2)}) %collective-permute-start.2) | collective-permute-done | bytes 393248 | tf_op jit(solution)/shard_map/ppermute | solution.py:205
  72.3 0.5 shard_map.220
  72.9 13.3 %all_to_all.44.parts_ref = bf16[4,272,256]{2,1,0:T(8,128)(2,1)S(1)} all-to-all(bf16[4,272,256]{2,1,0:T(8,128)(2,1)S(1)} %shard_map.220), channel_id=1, replica_groups=mesh['ep'=128,'tp'=4] {'tp'}, dimensions={0} | all-to-all | bytes 1114112 | tf_op jit(solution)/shard_map/all_to_all | solution.py:216
  86.1 0.2 shard_map.221
  86.3 7.9 %all_to_all.45.hidden_ref = bf16[4,256,128]{2,1,0:T(8,128)(2,1)S(1)} all-to-all(bf16[4,256,128]{2,1,0:T(8,128)(2,1)S(1)} %shard_map.221), channel_id=1, replica_groups=mesh['ep'=128,'tp'=4] {'tp'}, dimensions={0} | all-to-all | bytes 524288 | tf_op jit(solution)/shard_map/all_to_all | solution.py:218
  94.3 1.0 copy-done.2
  95.3 1.0 copy-done.4
  96.3 1.0 copy-done.6
  97.3 1.0 copy-done.8
  98.3 0.4 shard_map.222
  98.7 0.8 all_to_all.34
  99.5 18.8 %all-to-all-start.5 = ((bf16[128,2,512]{2,1,0:T(2,128)(2,1)}), bf16[128,2,512]{2,1,0:T(2,128)(2,1)S(1)}, u32[]{:S(2)}, u32[]{:S(2)}) async-start(bf16[128,2,512]{2,1,0:T(2,128)(2,1)} %all_to_all.34), calls=%async_computation.5 | async-start | bytes 524288 | tf_op jit(solution)/shard_map/all_to_all | solution.py:220
  118.3 0.6 fusion.10
  118.9 21.9 %all-to-all-done.5 = bf16[128,2,512]{2,1,0:T(2,128)(2,1)S(1)} async-done(((bf16[128,2,512]{2,1,0:T(2,128)(2,1)}), bf16[128,2,512]{2,1,0:T(2,128)(2,1)S(1)}, u32[]{:S(2)}, u32[]{:S(2)}) %all-to-all-start.5) | async-done | bytes 262176 | tf_op jit(solution)/shard_map/all_to_all | solution.py:220
  140.9 0.1 all_to_all.36
  141.0 0.1 fusion.37
  141.1 0.8 fusion.2
  (77 shorter events, 0.7 us)
Async XLA Ops:
  0.6 24.7 %copy-start = (bf16[1024,512]{1,0:T(8,128)(2,1)S(1)}, bf16[1024,512]{1,0:T(8,128)(2,1)}, u32[]{:S(2)}) copy-start(bf16[1024,512]{1,0:T(8,128)(2,1)} %param.34) | copy-start | bytes 3145732
  0.6 7.7 %copy-start.24 = (f32[2048]{0:T(1024)S(1)}, f32[2048]{0:T(1024)}, u32[]{:S(2)}) copy-start(f32[2048]{0:T(1024)} %param.24) | copy-start | bytes 24580
  0.7 7.7 %copy-start.30 = (f32[256]{0:T(256)S(1)}, f32[256]{0:T(256)}, u32[]{:S(2)}) copy-start(f32[256]{0:T(256)} %param.33) | copy-start | bytes 3076
  0.7 7.8 %copy-start.26 = (s32[48,2]{0,1:T(2,128)S(1)}, s32[48,2]{0,1:T(2,128)}, u32[]{:S(2)}) copy-start(s32[48,2]{0,1:T(2,128)} %param.36) | copy-start | bytes 1156
  0.7 8.6 %copy-start.29 = (f32[48,2]{0,1:T(2,128)S(1)}, f32[48,2]{0,1:T(2,128)}, u32[]{:S(2)}) copy-start(f32[48,2]{0,1:T(2,128)} %param.37) | copy-start | bytes 1156
  0.7 8.7 %copy-start.31 = (f32[48]{0:T(128)S(1)}, f32[48]{0:T(128)}, u32[]{:S(2)}) copy-start(f32[48]{0:T(128)} %param.38) | copy-start | bytes 580
  0.7 9.5 %copy-start.11 = (bf16[1,2048,128]{2,1,0:T(8,128)(2,1)S(1)}, bf16[1,2048,128]{2,1,0:T(8,128)(2,1)}, u32[]{:S(2)}) copy-start(bf16[1,2048,128]{2,1,0:T(8,128)(2,1)} %param.39) | copy-start | bytes 1572868
  0.7 9.5 %copy-start.10 = (bf16[1,2048,128]{2,1,0:T(8,128)(2,1)S(1)}, bf16[1,2048,128]{2,1,0:T(8,128)(2,1)}, u32[]{:S(2)}) copy-start(bf16[1,2048,128]{2,1,0:T(8,128)(2,1)} %param.40) | copy-start | bytes 1572868
  2.3 11.3 %all-to-all-start = ((bf16[4,48,512]{2,1,0:T(8,128)(2,1)}), bf16[4,48,512]{2,1,0:T(8,128)(2,1)S(1)}, u32[]{:S(2)}, u32[]{:S(2)}) async-start(bf16[4,48,512]{2,1,0:T(8,128)(2,1)} %broadcast_in_dim.22), calls=%async_computation | async-start | bytes 393216 | tf_op jit(solution)/shard_map/all_to_all | solution.py:16
  10.1 0.9 copy-start.12
  10.1 1.0 copy-start.13
  10.1 1.0 copy-start.14
  13.6 58.7 %copy-start.1 = (bf16[384,512]{1,0:T(8,128)(2,1)}, bf16[384,512]{1,0:T(8,128)(2,1)S(1)}, u32[]{:S(2)}) copy-start(bf16[384,512]{1,0:T(8,128)(2,1)S(1)} %get-tuple-element.14.refs_0_) | copy-start | bytes 1179652
  13.6 2.2 %copy-start.15 = (bf16[48,3,256]{2,0,1:T(8,128)(2,1)S(1)}, bf16[48,3,256]{2,0,1:T(8,128)(2,1)}, u32[]{:S(2)}) copy-start(bf16[48,3,256]{2,0,1:T(8,128)(2,1)} %param.22) | copy-start | bytes 221188
  13.6 2.2 %copy-start.25 = (f32[4,256]{1,0:T(4,128)S(1)}, f32[4,256]{1,0:T(4,128)}, u32[]{:S(2)}) copy-start(f32[4,256]{1,0:T(4,128)} %param.27) | copy-start | bytes 12292
  13.6 2.2 %copy-start.20 = (bf16[2,128,128]{2,1,0:T(8,128)(2,1)S(1)}, bf16[2,128,128]{2,1,0:T(8,128)(2,1)}, u32[]{:S(2)}) copy-start(bf16[2,128,128]{2,1,0:T(8,128)(2,1)} %param.31) | copy-start | bytes 196612
  13.6 2.2 %copy-start.23 = (f32[256]{0:T(256)S(1)}, f32[256]{0:T(256)}, u32[]{:S(2)}) copy-start(f32[256]{0:T(256)} %param.28) | copy-start | bytes 3076
  13.6 2.4 %copy-start.21 = (bf16[2,128,128]{2,1,0:T(8,128)(2,1)S(1)}, bf16[2,128,128]{2,1,0:T(8,128)(2,1)}, u32[]{:S(2)}) copy-start(bf16[2,128,128]{2,1,0:T(8,128)(2,1)} %param.29) | copy-start | bytes 196612
  13.6 2.5 %copy-start.22 = (f32[48,256]{1,0:T(8,128)S(1)}, f32[48,256]{1,0:T(8,128)}, u32[]{:S(2)}) copy-start(f32[48,256]{1,0:T(8,128)} %param.23) | copy-start | bytes 147460
  13.6 2.5 %copy-start.27 = (f32[256]{0:T(256)S(1)}, f32[256]{0:T(256)}, u32[]{:S(2)}) copy-start(f32[256]{0:T(256)} %param.32) | copy-start | bytes 3076
  13.6 2.5 %copy-start.28 = (f32[256]{0:T(256)S(1)}, f32[256]{0:T(256)}, u32[]{:S(2)}) copy-start(f32[256]{0:T(256)} %param.30) | copy-start | bytes 3076
  13.7 2.6 %copy-start.9 = (bf16[2048,256]{1,0:T(8,128)(2,1)S(1)}, bf16[2048,256]{1,0:T(8,128)(2,1)}, u32[]{:S(2)}) copy-start(bf16[2048,256]{1,0:T(8,128)(2,1)} %param.26) | copy-start | bytes 3145732
  15.8 9.5 %copy-start.17 = (bf16[48,512]{1,0:T(8,128)(2,1)S(1)}, bf16[48,512]{1,0:T(8,128)(2,1)}, u32[]{:S(2)}) copy-start(bf16[48,512]{1,0:T(8,128)(2,1)} %param.21) | copy-start | bytes 147460
  16.2 9.0 %copy-start.18 = (f32[48,256]{1,0:T(8,128)}, f32[48,256]{1,0:T(8,128)S(1)}, u32[]{:S(2)}) copy-start(f32[48,256]{1,0:T(8,128)S(1)} %fusion.26) | copy-start | bytes 147460
  26.7 43.8 %all-to-all-start.2 = ((bf16[128,2,512]{2,1,0:T(2,128)(2,1)}), bf16[128,2,512]{2,1,0:T(2,128)(2,1)S(1)}, u32[]{:S(2)}, u32[]{:S(2)}) async-start(bf16[128,2,512]{2,1,0:T(2,128)(2,1)} %all_to_all.29), calls=%async_computation.2 | async-start | bytes 524288 | tf_op jit(solution)/shard_map/all_to_all | solution.py:210
  48.0 22.7 %collective-permute-start = (bf16[384,512]{1,0:T(8,128)(2,1)}, bf16[384,512]{1,0:T(8,128)(2,1)S(1)}, u32[]{:S(2)}, u32[]{:S(2)}) collective-permute-start(bf16[384,512]{1,0:T(8,128)(2,1)} %get-tuple-element.15), channel_id=1, source_target_pairs={{0,1},{1,2},{2,3},{3,0},{4,5},{5,6},{6,7},{7,4},{8,9},{9,10},{10,1... | collective-permute-start | bytes 1179656 | tf_op jit(solution)/shard_map/ppermute | solution.py:205
  50.2 20.5 %collective-permute-start.1 = (bf16[384,512]{1,0:T(8,128)(2,1)}, bf16[384,512]{1,0:T(8,128)(2,1)S(1)}, u32[]{:S(2)}, u32[]{:S(2)}) collective-permute-start(bf16[384,512]{1,0:T(8,128)(2,1)} %get-tuple-element.16), channel_id=1, source_target_pairs={{0,2},{1,3},{2,0},{3,1},{4,6},{5,7},{6,4},{7,5},{8,10},{9,11},{10,... | collective-permute-start | bytes 1179656 | tf_op jit(solution)/shard_map/ppermute | solution.py:205
  53.9 18.5 %collective-permute-start.2 = (bf16[384,512]{1,0:T(8,128)(2,1)}, bf16[384,512]{1,0:T(8,128)(2,1)S(1)}, u32[]{:S(2)}, u32[]{:S(2)}) collective-permute-start(bf16[384,512]{1,0:T(8,128)(2,1)} %get-tuple-element.17), channel_id=1, source_target_pairs={{0,3},{1,0},{2,1},{3,2},{4,7},{5,4},{6,5},{7,6},{8,11},{9,8},{10,9... | collective-permute-start | bytes 1179656 | tf_op jit(solution)/shard_map/ppermute | solution.py:205
  70.7 2.2 %copy-start.3 = (bf16[384,512]{1,0:T(8,128)(2,1)}, bf16[384,512]{1,0:T(8,128)(2,1)S(1)}, u32[]{:S(2)}) copy-start(bf16[384,512]{1,0:T(8,128)(2,1)S(1)} %collective-permute-done.refs_1_) | copy-start | bytes 1179652
  70.7 15.5 %copy-start.5 = (bf16[384,512]{1,0:T(8,128)(2,1)}, bf16[384,512]{1,0:T(8,128)(2,1)S(1)}, u32[]{:S(2)}) copy-start(bf16[384,512]{1,0:T(8,128)(2,1)S(1)} %collective-permute-done.1.refs_2_) | copy-start | bytes 1179652
  72.3 13.8 %copy-start.7 = (bf16[384,512]{1,0:T(8,128)(2,1)}, bf16[384,512]{1,0:T(8,128)(2,1)S(1)}, u32[]{:S(2)}) copy-start(bf16[384,512]{1,0:T(8,128)(2,1)S(1)} %collective-permute-done.2.refs_3_) | copy-start | bytes 1179652
  94.3 1.0 copy-start.2
  95.3 1.0 copy-start.4
  96.3 1.0 copy-start.6
  97.3 1.0 copy-start.8
  98.2 20.0 %copy-start.16 = (bf16[48,3,256]{2,0,1:T(8,128)(2,1)S(1)}, bf16[48,3,256]{2,0,1:T(8,128)(2,1)}, u32[]{:S(2)}) copy-start(bf16[48,3,256]{2,0,1:T(8,128)(2,1)} %param.22) | copy-start | bytes 221188
  98.7 42.4 %copy-start.19 = (bf16[48,256]{1,0:T(8,128)(2,1)S(1)}, bf16[48,256]{1,0:T(8,128)(2,1)}, u32[]{:S(2)}) copy-start(bf16[48,256]{1,0:T(8,128)(2,1)} %get-tuple-element.12) | copy-start | bytes 73732
  99.5 41.4 %all-to-all-start.5 = ((bf16[128,2,512]{2,1,0:T(2,128)(2,1)}), bf16[128,2,512]{2,1,0:T(2,128)(2,1)S(1)}, u32[]{:S(2)}, u32[]{:S(2)}) async-start(bf16[128,2,512]{2,1,0:T(2,128)(2,1)} %all_to_all.34), calls=%async_computation.5 | async-start | bytes 524288 | tf_op jit(solution)/shard_map/all_to_all | solution.py:220

commit v3 on v1

v3 whole, which is shorter than its diff:
```python
import jax
import jax.numpy as jnp
from jax import lax
from jax.experimental import pallas as pl
from jax.experimental.pallas import tpu as pltpu
from jax.sharding import PartitionSpec as P

EPS = 1e-06
RATE = 8.0
CAPACITY = 2
SUM_ROWS = 16
F32 = jnp.float32
BF16 = jnp.bfloat16
VMEM = pl.BlockSpec(memory_space=pltpu.VMEM)
SMEM = pl.BlockSpec(memory_space=pltpu.SMEM)


def near(value):
    return pltpu.with_memory_space_constraint(value, pltpu.VMEM)


def call(kernel, outs, *args, scalar=None):
    scalars = () if scalar is None else (scalar,)
    return pl.pallas_call(
        kernel,
        out_shape=outs,
        in_specs=[SMEM] * len(scalars) + [VMEM] * len(args),
        out_specs=jax.tree.map(lambda _: VMEM, outs),
    )(*scalars, *args)


def dot(a, b):
    return jnp.dot(a, b, preferred_element_type=F32)


def dot_on(a, b, a_dim, b_dim):
    return lax.dot_general(a, b, (((a_dim,), (b_dim,)), ((), ())), preferred_element_type=F32)


def halves(value):
    high = value.astype(BF16)
    return high, (value - high.astype(F32)).astype(BF16)


def places(ids_ref, count, slots):
    ids = ids_ref[...]
    column = lax.broadcasted_iota(jnp.int32, (count, slots), 1)
    expert = lax.div(column, CAPACITY)
    place = lax.rem(column, CAPACITY)
    first = ids[:, 0:1] == expert
    second = ids[:, 1:2] == expert
    named = jnp.where(first | second, 1.0, 0.0)
    below = lax.broadcasted_iota(jnp.int32, (count, count), 1) < lax.broadcasted_iota(
        jnp.int32, (count, count), 0
    )
    earlier = dot(jnp.where(below, 1.0, 0.0).astype(BF16), named.astype(BF16))
    return jnp.where(earlier == place.astype(F32), named, 0.0), first


def dispatch_table(ids_ref, out_ref):
    out_ref[...] = places(ids_ref, *out_ref.shape)[0].astype(BF16)


def combine_tables(ids_ref, logits_ref, group_ref, high_ref, low_ref):
    hit, first = places(ids_ref, *high_ref.shape)
    raised = jnp.exp(logits_ref[...])
    weight = group_ref[...] * raised / (raised[:, 0:1] + raised[:, 1:2])
    high, low = halves(hit * jnp.where(first, weight[:, 0:1], weight[:, 1:2]))
    high_ref[...] = high
    low_ref[...] = low


def cut_weights(member_ref, gate_ref, up_ref, down_ref, *refs):
    *out_refs, done = refs
    members = len(out_refs)
    quarter = gate_ref.shape[1] // members
    half = quarter // 2
    width = gate_ref.shape[2]
    copies = []
    for k, out_ref in enumerate(out_refs):
        target = lax.rem(member_ref[0] + k, members)
        top = pl.multiple_of(target * quarter, quarter)
        pairs = [(down_ref.at[0, :, pl.ds(top, quarter)], out_ref.at[pl.ds(half, width), :])]
        for part in range(2):
            rows = pl.ds(pl.multiple_of(top + part * half, half), half)
            at = part * 2 * width
            into = [out_ref.at[pl.ds(0, half), pl.ds(at + j * width, width)] for j in range(2)]
            pairs += [(gate_ref.at[0, rows, :], into[0]), (up_ref.at[0, rows, :], into[1])]
        copies += [
            pltpu.make_async_copy(source, into, done.at[k, j])
            for j, (source, into) in enumerate(pairs)
        ]
    for copy in copies:
        copy.start()
    for copy in copies:
        copy.wait()


def block_gate(signal, weight, bias):
    blocks = weight.shape[0]
    grouped = signal.reshape(signal.shape[0], blocks, -1)
    mixed_out = jnp.einsum("sbi,bij->sbj", grouped, weight, preferred_element_type=F32)
    return jax.nn.sigmoid(mixed_out.reshape(signal.shape[0], -1) + bias)


def side_by_side(parts):
    size, rows, width = parts.shape
    return jnp.swapaxes(parts, 0, 1).reshape(rows, size * width)


def first_products(member_ref, rows_ref, gain_ref, weight_ref, out_ref, down_ref):
    members = weight_ref.shape[0]
    rows = rows_ref[...].astype(F32)
    count, width = rows.shape
    half = width // 2
    scaled = (rows * gain_ref[...]).astype(BF16)
    squares = rows * rows
    high, low = halves(squares)
    ones = jnp.ones((SUM_ROWS, width), BF16)
    sums_high, sums_low = halves(dot_on(ones, high, 1, 1) + dot_on(ones, low, 1, 1))
    place = lax.broadcasted_iota(jnp.int32, (SUM_ROWS, count), 0)
    sums = jnp.where(
        place == 0, sums_high.astype(F32), jnp.where(place == 1, sums_low.astype(F32), 0.0)
    ).astype(BF16)
    for k in range(members):
        product = dot(scaled[:, :half], weight_ref[k, :half, :half]) + dot(
            scaled[:, half:], weight_ref[k, :half, half:]
        )
        owner = lax.rem(member_ref[0] + (members - k), members)
        out_ref[owner, :count, :] = product.astype(BF16)
        out_ref[owner, count:, :] = sums
        down_ref[owner] = weight_ref[k, half:, :]


def hidden_units(parts_ref, out_ref):
    members, total, width = parts_ref.shape
    count = total - SUM_ROWS
    half = width // 2
    product = parts_ref[0, :count, :].astype(F32)
    sums = parts_ref[0, count:, :].astype(F32)
    for k in range(1, members):
        product = product + parts_ref[k, :count, :].astype(F32)
        sums = sums + parts_ref[k, count:, :].astype(F32)
    row_sum = jnp.sum(jnp.transpose(sums), axis=1, keepdims=True)
    product = product * lax.rsqrt(row_sum / (members * 2 * width) + EPS)
    gate = product[:, :half]
    hidden = (gate * jax.nn.sigmoid(gate) * product[:, half:]).astype(BF16)
    for k in range(members):
        out_ref[k] = hidden


def last_product(hidden_ref, down_ref, out_ref):
    total = dot(hidden_ref[0], down_ref[0])
    for k in range(1, hidden_ref.shape[0]):
        total = total + dot(hidden_ref[k], down_ref[k])
    out_ref[...] = total.astype(BF16)


def body(
    tokens,
    conv_state,
    lru_state,
    mix_gain,
    input_weight,
    branch_weight,
    conv_taps,
    conv_bias,
    recur_weight,
    recur_bias,
    inject_weight,
    inject_bias,
    decay_param,
    output_weight,
    moe_gain,
    route_ids,
    route_logits,
    group_weight,
    expert_gate,
    expert_up,
    expert_down,
):
    seq_count, quarter = tokens.shape
    members = lax.axis_size("tp")
    experts = lax.axis_size("ep")
    member = lax.axis_index("tp")
    place = member.astype(jnp.int32)[None]
    slots = experts * CAPACITY
    units = expert_gate.shape[2]

    token_parts = lax.all_to_all(
        jnp.broadcast_to(tokens[None], (members, *tokens.shape)), "tp", 0, 0, tiled=True
    )
    anywhere = pl.BlockSpec(memory_space=pl.ANY)
    pieces = pl.pallas_call(
        cut_weights,
        out_shape=[pltpu.VMEM((quarter // 2 + units, quarter), BF16)] * members,
        in_specs=[SMEM] + [anywhere] * 3,
        out_specs=[VMEM] * members,
        scratch_shapes=[pltpu.SemaphoreType.DMA((members, 5))],
    )(place, expert_gate, expert_up, expert_down)
    table = pltpu.VMEM((seq_count, slots), BF16)
    dispatch = call(dispatch_table, table, route_ids)
    combine_high, combine_low = call(
        combine_tables, [table] * 2, route_ids, route_logits, group_weight[:, None]
    )
    wide = token_parts.astype(F32)
    scale = lax.rsqrt(jnp.sum(wide * wide, axis=(0, 2)) / (members * quarter) + EPS)
    normed = (wide * scale[None, :, None] * mix_gain.reshape(members, 1, quarter)).astype(BF16)
    normed = side_by_side(normed)
    branch_x = dot(normed, input_weight).astype(BF16)
    branch_g = dot(normed, branch_weight).astype(BF16)
    window = jnp.concatenate([conv_state, branch_x[:, None, :]], axis=1)
    conv_sum = conv_bias + jnp.sum(window.astype(F32) * conv_taps[None], axis=1)
    conv_out = conv_sum.astype(BF16)
    recur_gate = block_gate(conv_out, recur_weight, recur_bias)
    inject_gate = block_gate(conv_out, inject_weight, inject_bias)
    log_rate = -RATE * recur_gate * jax.nn.softplus(-decay_param)
    new_state = jnp.exp(log_rate) * lru_state + jnp.sqrt(
        -jnp.expm1(2.0 * log_rate)
    ) * inject_gate * conv_out.astype(F32)
    mixer_out = (new_state * jax.nn.gelu(branch_g.astype(F32))).astype(BF16)
    copies = jnp.broadcast_to(mixer_out[None], (members, *mixer_out.shape))
    gain_part = lax.dynamic_slice_in_dim(moe_gain, member * quarter, quarter, 0)[None]
    copies, *sends = lax.optimization_barrier((copies, *pieces[1:]))
    mixer_parts = lax.all_to_all(copies, "tp", 0, 0, tiled=True)
    weights = [pieces[0]]
    for k in range(1, members):
        ring = [(m, (m + k) % members) for m in range(members)]
        weights.append(lax.ppermute(sends[k - 1], "tp", ring))
    stream = (tokens.astype(F32) + dot(side_by_side(mixer_parts), output_weight)).astype(BF16)

    outgoing = dot_on(dispatch, stream, 0, 0).astype(BF16).reshape(experts, CAPACITY, quarter)
    arrived = lax.all_to_all(outgoing, "ep", 0, 0, tiled=True)
    arrived = arrived.reshape(slots, quarter)
    products, down = call(
        first_products,
        [
            pltpu.VMEM((members, slots + SUM_ROWS, 2 * units), BF16),
            pltpu.VMEM((members, units, quarter), BF16),
        ],
        near(arrived),
        gain_part,
        near(jnp.stack(weights)),
        scalar=place,
    )
    products = lax.all_to_all(products, "tp", 0, 0, tiled=True)
    hidden = call(hidden_units, pltpu.VMEM((members, slots, units), BF16), near(products))
    hidden = lax.all_to_all(hidden, "tp", 0, 0, tiled=True)
    answer = call(
        last_product, pltpu.VMEM((slots, quarter), BF16), near(hidden), near(down)
    )
    returned = lax.all_to_all(answer, "ep", 0, 0, tiled=True)
    routed = dot(combine_high, returned) + dot(combine_low, returned)
    result = (stream.astype(F32) + routed).astype(BF16)
    return (result, new_state, window[:, 1:])


def solution(mesh):
    in_specs = (
        P("ep", "tp"),
        P("ep", None, "tp"),
        P("ep", "tp"),
        P(),
        P(None, "tp"),
        P(None, "tp"),
        P(None, "tp"),
        P("tp"),
        P("tp", None, None),
        P("tp"),
        P("tp", None, None),
        P("tp"),
        P("tp"),
        P(None, "tp"),
        P(),
        P("ep", None),
        P("ep", None),
        P("ep"),
        P("ep", None, "tp"),
        P("ep", None, "tp"),
        P("ep", "tp", None),
    )
    out_specs = (P("ep", "tp"), P("ep", "tp"), P("ep", None, "tp"))
    return jax.shard_map(body, mesh=mesh, in_specs=in_specs, out_specs=out_specs, check_vma=False)
```

time: 140 us -> 140 us (level)
  blocking collectives: 60.7 us -> 21.2 us
  starting transfers between devices: 18.9 us -> 56.6 us
  Pallas kernels: 0 us -> 5.45 us
  waiting for transfers between devices: 42.7 us -> 39.6 us
  other arithmetic: 3.97 us -> 2.24 us
    all_to_all x2, blocking collectives: 60.7 us -> 21.2 us  [the longest x1 13.3 us: body(): products = lax.all_to_all(products, 'tp', 0, 0, tiled=True)]
    all_to_all x3, starting transfers between devices: 11.1 us -> 29.3 us  [the longest x1 21.9 us: body(): arrived = lax.all_to_all(outgoing, 'ep', 0, 0, tiled=True)]
    all_to_all x3, waiting for transfers between devices: 20.9 us -> 5.74 us  [the longest x1 2.97 us: body(): mixer_parts = lax.all_to_all(copies, 'tp', 0, 0, tiled=True)]
    ppermute x0 -> x3, waiting for transfers between devices: none -> 14.4 us  [body(): weights.append(lax.ppermute(sends[k - 1], 'tp', ring))]
    all_to_all x1, starting transfers between devices: 7.72 us -> 18.8 us  [body(): returned = lax.all_to_all(answer, 'ep', 0, 0, tiled=True)]
    ppermute x0 -> x3, starting transfers between devices: none -> 8.43 us  [body(): weights.append(lax.ppermute(sends[k - 1], 'tp', ring))]
    pallas_call x0 -> x6, Pallas kernels: none -> 5.45 us  [the longest x5 3.86 us: call(): pl.pallas_call(kernel, out_shape=outs, in_specs=[SMEM] * len(scalars) + [...]
    all_to_all x1, waiting for transfers between devices: 21.8 us -> 19.5 us  [body(): returned = lax.all_to_all(answer, 'ep', 0, 0, tiled=True)]
  transfers between devices with their start and end apart: 4 -> 7, of which waited for: 4 -> 6; matrix products, arithmetic and copies ran while one was open for 3% -> 4% of each run, Pallas kernels for 0% -> 3%
where the time goes in v3:
time: 140 us; the launch traced here: 139 us
  starting transfers between devices  56.6 us (40%)
  waiting for transfers between devices  39.6 us (28%)
  blocking collectives  21.2 us (15%)
  local copies, waits for them, and re-layouts  8.22 us (6%)
  Pallas kernels  5.45 us (4%)
  matrix products  4.82 us (3%)
  other arithmetic  2.24 us (2%)
    all_to_all x1, starting transfers between devices, body(): arrived = lax.all_to_all(outgoing, 'ep', 0, 0, tiled=True)  21.9 us
    all_to_all x1, waiting for transfers between devices, body(): returned = lax.all_to_all(answer, 'ep', 0, 0, tiled=True)  19.5 us
    all_to_all x1, starting transfers between devices, body(): returned = lax.all_to_all(answer, 'ep', 0, 0, tiled=True)  18.8 us
    ppermute x3, waiting for transfers between devices, body(): weights.append(lax.ppermute(sends[k - 1], 'tp', ring))  14.4 us
    all_to_all x1, blocking collectives, body(): products = lax.all_to_all(products, 'tp', 0, 0, tiled=True)  13.3 us
    ppermute x3, starting transfers between devices, body(): weights.append(lax.ppermute(sends[k - 1], 'tp', ring))  8.43 us
    all_to_all x1, blocking collectives, body(): hidden = lax.all_to_all(hidden, 'tp', 0, 0, tiled=True)  7.92 us
    dot_general x5, matrix products, dot(): return jnp.dot(a, b, preferred_element_type=F32)  4.28 us
  transfers between devices with their start and end apart: 7, of which 6 were waited for; matrix products, arithmetic and copies ran while one was open for 4% of the time, Pallas kernels for 3%

profile of v3, /device:TPU:33, one launch (start us, length us, event | category | flops | bytes accessed | tf_op | source)
XLA Modules:
  0.0 139.2 jit_solution(15253752687113821880)
XLA Ops:
  0.6 0.0 copy-start
  0.7 1.5 %broadcast_in_dim.12 = bf16[4,48,512]{2,1,0:T(8,128)(2,1)} broadcast(bf16[48,512]{1,0:T(8,128)(2,1)} %param.21), dimensions={1,2} | broadcast | bytes 245760 | tf_op jit(solution)/shard_map/broadcast_in_dim | solution.py:191
  2.2 4.2 %all-to-all-start = ((bf16[4,48,512]{2,1,0:T(8,128)(2,1)}), bf16[4,48,512]{2,1,0:T(8,128)(2,1)S(1)}, u32[]{:S(2)}, u32[]{:S(2)}) async-start(bf16[4,48,512]{2,1,0:T(8,128)(2,1)} %broadcast_in_dim.12), calls=%async_computation | async-start | bytes 393216 | tf_op jit(solution)/shard_map/all_to_all | solution.py:190
  6.4 0.7 mul.88
  7.1 1.6 %shard_map.220 = (bf16[384,512]{1,0:T(8,128)(2,1)S(1)}, bf16[384,512]{1,0:T(8,128)(2,1)S(1)}, bf16[384,512]{1,0:T(8,128)(2,1)S(1)}, bf16[384,512]{1,0:T(8,128)(2,1)S(1)}) custom-call(s32[1]{0:T(128)} %bitcast.5.member_ref, bf16[1,2048,128]{2,1,0:T(8,128)(2,1)} %gate_ref.1, bf16[1,2048,128]{2,1,0:T(8,128)(2,1)} %up_ref.1, bf16[1,128,2048]{2,1,0:T(8,128)(2,1)} %down_ref.1), custom_call_target="tpu_custom_call" | custom-call | tf_op jit(solution)/shard_map/pallas_call | solution.py:194
  8.7 0.0 copy-start.7
  8.8 2.8 %all-to-all-done = bf16[4,48,512]{2,1,0:T(8,128)(2,1)S(1)} async-done(((bf16[4,48,512]{2,1,0:T(8,128)(2,1)}), bf16[4,48,512]{2,1,0:T(8,128)(2,1)S(1)}, u32[]{:S(2)}, u32[]{:S(2)}) %all-to-all-start) | async-done | bytes 196640 | tf_op jit(solution)/shard_map/all_to_all | solution.py:190
  11.5 0.1 fusion.6
  11.7 0.1 fusion.9
  11.9 1.5 %fusion.5 = bf16[48,1,256]{2,0,1:T(8,128)(2,1)S(1)} fusion(bf16[48,2048]{1,0:T(8,128)(2,1)S(1)} %bitcast.83, bf16[2048,256]{1,0:T(8,128)(2,1)} %param.25), kind=kOutput, calls=%fused_computation.13 | convolution fusion | flops 50343936 | bytes 1269760 | tf_op jit(solution)/shard_map/dot_general | solution.py:33
  13.5 0.1 convolution_bitcast_fusion
  13.6 0.1 convolution_bitcast_fusion.1
  13.8 0.1 fusion.26
  13.9 0.0 copy-start.4
  13.9 0.3 fusion.19
  14.2 0.6 broadcast_in_dim.14
  14.8 3.3 %all-to-all-start.1 = ((bf16[4,48,256]{2,1,0:T(8,128)(2,1)}), bf16[4,48,256]{2,1,0:T(8,128)(2,1)S(1)}, u32[]{:S(2)}, u32[]{:S(2)}) async-start(bf16[4,48,256]{2,1,0:T(8,128)(2,1)} %broadcast_in_dim.14), calls=%async_computation.1 | async-start | bytes 196608 | tf_op jit(solution)/shard_map/all_to_all | solution.py:225
  18.2 0.7 copy.41.ids_ref
  18.9 0.9 shard_map.222
  19.8 3.0 %all-to-all-done.1 = bf16[4,48,256]{2,1,0:T(8,128)(2,1)S(1)} async-done(((bf16[4,48,256]{2,1,0:T(8,128)(2,1)}), bf16[4,48,256]{2,1,0:T(8,128)(2,1)S(1)}, u32[]{:S(2)}, u32[]{:S(2)}) %all-to-all-start.1) | async-done | bytes 98336 | tf_op jit(solution)/shard_map/all_to_all | solution.py:225
  22.8 1.5 %fusion.2 = bf16[48,512]{1,0:T(8,128)(2,1)S(1)} fusion(bf16[48,1024]{1,0:T(8,128)(2,1)S(1)} %bitcast.88, bf16[1024,512]{1,0:T(8,128)(2,1)} %param.34, bf16[48,512]{1,0:T(8,128)(2,1)S(1)} %copy-done.3), kind=kOutput, calls=%fused_computation.6 | convolution fusion | flops 50405376 | bytes 1245184 | tf_op jit(solution)/shard_map/dot_general | solution.py:33
  24.3 0.3 fusion
  24.6 0.8 reshape.52
  25.4 21.9 %all-to-all-start.2 = ((bf16[128,2,512]{2,1,0:T(2,128)(2,1)}), bf16[128,2,512]{2,1,0:T(2,128)(2,1)S(1)}, u32[]{:S(2)}, u32[]{:S(2)}) async-start(bf16[128,2,512]{2,1,0:T(2,128)(2,1)} %reshape.52), calls=%async_computation.2 | async-start | bytes 524288 | tf_op jit(solution)/shard_map/all_to_all | solution.py:233
  47.3 2.2 %collective-permute-start = (bf16[384,512]{1,0:T(8,128)(2,1)S(1)}, bf16[384,512]{1,0:T(8,128)(2,1)S(1)}, u32[]{:S(2)}, u32[]{:S(2)}) collective-permute-start(bf16[384,512]{1,0:T(8,128)(2,1)S(1)} %get-tuple-element.21), channel_id=1, source_target_pairs={{0,1},{1,2},{2,3},{3,0},{4,5},{5,6},{6,7},{7,4},{8,9},{9,10},{10,1... | collective-permute-start | bytes 1179656 | tf_op jit(solution)/shard_map/ppermute | solution.py:229
  49.5 3.7 %collective-permute-start.1 = (bf16[384,512]{1,0:T(8,128)(2,1)S(1)}, bf16[384,512]{1,0:T(8,128)(2,1)S(1)}, u32[]{:S(2)}, u32[]{:S(2)}) collective-permute-start(bf16[384,512]{1,0:T(8,128)(2,1)S(1)} %get-tuple-element.22), channel_id=1, source_target_pairs={{0,2},{1,3},{2,0},{3,1},{4,6},{5,7},{6,4},{7,5},{8,10},{9,11},{10,... | collective-permute-start | bytes 1179656 | tf_op jit(solution)/shard_map/ppermute | solution.py:229
  53.2 2.5 %collective-permute-start.2 = (bf16[384,512]{1,0:T(8,128)(2,1)S(1)}, bf16[384,512]{1,0:T(8,128)(2,1)}, u32[]{:S(2)}, u32[]{:S(2)}) collective-permute-start(bf16[384,512]{1,0:T(8,128)(2,1)S(1)} %get-tuple-element.23), channel_id=1, source_target_pairs={{0,3},{1,0},{2,1},{3,2},{4,7},{5,4},{6,5},{7,6},{8,11},{9,8},{10,9... | collective-permute-start | bytes 1179656 | tf_op jit(solution)/shard_map/ppermute | solution.py:229
  55.7 1.3 dynamic_slice.3
  57.1 4.2 %collective-permute-done = bf16[384,512]{1,0:T(8,128)(2,1)S(1)} collective-permute-done((bf16[384,512]{1,0:T(8,128)(2,1)S(1)}, bf16[384,512]{1,0:T(8,128)(2,1)S(1)}, u32[]{:S(2)}, u32[]{:S(2)}) %collective-permute-start) | collective-permute-done | bytes 393248 | tf_op jit(solution)/shard_map/ppermute | solution.py:229
  61.3 7.3 %collective-permute-done.1 = bf16[384,512]{1,0:T(8,128)(2,1)S(1)} collective-permute-done((bf16[384,512]{1,0:T(8,128)(2,1)S(1)}, bf16[384,512]{1,0:T(8,128)(2,1)S(1)}, u32[]{:S(2)}, u32[]{:S(2)}) %collective-permute-start.1) | collective-permute-done | bytes 393248 | tf_op jit(solution)/shard_map/ppermute | solution.py:229
  68.5 2.9 %collective-permute-done.2 = bf16[384,512]{1,0:T(8,128)(2,1)} collective-permute-done((bf16[384,512]{1,0:T(8,128)(2,1)S(1)}, bf16[384,512]{1,0:T(8,128)(2,1)}, u32[]{:S(2)}, u32[]{:S(2)}) %collective-permute-start.2) | collective-permute-done | bytes 393248 | tf_op jit(solution)/shard_map/ppermute | solution.py:229
  71.5 1.2 pad_maximum_fusion.weight_ref
  72.7 0.1 reshape.53.rows_ref
  72.8 1.3 shard_map.223
  74.1 13.3 %all_to_all.37.parts_ref = bf16[4,272,256]{2,1,0:T(8,128)(2,1)S(1)} all-to-all(bf16[4,272,256]{2,1,0:T(8,128)(2,1)S(1)} %get-tuple-element.24), channel_id=1, replica_groups=mesh['ep'=128,'tp'=4] {'tp'}, dimensions={0} | all-to-all | bytes 1114112 | tf_op jit(solution)/shard_map/all_to_all | solution.py:246
  87.4 0.2 shard_map.224
  87.6 7.9 %all_to_all.38.hidden_ref = bf16[4,256,128]{2,1,0:T(8,128)(2,1)S(1)} all-to-all(bf16[4,256,128]{2,1,0:T(8,128)(2,1)S(1)} %shard_map.224), channel_id=1, replica_groups=mesh['ep'=128,'tp'=4] {'tp'}, dimensions={0} | all-to-all | bytes 524288 | tf_op jit(solution)/shard_map/all_to_all | solution.py:248
  95.5 0.4 shard_map.225
  95.9 0.8 all_to_all.28
  96.7 18.8 %all-to-all-start.5 = ((bf16[128,2,512]{2,1,0:T(2,128)(2,1)}), bf16[128,2,512]{2,1,0:T(2,128)(2,1)S(1)}, u32[]{:S(2)}, u32[]{:S(2)}) async-start(bf16[128,2,512]{2,1,0:T(2,128)(2,1)} %all_to_all.28), calls=%async_computation.5 | async-start | bytes 524288 | tf_op jit(solution)/shard_map/all_to_all | solution.py:252
  115.5 0.7 copy.42.logits_ref
  116.2 0.7 copy.43.group_ref
  116.9 1.0 shard_map.221
  118.0 0.6 fusion.10
  118.6 19.5 %all-to-all-done.5 = bf16[128,2,512]{2,1,0:T(2,128)(2,1)S(1)} async-done(((bf16[128,2,512]{2,1,0:T(2,128)(2,1)}), bf16[128,2,512]{2,1,0:T(2,128)(2,1)S(1)}, u32[]{:S(2)}, u32[]{:S(2)}) %all-to-all-start.5) | async-done | bytes 262176 | tf_op jit(solution)/shard_map/all_to_all | solution.py:252
  138.1 0.1 all_to_all.30
  138.2 0.1 fusion.36
  138.4 0.8 fusion.3
  (33 shorter events, 0.1 us)
Async XLA Ops:
  0.6 12.8 %copy-start = (bf16[2,128,128]{2,1,0:T(8,128)(2,1)S(1)}, bf16[2,128,128]{2,1,0:T(8,128)(2,1)}, u32[]{:S(2)}) copy-start(bf16[2,128,128]{2,1,0:T(8,128)(2,1)} %param.31) | copy-start | bytes 196612
  0.6 8.0 %copy-start.13 = (f32[256]{0:T(256)S(1)}, f32[256]{0:T(256)}, u32[]{:S(2)}) copy-start(f32[256]{0:T(256)} %param.33) | copy-start | bytes 3076
  2.2 9.4 %all-to-all-start = ((bf16[4,48,512]{2,1,0:T(8,128)(2,1)}), bf16[4,48,512]{2,1,0:T(8,128)(2,1)S(1)}, u32[]{:S(2)}, u32[]{:S(2)}) async-start(bf16[4,48,512]{2,1,0:T(8,128)(2,1)} %broadcast_in_dim.12), calls=%async_computation | async-start | bytes 393216 | tf_op jit(solution)/shard_map/all_to_all | solution.py:190
  7.1 6.3 %copy-start.2 = (bf16[48,3,256]{2,0,1:T(8,128)(2,1)S(1)}, bf16[48,3,256]{2,0,1:T(8,128)(2,1)}, u32[]{:S(2)}) copy-start(bf16[48,3,256]{2,0,1:T(8,128)(2,1)} %param.22) | copy-start | bytes 221188
  7.1 6.3 %copy-start.8 = (f32[4,256]{1,0:T(4,128)S(1)}, f32[4,256]{1,0:T(4,128)}, u32[]{:S(2)}) copy-start(f32[4,256]{1,0:T(4,128)} %param.27) | copy-start | bytes 12292
  8.7 4.8 %copy-start.7 = (f32[256]{0:T(256)S(1)}, f32[256]{0:T(256)}, u32[]{:S(2)}) copy-start(f32[256]{0:T(256)} %param.28) | copy-start | bytes 3076
  8.7 4.9 %copy-start.5 = (bf16[2,128,128]{2,1,0:T(8,128)(2,1)S(1)}, bf16[2,128,128]{2,1,0:T(8,128)(2,1)}, u32[]{:S(2)}) copy-start(bf16[2,128,128]{2,1,0:T(8,128)(2,1)} %param.29) | copy-start | bytes 196612
  8.7 5.0 %copy-start.6 = (f32[48,256]{1,0:T(8,128)S(1)}, f32[48,256]{1,0:T(8,128)}, u32[]{:S(2)}) copy-start(f32[48,256]{1,0:T(8,128)} %param.23) | copy-start | bytes 147460
  8.7 5.0 %copy-start.9 = (f32[256]{0:T(256)S(1)}, f32[256]{0:T(256)}, u32[]{:S(2)}) copy-start(f32[256]{0:T(256)} %param.32) | copy-start | bytes 3076
  8.7 5.0 %copy-start.10 = (f32[256]{0:T(256)S(1)}, f32[256]{0:T(256)}, u32[]{:S(2)}) copy-start(f32[256]{0:T(256)} %param.30) | copy-start | bytes 3076
  8.7 5.1 %copy-start.1 = (bf16[2048,256]{1,0:T(8,128)(2,1)S(1)}, bf16[2048,256]{1,0:T(8,128)(2,1)}, u32[]{:S(2)}) copy-start(bf16[2048,256]{1,0:T(8,128)(2,1)} %param.26) | copy-start | bytes 3145732
  11.8 6.3 %copy-start.11 = (s32[48,2]{0,1:T(2,128)S(1)}, s32[48,2]{0,1:T(2,128)}, u32[]{:S(2)}) copy-start(s32[48,2]{0,1:T(2,128)} %param.36) | copy-start | bytes 1156
  13.4 9.4 %copy-start.3 = (bf16[48,512]{1,0:T(8,128)(2,1)S(1)}, bf16[48,512]{1,0:T(8,128)(2,1)}, u32[]{:S(2)}) copy-start(bf16[48,512]{1,0:T(8,128)(2,1)} %param.21) | copy-start | bytes 147460
  13.9 10.4 %copy-start.4 = (f32[48,256]{1,0:T(8,128)}, f32[48,256]{1,0:T(8,128)S(1)}, u32[]{:S(2)}) copy-start(f32[48,256]{1,0:T(8,128)S(1)} %fusion.26) | copy-start | bytes 147460
  14.8 7.9 %all-to-all-start.1 = ((bf16[4,48,256]{2,1,0:T(8,128)(2,1)}), bf16[4,48,256]{2,1,0:T(8,128)(2,1)S(1)}, u32[]{:S(2)}, u32[]{:S(2)}) async-start(bf16[4,48,256]{2,1,0:T(8,128)(2,1)} %broadcast_in_dim.14), calls=%async_computation.1 | async-start | bytes 196608 | tf_op jit(solution)/shard_map/all_to_all | solution.py:225
  25.4 47.2 %all-to-all-start.2 = ((bf16[128,2,512]{2,1,0:T(2,128)(2,1)}), bf16[128,2,512]{2,1,0:T(2,128)(2,1)S(1)}, u32[]{:S(2)}, u32[]{:S(2)}) async-start(bf16[128,2,512]{2,1,0:T(2,128)(2,1)} %reshape.52), calls=%async_computation.2 | async-start | bytes 524288 | tf_op jit(solution)/shard_map/all_to_all | solution.py:233
  47.3 14.0 %collective-permute-start = (bf16[384,512]{1,0:T(8,128)(2,1)S(1)}, bf16[384,512]{1,0:T(8,128)(2,1)S(1)}, u32[]{:S(2)}, u32[]{:S(2)}) collective-permute-start(bf16[384,512]{1,0:T(8,128)(2,1)S(1)} %get-tuple-element.21), channel_id=1, source_target_pairs={{0,1},{1,2},{2,3},{3,0},{4,5},{5,6},{6,7},{7,4},{8,9},{9,10},{10,1... | collective-permute-start | bytes 1179656 | tf_op jit(solution)/shard_map/ppermute | solution.py:229
  49.5 19.0 %collective-permute-start.1 = (bf16[384,512]{1,0:T(8,128)(2,1)S(1)}, bf16[384,512]{1,0:T(8,128)(2,1)S(1)}, u32[]{:S(2)}, u32[]{:S(2)}) collective-permute-start(bf16[384,512]{1,0:T(8,128)(2,1)S(1)} %get-tuple-element.22), channel_id=1, source_target_pairs={{0,2},{1,3},{2,0},{3,1},{4,6},{5,7},{6,4},{7,5},{8,10},{9,11},{10,... | collective-permute-start | bytes 1179656 | tf_op jit(solution)/shard_map/ppermute | solution.py:229
  53.2 18.3 %collective-permute-start.2 = (bf16[384,512]{1,0:T(8,128)(2,1)S(1)}, bf16[384,512]{1,0:T(8,128)(2,1)}, u32[]{:S(2)}, u32[]{:S(2)}) collective-permute-start(bf16[384,512]{1,0:T(8,128)(2,1)S(1)} %get-tuple-element.23), channel_id=1, source_target_pairs={{0,3},{1,0},{2,1},{3,2},{4,7},{5,4},{6,5},{7,6},{8,11},{9,8},{10,9... | collective-permute-start | bytes 1179656 | tf_op jit(solution)/shard_map/ppermute | solution.py:229
  87.4 28.2 %copy-start.12 = (f32[48,2]{0,1:T(2,128)S(1)}, f32[48,2]{0,1:T(2,128)}, u32[]{:S(2)}) copy-start(f32[48,2]{0,1:T(2,128)} %param.37) | copy-start | bytes 1156
  87.4 28.9 %copy-start.14 = (f32[48]{0:T(128)S(1)}, f32[48]{0:T(128)}, u32[]{:S(2)}) copy-start(f32[48]{0:T(128)} %param.38) | copy-start | bytes 580
  96.7 41.4 %all-to-all-start.5 = ((bf16[128,2,512]{2,1,0:T(2,128)(2,1)}), bf16[128,2,512]{2,1,0:T(2,128)(2,1)S(1)}, u32[]{:S(2)}, u32[]{:S(2)}) async-start(bf16[128,2,512]{2,1,0:T(2,128)(2,1)} %all_to_all.28), calls=%async_computation.5 | async-start | bytes 524288 | tf_op jit(solution)/shard_map/all_to_all | solution.py:252

commit v4 on v3

--- a/solution.py
+++ b/solution.py
@@ -1,3 +1,5 @@
+import functools
+
 import jax
 import jax.numpy as jnp
 from jax import lax
@@ -57,62 +59,152 @@
     return jnp.where(earlier == place.astype(F32), named, 0.0), first
 
 
-def dispatch_table(ids_ref, out_ref):
-    out_ref[...] = places(ids_ref, *out_ref.shape)[0].astype(BF16)
-
-
-def combine_tables(ids_ref, logits_ref, group_ref, high_ref, low_ref):
+def combine_tables(ids_ref, logits_ref, group_ref, piece_ref, high_ref, low_ref, near_ref, done):
+    copy = pltpu.make_async_copy(piece_ref, near_ref, done)
+    copy.start()
     hit, first = places(ids_ref, *high_ref.shape)
     raised = jnp.exp(logits_ref[...])
     weight = group_ref[...] * raised / (raised[:, 0:1] + raised[:, 1:2])
     high, low = halves(hit * jnp.where(first, weight[:, 0:1], weight[:, 1:2]))
     high_ref[...] = high
     low_ref[...] = low
-
-
-def cut_weights(member_ref, gate_ref, up_ref, down_ref, *refs):
-    *out_refs, done = refs
-    members = len(out_refs)
+    copy.wait()
+
+
+def cut_weights(member_ref, gate_ref, up_ref, down_ref, *refs, members):
+    *rest, piece_ref, reads, writes, loads = refs
+    count = (len(rest) - members) // 2
+    far_refs, out_refs, near_refs = rest[:count], rest[count : count + members], rest[count + members :]
     quarter = gate_ref.shape[1] // members
     half = quarter // 2
     width = gate_ref.shape[2]
-    copies = []
-    for k, out_ref in enumerate(out_refs):
+    order = (2, 1, 3, 0)
+    copies = {}
+    for k in order:
         target = lax.rem(member_ref[0] + k, members)
         top = pl.multiple_of(target * quarter, quarter)
-        pairs = [(down_ref.at[0, :, pl.ds(top, quarter)], out_ref.at[pl.ds(half, width), :])]
+        piece = piece_ref.at[k]
+        pairs = [(down_ref.at[0, :, pl.ds(top, quarter)], piece.at[pl.ds(half, width), :])]
         for part in range(2):
             rows = pl.ds(pl.multiple_of(top + part * half, half), half)
             at = part * 2 * width
-            into = [out_ref.at[pl.ds(0, half), pl.ds(at + j * width, width)] for j in range(2)]
+            into = [piece.at[pl.ds(0, half), pl.ds(at + j * width, width)] for j in range(2)]
             pairs += [(gate_ref.at[0, rows, :], into[0]), (up_ref.at[0, rows, :], into[1])]
-        copies += [
-            pltpu.make_async_copy(source, into, done.at[k, j])
+        copies[k] = [
+            pltpu.make_async_copy(source, into, reads.at[k, j])
             for j, (source, into) in enumerate(pairs)
         ]
-    for copy in copies:
+        for copy in copies[k]:
+            copy.start()
+    near_copies = [
+        pltpu.make_async_copy(source, into, loads.at[j])
+        for j, (source, into) in enumerate(zip(far_refs, near_refs))
+    ]
+    for copy in near_copies:
         copy.start()
-    for copy in copies:
+    out_copies = []
+    for k in order:
+        for copy in copies[k]:
+            copy.wait()
+        out_copies.append(pltpu.make_async_copy(piece_ref.at[k], out_refs[k], writes.at[k]))
+        out_copies[-1].start()
+    for copy in near_copies + out_copies:
         copy.wait()
 
 
-def block_gate(signal, weight, bias):
-    blocks = weight.shape[0]
-    grouped = signal.reshape(signal.shape[0], blocks, -1)
-    mixed_out = jnp.einsum("sbi,bij->sbj", grouped, weight, preferred_element_type=F32)
-    return jax.nn.sigmoid(mixed_out.reshape(signal.shape[0], -1) + bias)
-
-
-def side_by_side(parts):
-    size, rows, width = parts.shape
-    return jnp.swapaxes(parts, 0, 1).reshape(rows, size * width)
-
-
-def first_products(member_ref, rows_ref, gain_ref, weight_ref, out_ref, down_ref):
-    members = weight_ref.shape[0]
+def mixer(
+    parts_ref,
+    gain_ref,
+    input_ref,
+    branch_ref,
+    conv_ref,
+    taps_ref,
+    bias_ref,
+    recur_ref,
+    recur_bias_ref,
+    inject_ref,
+    inject_bias_ref,
+    decay_ref,
+    lru_ref,
+    copies_ref,
+    state_ref,
+    window_ref,
+):
+    members, count, quarter = parts_ref.shape
+    taps = taps_ref.shape[0]
+    squares = jnp.zeros((count, 1), F32)
+    for m in range(members):
+        wide = parts_ref[m].astype(F32)
+        squares = squares + jnp.sum(wide * wide, axis=1, keepdims=True)
+    scale = lax.rsqrt(squares / (members * quarter) + EPS)
+    normed = jnp.concatenate(
+        [
+            (
+                parts_ref[m].astype(F32) * scale * gain_ref[:, m * quarter : (m + 1) * quarter]
+            ).astype(BF16)
+            for m in range(members)
+        ],
+        axis=1,
+    )
+    branch_x = dot(normed, input_ref[...]).astype(BF16)
+    branch_g = dot(normed, branch_ref[...]).astype(BF16)
+    rows = [conv_ref[j] for j in range(taps - 1)] + [branch_x]
+    conv_sum = rows[0].astype(F32) * taps_ref[0:1]
+    for j in range(1, taps):
+        conv_sum = conv_sum + rows[j].astype(F32) * taps_ref[j : j + 1]
+        window_ref[j - 1] = rows[j]
+    conv_out = (bias_ref[...] + conv_sum).astype(BF16)
+    blocks, size, _ = recur_ref.shape
+
+    def gate(weight_ref, gate_bias_ref):
+        product = [
+            dot(conv_out[:, b * size : (b + 1) * size], weight_ref[b]) for b in range(blocks)
+        ]
+        return jax.nn.sigmoid(jnp.concatenate(product, axis=1) + gate_bias_ref[...])
+
+    rate = -RATE * jax.nn.softplus(-decay_ref[...])
+    log_rate = gate(recur_ref, recur_bias_ref) * rate
+    inject = gate(inject_ref, inject_bias_ref)
+    kept = jnp.exp(log_rate)
+    rest = -jnp.tanh(log_rate) * (1.0 + kept * kept)
+    state = kept * lru_ref[...] + jnp.sqrt(rest) * inject * conv_out.astype(F32)
+    state_ref[...] = state
+    out = (state * jax.nn.gelu(branch_g.astype(F32))).astype(BF16)
+    for m in range(members):
+        copies_ref[m] = out
+
+
+def stream_rows(parts_ref, tokens_ref, ids_ref, weight_ref, stream_ref, out_ref, near_ref, done):
+    copy = pltpu.make_async_copy(weight_ref, near_ref, done)
+    copy.start()
+    slots, count = out_ref.shape[0], tokens_ref.shape[0]
+    row = lax.broadcasted_iota(jnp.int32, (slots, count), 0)
+    expert = lax.div(row, CAPACITY)
+    place = lax.rem(row, CAPACITY)
+    ids = ids_ref[...]
+    named = jnp.where((ids[0:1] == expert) | (ids[1:2] == expert), 1.0, 0.0)
+    before = lax.broadcasted_iota(jnp.int32, (count, count), 0) < lax.broadcasted_iota(
+        jnp.int32, (count, count), 1
+    )
+    earlier = dot(named.astype(BF16), jnp.where(before, 1.0, 0.0).astype(BF16))
+    dispatch = jnp.where(earlier == place.astype(F32), named, 0.0).astype(BF16)
+    copy.wait()
+    members, _, width = parts_ref.shape
+    mixed = dot(parts_ref[0], near_ref[:width, :])
+    for m in range(1, members):
+        mixed = mixed + dot(parts_ref[m], near_ref[m * width : (m + 1) * width, :])
+    stream = (tokens_ref[...].astype(F32) + mixed).astype(BF16)
+    stream_ref[...] = stream
+    out_ref[...] = dot(dispatch, stream).astype(BF16)
+
+
+def first_products(member_ref, rows_ref, gain_ref, *refs):
+    *weight_refs, out_ref, down_ref = refs
+    members = len(weight_refs)
+    count, width = rows_ref.shape
+    half = width // 2
+    owners = [lax.rem(member_ref[0] + (members - k), members) for k in range(members)]
     rows = rows_ref[...].astype(F32)
-    count, width = rows.shape
-    half = width // 2
     scaled = (rows * gain_ref[...]).astype(BF16)
     squares = rows * rows
     high, low = halves(squares)
@@ -123,13 +215,13 @@
         place == 0, sums_high.astype(F32), jnp.where(place == 1, sums_low.astype(F32), 0.0)
     ).astype(BF16)
     for k in range(members):
-        product = dot(scaled[:, :half], weight_ref[k, :half, :half]) + dot(
-            scaled[:, half:], weight_ref[k, :half, half:]
+        out_ref[k, count:, :] = sums
+    for k, cut in enumerate(weight_refs):
+        down_ref[owners[k]] = cut[half:, :]
+        product = dot(scaled[:, :half], cut[:half, :half]) + dot(
+            scaled[:, half:], cut[:half, half:]
         )
-        owner = lax.rem(member_ref[0] + (members - k), members)
-        out_ref[owner, :count, :] = product.astype(BF16)
-        out_ref[owner, count:, :] = sums
-        down_ref[owner] = weight_ref[k, half:, :]
+        out_ref[owners[k], :count, :] = product.astype(BF16)
 
 
 def hidden_units(parts_ref, out_ref):
@@ -180,6 +272,7 @@
     expert_down,
 ):
     seq_count, quarter = tokens.shape
+    channels = lru_state.shape[1]
     members = lax.axis_size("tp")
     experts = lax.axis_size("ep")
     member = lax.axis_index("tp")
@@ -191,45 +284,70 @@
         jnp.broadcast_to(tokens[None], (members, *tokens.shape)), "tp", 0, 0, tiled=True
     )
     anywhere = pl.BlockSpec(memory_space=pl.ANY)
-    pieces = pl.pallas_call(
-        cut_weights,
-        out_shape=[pltpu.VMEM((quarter // 2 + units, quarter), BF16)] * members,
-        in_specs=[SMEM] + [anywhere] * 3,
-        out_specs=[VMEM] * members,
-        scratch_shapes=[pltpu.SemaphoreType.DMA((members, 5))],
-    )(place, expert_gate, expert_up, expert_down)
+    piece = (quarter // 2 + units, quarter)
+    operands = [
+        mix_gain[None],
+        input_weight,
+        branch_weight,
+        jnp.swapaxes(conv_state, 0, 1),
+        conv_taps,
+        conv_bias[None],
+        recur_weight,
+        recur_bias[None],
+        inject_weight,
+        inject_bias[None],
+        decay_param[None],
+        lru_state,
+    ]
+    cutting = pl.pallas_call(
+        functools.partial(cut_weights, members=members),
+        out_shape=[jax.ShapeDtypeStruct(piece, BF16)] * members
+        + [pltpu.VMEM(value.shape, value.dtype) for value in operands],
+        in_specs=[SMEM] + [anywhere] * (3 + len(operands)),
+        out_specs=[anywhere] * members + [VMEM] * len(operands),
+        scratch_shapes=[
+            pltpu.VMEM((members, *piece), BF16),
+            pltpu.SemaphoreType.DMA((members, 5)),
+            pltpu.SemaphoreType.DMA((members,)),
+            pltpu.SemaphoreType.DMA((len(operands),)),
+        ],
+    )
+    loaded = cutting(place, expert_gate, expert_up, expert_down, *operands)
+    pieces, operands = loaded[:members], loaded[members:]
     table = pltpu.VMEM((seq_count, slots), BF16)
-    dispatch = call(dispatch_table, table, route_ids)
-    combine_high, combine_low = call(
-        combine_tables, [table] * 2, route_ids, route_logits, group_weight[:, None]
-    )
-    wide = token_parts.astype(F32)
-    scale = lax.rsqrt(jnp.sum(wide * wide, axis=(0, 2)) / (members * quarter) + EPS)
-    normed = (wide * scale[None, :, None] * mix_gain.reshape(members, 1, quarter)).astype(BF16)
-    normed = side_by_side(normed)
-    branch_x = dot(normed, input_weight).astype(BF16)
-    branch_g = dot(normed, branch_weight).astype(BF16)
-    window = jnp.concatenate([conv_state, branch_x[:, None, :]], axis=1)
-    conv_sum = conv_bias + jnp.sum(window.astype(F32) * conv_taps[None], axis=1)
-    conv_out = conv_sum.astype(BF16)
-    recur_gate = block_gate(conv_out, recur_weight, recur_bias)
-    inject_gate = block_gate(conv_out, inject_weight, inject_bias)
-    log_rate = -RATE * recur_gate * jax.nn.softplus(-decay_param)
-    new_state = jnp.exp(log_rate) * lru_state + jnp.sqrt(
-        -jnp.expm1(2.0 * log_rate)
-    ) * inject_gate * conv_out.astype(F32)
-    mixer_out = (new_state * jax.nn.gelu(branch_g.astype(F32))).astype(BF16)
-    copies = jnp.broadcast_to(mixer_out[None], (members, *mixer_out.shape))
-    gain_part = lax.dynamic_slice_in_dim(moe_gain, member * quarter, quarter, 0)[None]
-    copies, *sends = lax.optimization_barrier((copies, *pieces[1:]))
+    combine_high, combine_low, own_piece = pl.pallas_call(
+        combine_tables,
+        out_shape=[table, table, pltpu.VMEM(piece, BF16)],
+        in_specs=[VMEM] * 3 + [anywhere],
+        out_specs=[VMEM] * 3,
+        scratch_shapes=[pltpu.SemaphoreType.DMA],
+    )(route_ids, route_logits, group_weight[:, None], pieces[0])
+    copies, new_state, window = call(
+        mixer,
+        [
+            pltpu.VMEM((members, seq_count, channels), BF16),
+            jax.ShapeDtypeStruct((seq_count, channels), F32),
+            jax.ShapeDtypeStruct((conv_state.shape[1], seq_count, channels), BF16),
+        ],
+        near(token_parts),
+        *[near(value) for value in operands],
+    )
+    first_feature = member * quarter
+    gain_part = lax.dynamic_slice_in_dim(moe_gain, first_feature, quarter, 0)[None]
     mixer_parts = lax.all_to_all(copies, "tp", 0, 0, tiled=True)
-    weights = [pieces[0]]
+    weights = []
     for k in range(1, members):
         ring = [(m, (m + k) % members) for m in range(members)]
-        weights.append(lax.ppermute(sends[k - 1], "tp", ring))
-    stream = (tokens.astype(F32) + dot(side_by_side(mixer_parts), output_weight)).astype(BF16)
-
-    outgoing = dot_on(dispatch, stream, 0, 0).astype(BF16).reshape(experts, CAPACITY, quarter)
+        weights.append(lax.ppermute(pieces[k], "tp", ring))
+    stream, outgoing = pl.pallas_call(
+        stream_rows,
+        out_shape=[pltpu.VMEM((seq_count, quarter), BF16), pltpu.VMEM((slots, quarter), BF16)],
+        in_specs=[VMEM] * 3 + [anywhere],
+        out_specs=[VMEM] * 2,
+        scratch_shapes=[pltpu.VMEM(output_weight.shape, BF16), pltpu.SemaphoreType.DMA],
+    )(near(mixer_parts), tokens, route_ids.T, output_weight)
+
+    outgoing = outgoing.reshape(experts, CAPACITY, quarter)
     arrived = lax.all_to_all(outgoing, "ep", 0, 0, tiled=True)
     arrived = arrived.reshape(slots, quarter)
     products, down = call(
@@ -240,7 +358,8 @@
         ],
         near(arrived),
         gain_part,
-        near(jnp.stack(weights)),
+        near(own_piece),
+        *[near(w) for w in weights],
         scalar=place,
     )
     products = lax.all_to_all(products, "tp", 0, 0, tiled=True)
@@ -252,7 +371,7 @@
     returned = lax.all_to_all(answer, "ep", 0, 0, tiled=True)
     routed = dot(combine_high, returned) + dot(combine_low, returned)
     result = (stream.astype(F32) + routed).astype(BF16)
-    return (result, new_state, window[:, 1:])
+    return (result, new_state, jnp.swapaxes(window, 0, 1))
 
 
 def solution(mesh):

time: 140 us -> 136 us (0.971)
  blocking collectives: 21.2 us -> 69.4 us
  waiting for transfers between devices: 39.6 us -> 11.3 us
  starting transfers between devices: 56.6 us -> 34.6 us
  Pallas kernels: 5.45 us -> 11 us
  matrix products: 4.82 us -> 0.94 us
  other arithmetic: 2.24 us -> 0 us
  local copies, waits for them, and re-layouts: 8.22 us -> 6.75 us
    all_to_all x0 -> x2, blocking collectives: none -> 48.2 us  [the longest x1 41.2 us: body(): returned = lax.all_to_all(answer, 'ep', 0, 0, tiled=True)]
    all_to_all x2 -> x0, waiting for transfers between devices: 22.5 us -> none  [the longest x1 19.5 us: body(): returned = lax.all_to_all(answer, 'ep', 0, 0, tiled=True)]
    all_to_all x2 -> x0, starting transfers between devices: 22.1 us -> none  [the longest x1 18.8 us: body(): returned = lax.all_to_all(answer, 'ep', 0, 0, tiled=True)]
    ppermute x3, waiting for transfers between devices: 14.4 us -> 1.39 us  [body(): weights.append(lax.ppermute(pieces[k], 'tp', ring))]
    all_to_all x1, waiting for transfers between devices: 0.01 us -> 8.16 us  [body(): arrived = lax.all_to_all(outgoing, 'ep', 0, 0, tiled=True)]
    pallas_call x1 -> x3, Pallas kernels: 1.6 us -> 7.75 us  [the longest x1 3.45 us: body(): loaded = cutting(place, expert_gate, expert_up, expert_down, *operands)]
    dot_general x5 -> x2, matrix products: 4.28 us -> 0.94 us  [dot(): return jnp.dot(a, b, preferred_element_type=F32)]
    pallas_call x5 -> x4, Pallas kernels: 3.86 us -> 3.25 us  [call(): pl.pallas_call(kernel, out_shape=outs, in_specs=[SMEM] * len(scalars) + [...]
  transfers between devices with their start and end apart: 7 -> 5, of which waited for: 6 -> 3; matrix products, arithmetic and copies ran while one was open for 4% -> 3% of each run, Pallas kernels for 3% -> 4%
where the time goes in v4:
time: 136 us; the launch traced here: 135 us
  blocking collectives  69.4 us (51%)
  starting transfers between devices  34.6 us (25%)
  waiting for transfers between devices  11.3 us (8%)
  Pallas kernels  11 us (8%)
  local copies, waits for them, and re-layouts  6.75 us (5%)
    all_to_all x1, blocking collectives, body(): returned = lax.all_to_all(answer, 'ep', 0, 0, tiled=True)  41.2 us
    all_to_all x1, starting transfers between devices, body(): arrived = lax.all_to_all(outgoing, 'ep', 0, 0, tiled=True)  22 us
    all_to_all x1, blocking collectives, body(): products = lax.all_to_all(products, 'tp', 0, 0, tiled=True)  13.3 us
    ppermute x3, starting transfers between devices, body(): weights.append(lax.ppermute(pieces[k], 'tp', ring))  8.43 us
    all_to_all x1, waiting for transfers between devices, body(): arrived = lax.all_to_all(outgoing, 'ep', 0, 0, tiled=True)  8.16 us
    all_to_all x1, blocking collectives, body(): hidden = lax.all_to_all(hidden, 'tp', 0, 0, tiled=True)  7.92 us
    all_to_all x1, blocking collectives, body(): mixer_parts = lax.all_to_all(copies, 'tp', 0, 0, tiled=True)  7.01 us
    all_to_all x1, starting transfers between devices, body(): lax.all_to_all(jnp.broadcast_to(tokens[None], (members, *tokens.shape)),...  4.18 us
  transfers between devices with their start and end apart: 5, of which 3 were waited for; matrix products, arithmetic and copies ran while one was open for 3% of the time, Pallas kernels for 4%

profile of v4, /device:TPU:33, one launch (start us, length us, event | category | flops | bytes accessed | tf_op | source)
XLA Modules:
  0.0 134.8 jit_solution(13130162380419738518)
XLA Ops:
  0.6 1.5 %broadcast_in_dim.30 = bf16[4,48,512]{2,1,0:T(8,128)(2,1)} broadcast(bf16[48,512]{1,0:T(8,128)(2,1)} %tokens_ref.1), dimensions={1,2} | broadcast | bytes 245760 | tf_op jit(solution)/shard_map/broadcast_in_dim | solution.py:284
  2.1 4.2 %all-to-all-start = ((bf16[4,48,512]{2,1,0:T(8,128)(2,1)}), bf16[4,48,512]{2,1,0:T(8,128)(2,1)S(1)}, u32[]{:S(2)}, u32[]{:S(2)}) async-start(bf16[4,48,512]{2,1,0:T(8,128)(2,1)} %broadcast_in_dim.30), calls=%async_computation | async-start | bytes 393216 | tf_op jit(solution)/shard_map/all_to_all | solution.py:283
  6.3 3.5 %shard_map.220 = (bf16[384,512]{1,0:T(8,128)(2,1)}, bf16[384,512]{1,0:T(8,128)(2,1)}, bf16[384,512]{1,0:T(8,128)(2,1)}, bf16[384,512]{1,0:T(8,128)(2,1)}, f32[1,...) custom-call(s32[1]{0:T(128)} %bitcast.member_ref, ...), custom_call_target="tpu_custom_call" | custom-call | tf_op jit(solution)/shard_map/pallas_call | solution.py:315
  9.8 1.7 %all-to-all-done.parts_ref = bf16[4,48,512]{2,1,0:T(8,128)(2,1)S(1)} async-done(((bf16[4,48,512]{2,1,0:T(8,128)(2,1)}), bf16[4,48,512]{2,1,0:T(8,128)(2,1)S(1)}, u32[]{:S(2)}, u32[]{:S(2)}) %all-to-all-start) | async-done | bytes 196640 | tf_op jit(solution)/shard_map/all_to_all | solution.py:283
  11.5 1.3 shard_map.221
  12.8 7.0 %all_to_all.37.parts_ref = bf16[4,48,256]{2,1,0:T(8,128)(2,1)S(1)} all-to-all(bf16[4,48,256]{2,1,0:T(8,128)(2,1)S(1)} %get-tuple-element.41), channel_id=1, replica_groups=mesh['ep'=128,'tp'=4] {'tp'}, dimensions={0} | all-to-all | bytes 196608 | tf_op jit(solution)/shard_map/all_to_all | solution.py:337
  19.9 2.5 %shard_map.222 = (bf16[48,512]{1,0:T(8,128)(2,1)S(1)}, bf16[256,512]{1,0:T(8,128)(2,1)S(1)}) custom-call(bf16[4,48,256]{2,1,0:T(8,128)(2,1)S(1)} %all_to_all.37.parts_ref, bf16[48,512]{1,0:T(8,128)(2,1)} %tokens_ref.1, s32[2,48]{1,0:T(2,128)} %bitcast.18, bf16[1024,512]{1,0:T(8,128)(2,1)} %weight_ref.1), custom_call_target="tpu_custom_call" | custom-call | tf_op jit(solution)/shard_map/pallas_call | solution.py:342
  22.4 0.0 copy-start.4
  22.4 0.8 reshape.15
  23.2 0.0 copy-start.3
  23.2 22.0 %all-to-all-start.2 = ((bf16[128,2,512]{2,1,0:T(2,128)(2,1)}), bf16[128,2,512]{2,1,0:T(2,128)(2,1)S(1)}, u32[]{:S(2)}, u32[]{:S(2)}) async-start(bf16[128,2,512]{2,1,0:T(2,128)(2,1)} %reshape.15), calls=%async_computation.2 | async-start | bytes 524288 | tf_op jit(solution)/shard_map/all_to_all | solution.py:351
  45.2 2.2 %collective-permute-start = (bf16[384,512]{1,0:T(8,128)(2,1)}, bf16[384,512]{1,0:T(8,128)(2,1)S(1)}, u32[]{:S(2)}, u32[]{:S(2)}) collective-permute-start(bf16[384,512]{1,0:T(8,128)(2,1)} %get-tuple-element.47), channel_id=1, source_target_pairs={{0,1},{1,2},{2,3},{3,0},{4,5},{5,6},{6,7},{7,4},{8,9},{9,10},{10,1... | collective-permute-start | bytes 1179656 | tf_op jit(solution)/shard_map/ppermute | solution.py:341
  47.4 0.0 copy-done.4
  47.4 0.0 copy-start
  47.4 3.7 %collective-permute-start.1 = (bf16[384,512]{1,0:T(8,128)(2,1)S(1)}, bf16[384,512]{1,0:T(8,128)(2,1)S(1)}, u32[]{:S(2)}, u32[]{:S(2)}) collective-permute-start(bf16[384,512]{1,0:T(8,128)(2,1)S(1)} %copy-done.4), channel_id=1, source_target_pairs={{0,2},{1,3},{2,0},{3,1},{4,6},{5,7},{6,4},{7,5},{8,10},{9,11},{10,... | collective-permute-start | bytes 1179656 | tf_op jit(solution)/shard_map/ppermute | solution.py:341
  51.1 0.0 copy-done.3
  51.1 0.0 copy-start.1
  51.2 2.5 %collective-permute-start.2 = (bf16[384,512]{1,0:T(8,128)(2,1)S(1)}, bf16[384,512]{1,0:T(8,128)(2,1)S(1)}, u32[]{:S(2)}, u32[]{:S(2)}) collective-permute-start(bf16[384,512]{1,0:T(8,128)(2,1)S(1)} %copy-done.3), channel_id=1, source_target_pairs={{0,3},{1,0},{2,1},{3,2},{4,7},{5,4},{6,5},{7,6},{8,11},{9,8},{10,9... | collective-permute-start | bytes 1179656 | tf_op jit(solution)/shard_map/ppermute | solution.py:341
  53.7 0.0 copy-done
  53.7 0.7 copy.24.ids_ref
  54.4 0.0 copy-done.1
  54.4 0.7 copy.25.logits_ref
  55.1 0.0 copy-start.2
  55.1 0.7 copy-done.2
  55.8 0.7 copy.26.group_ref
  56.5 1.4 %dynamic_slice.3 = f32[512]{0:T(512)} dynamic-slice(f32[2048]{0:T(1024)} %param.35, s32[]{:T(128)S(6)} %select_n.3), dynamic_slice_sizes={512} | dynamic-slice | bytes 4100 | tf_op jit(solution)/shard_map/dynamic_slice | solution.py:336
  57.8 1.8 %shard_map.223 = (bf16[48,256]{1,0:T(8,128)(2,1)S(1)}, bf16[48,256]{1,0:T(8,128)(2,1)S(1)}, bf16[384,512]{1,0:T(8,128)(2,1)S(1)}) custom-call(s32[48,2]{1,0:T(8,128)} %copy.24.ids_ref, f32[48,2]{1,0:T(8,128)} %copy.25.logits_ref, f32[48,1]{1,0:T(8,128)} %copy.26.group_ref, bf16[384,512]{1,0:T(8,128)(2,1)} %get-tuple-element.43.piece_ref), custom_call_target="tpu_custom_call" | custom-call | tf_op jit(solution)/shard_map/pallas_call | solution.py:318
  59.6 8.2 %all-to-all-done.2 = bf16[128,2,512]{2,1,0:T(2,128)(2,1)S(1)} async-done(((bf16[128,2,512]{2,1,0:T(2,128)(2,1)}), bf16[128,2,512]{2,1,0:T(2,128)(2,1)S(1)}, u32[]{:S(2)}, u32[]{:S(2)}) %all-to-all-start.2) | async-done | bytes 262176 | tf_op jit(solution)/shard_map/all_to_all | solution.py:351
  67.8 0.1 reshape.16.rows_ref
  67.9 0.0 collective-permute-done.refs_1_
  67.9 0.0 collective-permute-done.1.refs_2_
  67.9 1.4 %collective-permute-done.2.refs_3_ = bf16[384,512]{1,0:T(8,128)(2,1)S(1)} collective-permute-done((bf16[384,512]{1,0:T(8,128)(2,1)S(1)}, bf16[384,512]{1,0:T(8,128)(2,1)S(1)}, u32[]{:S(2)}, u32[]{:S(2)}) %collective-permute-start.2) | collective-permute-done | bytes 393248 | tf_op jit(solution)/shard_map/ppermute | solution.py:341
  69.3 1.3 shard_map.224
  70.6 13.3 %all_to_all.38.parts_ref = bf16[4,272,256]{2,1,0:T(8,128)(2,1)S(1)} all-to-all(bf16[4,272,256]{2,1,0:T(8,128)(2,1)S(1)} %get-tuple-element.50), channel_id=1, replica_groups=mesh['ep'=128,'tp'=4] {'tp'}, dimensions={0} | all-to-all | bytes 1114112 | tf_op jit(solution)/shard_map/all_to_all | solution.py:365
  83.9 0.2 shard_map.225
  84.1 7.9 %all_to_all.39.hidden_ref = bf16[4,256,128]{2,1,0:T(8,128)(2,1)S(1)} all-to-all(bf16[4,256,128]{2,1,0:T(8,128)(2,1)S(1)} %shard_map.225), channel_id=1, replica_groups=mesh['ep'=128,'tp'=4] {'tp'}, dimensions={0} | all-to-all | bytes 524288 | tf_op jit(solution)/shard_map/all_to_all | solution.py:367
  92.0 0.4 shard_map.226
  92.5 0.1 all_to_all.28
  92.6 41.2 %all_to_all.40 = bf16[128,2,512]{2,1,0:T(2,128)(2,1)S(1)} all-to-all(bf16[128,2,512]{2,1,0:T(2,128)(2,1)S(1)} %all_to_all.28), channel_id=1, replica_groups=mesh['ep'=128,'tp'=4] {'ep'}, dimensions={0} | all-to-all | bytes 524288 | tf_op jit(solution)/shard_map/all_to_all | solution.py:371
  133.7 0.1 all_to_all.30
  133.8 0.1 fusion.2
  134.0 0.8 fusion.1
Async XLA Ops:
  2.1 9.4 %all-to-all-start = ((bf16[4,48,512]{2,1,0:T(8,128)(2,1)}), bf16[4,48,512]{2,1,0:T(8,128)(2,1)S(1)}, u32[]{:S(2)}, u32[]{:S(2)}) async-start(bf16[4,48,512]{2,1,0:T(8,128)(2,1)} %broadcast_in_dim.30), calls=%async_computation | async-start | bytes 393216 | tf_op jit(solution)/shard_map/all_to_all | solution.py:283
  22.4 25.0 %copy-start.4 = (bf16[384,512]{1,0:T(8,128)(2,1)S(1)}, bf16[384,512]{1,0:T(8,128)(2,1)}, u32[]{:S(2)}) copy-start(bf16[384,512]{1,0:T(8,128)(2,1)} %get-tuple-element.48) | copy-start | bytes 1179652
  23.2 27.9 %copy-start.3 = (bf16[384,512]{1,0:T(8,128)(2,1)S(1)}, bf16[384,512]{1,0:T(8,128)(2,1)}, u32[]{:S(2)}) copy-start(bf16[384,512]{1,0:T(8,128)(2,1)} %get-tuple-element.49) | copy-start | bytes 1179652
  23.2 44.6 %all-to-all-start.2 = ((bf16[128,2,512]{2,1,0:T(2,128)(2,1)}), bf16[128,2,512]{2,1,0:T(2,128)(2,1)S(1)}, u32[]{:S(2)}, u32[]{:S(2)}) async-start(bf16[128,2,512]{2,1,0:T(2,128)(2,1)} %reshape.15), calls=%async_computation.2 | async-start | bytes 524288 | tf_op jit(solution)/shard_map/all_to_all | solution.py:351
  45.2 22.7 %collective-permute-start = (bf16[384,512]{1,0:T(8,128)(2,1)}, bf16[384,512]{1,0:T(8,128)(2,1)S(1)}, u32[]{:S(2)}, u32[]{:S(2)}) collective-permute-start(bf16[384,512]{1,0:T(8,128)(2,1)} %get-tuple-element.47), channel_id=1, source_target_pairs={{0,1},{1,2},{2,3},{3,0},{4,5},{5,6},{6,7},{7,4},{8,9},{9,10},{10,1... | collective-permute-start | bytes 1179656 | tf_op jit(solution)/shard_map/ppermute | solution.py:341
  47.4 6.3 %copy-start = (s32[48,2]{0,1:T(2,128)S(1)}, s32[48,2]{0,1:T(2,128)}, u32[]{:S(2)}) copy-start(s32[48,2]{0,1:T(2,128)} %param.36) | copy-start | bytes 1156
  47.4 20.5 %collective-permute-start.1 = (bf16[384,512]{1,0:T(8,128)(2,1)S(1)}, bf16[384,512]{1,0:T(8,128)(2,1)S(1)}, u32[]{:S(2)}, u32[]{:S(2)}) collective-permute-start(bf16[384,512]{1,0:T(8,128)(2,1)S(1)} %copy-done.4), channel_id=1, source_target_pairs={{0,2},{1,3},{2,0},{3,1},{4,6},{5,7},{6,4},{7,5},{8,10},{9,11},{10,... | collective-permute-start | bytes 1179656 | tf_op jit(solution)/shard_map/ppermute | solution.py:341
  51.1 3.3 %copy-start.1 = (f32[48,2]{0,1:T(2,128)S(1)}, f32[48,2]{0,1:T(2,128)}, u32[]{:S(2)}) copy-start(f32[48,2]{0,1:T(2,128)} %param.37) | copy-start | bytes 1156
  51.2 18.1 %collective-permute-start.2 = (bf16[384,512]{1,0:T(8,128)(2,1)S(1)}, bf16[384,512]{1,0:T(8,128)(2,1)S(1)}, u32[]{:S(2)}, u32[]{:S(2)}) collective-permute-start(bf16[384,512]{1,0:T(8,128)(2,1)S(1)} %copy-done.3), channel_id=1, source_target_pairs={{0,3},{1,0},{2,1},{3,2},{4,7},{5,4},{6,5},{7,6},{8,11},{9,8},{10,9... | collective-permute-start | bytes 1179656 | tf_op jit(solution)/shard_map/ppermute | solution.py:341
  55.1 0.7 copy-start.2

commit v5 on v4

--- a/solution.py
+++ b/solution.py
@@ -44,37 +44,79 @@
     return high, (value - high.astype(F32)).astype(BF16)
 
 
-def places(ids_ref, count, slots):
+def places(ids_ref, slots):
     ids = ids_ref[...]
-    column = lax.broadcasted_iota(jnp.int32, (count, slots), 1)
-    expert = lax.div(column, CAPACITY)
-    place = lax.rem(column, CAPACITY)
-    first = ids[:, 0:1] == expert
-    second = ids[:, 1:2] == expert
-    named = jnp.where(first | second, 1.0, 0.0)
-    below = lax.broadcasted_iota(jnp.int32, (count, count), 1) < lax.broadcasted_iota(
-        jnp.int32, (count, count), 0
-    )
-    earlier = dot(jnp.where(below, 1.0, 0.0).astype(BF16), named.astype(BF16))
+    count = ids.shape[1]
+    row = lax.broadcasted_iota(jnp.int32, (slots, count), 0)
+    expert = lax.div(row, CAPACITY)
+    place = lax.rem(row, CAPACITY)
+    first = ids[0:1] == expert
+    named = jnp.where(first | (ids[1:2] == expert), 1.0, 0.0)
+    before = lax.broadcasted_iota(jnp.int32, (count, count), 0) < lax.broadcasted_iota(
+        jnp.int32, (count, count), 1
+    )
+    earlier = dot(named.astype(BF16), jnp.where(before, 1.0, 0.0).astype(BF16))
     return jnp.where(earlier == place.astype(F32), named, 0.0), first
 
 
-def combine_tables(ids_ref, logits_ref, group_ref, piece_ref, high_ref, low_ref, near_ref, done):
-    copy = pltpu.make_async_copy(piece_ref, near_ref, done)
-    copy.start()
-    hit, first = places(ids_ref, *high_ref.shape)
+def dispatch_table(
+    ids_ref, weight_ref, tokens_ref, out_ref, weight_near_ref, tokens_near_ref, ids_near_ref, done
+):
+    copies = [
+        pltpu.make_async_copy(source, into, done.at[j])
+        for j, (source, into) in enumerate(
+            [
+                (ids_ref, ids_near_ref),
+                (weight_ref, weight_near_ref),
+                (tokens_ref, tokens_near_ref),
+            ]
+        )
+    ]
+    for copy in copies:
+        copy.start()
+    copies[0].wait()
+    out_ref[...] = places(ids_near_ref, out_ref.shape[0])[0].astype(BF16)
+    for copy in copies[1:]:
+        copy.wait()
+
+
+def combine_tables(
+    member_ref,
+    ids_ref,
+    logits_ref,
+    group_ref,
+    piece_ref,
+    gain_ref,
+    high_ref,
+    low_ref,
+    piece_near_ref,
+    gain_near_ref,
+    done,
+):
+    quarter = gain_near_ref.shape[1]
+    own = pl.multiple_of(member_ref[0] * quarter, quarter)
+    copies = [
+        pltpu.make_async_copy(piece_ref, piece_near_ref, done.at[0]),
+        pltpu.make_async_copy(gain_ref.at[:, pl.ds(own, quarter)], gain_near_ref, done.at[1]),
+    ]
+    for copy in copies:
+        copy.start()
+    hit, first = places(ids_ref, high_ref.shape[0])
     raised = jnp.exp(logits_ref[...])
-    weight = group_ref[...] * raised / (raised[:, 0:1] + raised[:, 1:2])
-    high, low = halves(hit * jnp.where(first, weight[:, 0:1], weight[:, 1:2]))
+    weight = group_ref[...] * raised / (raised[0:1] + raised[1:2])
+    high, low = halves(hit * jnp.where(first, weight[0:1], weight[1:2]))
     high_ref[...] = high
     low_ref[...] = low
-    copy.wait()
+    for copy in copies:
+        copy.wait()
 
 
 def cut_weights(member_ref, gate_ref, up_ref, down_ref, *refs, members):
     *rest, piece_ref, reads, writes, loads = refs
-    count = (len(rest) - members) // 2
-    far_refs, out_refs, near_refs = rest[:count], rest[count : count + members], rest[count + members :]
+    pieces = 2 * members - 2
+    count = (len(rest) - pieces) // 2
+    far_refs, rest = rest[:count], rest[count:]
+    out_refs, near_refs = rest[:pieces], rest[pieces:]
     quarter = gate_ref.shape[1] // members
     half = quarter // 2
     width = gate_ref.shape[2]
@@ -102,12 +144,19 @@
     ]
     for copy in near_copies:
         copy.start()
+    whole = pl.ds(0, half + width)
+    parts = [(0, whole), (2, whole)]
+    for k in (1, 3):
+        parts += [(k, pl.ds(0, half)), (k, pl.ds(half, width))]
     out_copies = []
     for k in order:
         for copy in copies[k]:
             copy.wait()
-        out_copies.append(pltpu.make_async_copy(piece_ref.at[k], out_refs[k], writes.at[k]))
-        out_copies[-1].start()
+        for j, (owner, rows) in enumerate(parts):
+            if owner == k:
+                copy = pltpu.make_async_copy(piece_ref.at[k, rows], out_refs[j], writes.at[j])
+                copy.start()
+                out_copies.append(copy)
     for copy in near_copies + out_copies:
         copy.wait()
 
@@ -174,32 +223,18 @@
         copies_ref[m] = out
 
 
-def stream_rows(parts_ref, tokens_ref, ids_ref, weight_ref, stream_ref, out_ref, near_ref, done):
-    copy = pltpu.make_async_copy(weight_ref, near_ref, done)
-    copy.start()
-    slots, count = out_ref.shape[0], tokens_ref.shape[0]
-    row = lax.broadcasted_iota(jnp.int32, (slots, count), 0)
-    expert = lax.div(row, CAPACITY)
-    place = lax.rem(row, CAPACITY)
-    ids = ids_ref[...]
-    named = jnp.where((ids[0:1] == expert) | (ids[1:2] == expert), 1.0, 0.0)
-    before = lax.broadcasted_iota(jnp.int32, (count, count), 0) < lax.broadcasted_iota(
-        jnp.int32, (count, count), 1
-    )
-    earlier = dot(named.astype(BF16), jnp.where(before, 1.0, 0.0).astype(BF16))
-    dispatch = jnp.where(earlier == place.astype(F32), named, 0.0).astype(BF16)
-    copy.wait()
+def stream_rows(parts_ref, weight_ref, tokens_ref, dispatch_ref, stream_ref, out_ref):
     members, _, width = parts_ref.shape
-    mixed = dot(parts_ref[0], near_ref[:width, :])
+    mixed = dot(parts_ref[0], weight_ref[:width, :])
     for m in range(1, members):
-        mixed = mixed + dot(parts_ref[m], near_ref[m * width : (m + 1) * width, :])
+        mixed = mixed + dot(parts_ref[m], weight_ref[m * width : (m + 1) * width, :])
     stream = (tokens_ref[...].astype(F32) + mixed).astype(BF16)
     stream_ref[...] = stream
-    out_ref[...] = dot(dispatch, stream).astype(BF16)
+    out_ref[...] = dot(dispatch_ref[...], stream).astype(BF16)
 
 
 def first_products(member_ref, rows_ref, gain_ref, *refs):
-    *weight_refs, out_ref, down_ref = refs
+    *weight_refs, out_ref = refs
     members = len(weight_refs)
     count, width = rows_ref.shape
     half = width // 2
@@ -217,7 +252,6 @@
     for k in range(members):
         out_ref[k, count:, :] = sums
     for k, cut in enumerate(weight_refs):
-        down_ref[owners[k]] = cut[half:, :]
         product = dot(scaled[:, :half], cut[:half, :half]) + dot(
             scaled[:, half:], cut[:half, half:]
         )
@@ -241,10 +275,13 @@
         out_ref[k] = hidden
 
 
-def last_product(hidden_ref, down_ref, out_ref):
-    total = dot(hidden_ref[0], down_ref[0])
-    for k in range(1, hidden_ref.shape[0]):
-        total = total + dot(hidden_ref[k], down_ref[k])
+def last_product(member_ref, hidden_ref, *refs):
+    *weight_refs, out_ref = refs
+    members, _, width = hidden_ref.shape
+    total = jnp.zeros(out_ref.shape, F32)
+    for k, weight_ref in enumerate(weight_refs):
+        owner = lax.rem(member_ref[0] + (members - k), members)
+        total = total + dot(hidden_ref[owner], weight_ref[weight_ref.shape[0] - width :, :])
     out_ref[...] = total.astype(BF16)
 
 
@@ -284,7 +321,6 @@
         jnp.broadcast_to(tokens[None], (members, *tokens.shape)), "tp", 0, 0, tiled=True
     )
     anywhere = pl.BlockSpec(memory_space=pl.ANY)
-    piece = (quarter // 2 + units, quarter)
     operands = [
         mix_gain[None],
         input_weight,
@@ -299,29 +335,43 @@
         decay_param[None],
         lru_state,
     ]
+    half, whole = (quarter // 2, quarter), (quarter // 2 + units, quarter)
+    cuts = [whole, whole, half, (units, quarter), half, (units, quarter)]
     cutting = pl.pallas_call(
         functools.partial(cut_weights, members=members),
-        out_shape=[jax.ShapeDtypeStruct(piece, BF16)] * members
+        out_shape=[jax.ShapeDtypeStruct(shape, BF16) for shape in cuts]
         + [pltpu.VMEM(value.shape, value.dtype) for value in operands],
         in_specs=[SMEM] + [anywhere] * (3 + len(operands)),
-        out_specs=[anywhere] * members + [VMEM] * len(operands),
+        out_specs=[anywhere] * len(cuts) + [VMEM] * len(operands),
         scratch_shapes=[
-            pltpu.VMEM((members, *piece), BF16),
+            pltpu.VMEM((members, *whole), BF16),
             pltpu.SemaphoreType.DMA((members, 5)),
-            pltpu.SemaphoreType.DMA((members,)),
+            pltpu.SemaphoreType.DMA((len(cuts),)),
             pltpu.SemaphoreType.DMA((len(operands),)),
         ],
     )
     loaded = cutting(place, expert_gate, expert_up, expert_down, *operands)
-    pieces, operands = loaded[:members], loaded[members:]
-    table = pltpu.VMEM((seq_count, slots), BF16)
-    combine_high, combine_low, own_piece = pl.pallas_call(
+    own, across, *sides = loaded[: len(cuts)]
+    operands = [near(value) for value in loaded[len(cuts) :]]
+    table = pltpu.VMEM((slots, seq_count), BF16)
+    ids = route_ids.T
+    dispatch, output_near, tokens_near = pl.pallas_call(
+        dispatch_table,
+        out_shape=[table, pltpu.VMEM(output_weight.shape, BF16), pltpu.VMEM(tokens.shape, BF16)],
+        in_specs=[anywhere] * 3,
+        out_specs=[VMEM] * 3,
+        scratch_shapes=[
+            pltpu.VMEM(ids.shape, ids.dtype),
+            pltpu.SemaphoreType.DMA((3,)),
+        ],
+    )(ids, output_weight, tokens)
+    combine_high, combine_low, own, gain_part = pl.pallas_call(
         combine_tables,
-        out_shape=[table, table, pltpu.VMEM(piece, BF16)],
-        in_specs=[VMEM] * 3 + [anywhere],
-        out_specs=[VMEM] * 3,
-        scratch_shapes=[pltpu.SemaphoreType.DMA],
-    )(route_ids, route_logits, group_weight[:, None], pieces[0])
+        out_shape=[table, table, pltpu.VMEM(whole, BF16), pltpu.VMEM((1, quarter), F32)],
+        in_specs=[SMEM] + [VMEM] * 3 + [anywhere] * 2,
+        out_specs=[VMEM] * 4,
+        scratch_shapes=[pltpu.SemaphoreType.DMA((2,))],
+    )(place, ids, route_logits.T, group_weight[None], own, moe_gain[None])
     copies, new_state, window = call(
         mixer,
         [
@@ -330,46 +380,59 @@
             jax.ShapeDtypeStruct((conv_state.shape[1], seq_count, channels), BF16),
         ],
         near(token_parts),
-        *[near(value) for value in operands],
-    )
-    first_feature = member * quarter
-    gain_part = lax.dynamic_slice_in_dim(moe_gain, first_feature, quarter, 0)[None]
+        *operands,
+    )
     mixer_parts = lax.all_to_all(copies, "tp", 0, 0, tiled=True)
-    weights = []
-    for k in range(1, members):
-        ring = [(m, (m + k) % members) for m in range(members)]
-        weights.append(lax.ppermute(pieces[k], "tp", ring))
-    stream, outgoing = pl.pallas_call(
+
+    def onward(value, step):
+        ring = [(m, (m + step) % members) for m in range(members)]
+        return lax.ppermute(value, "tp", ring)
+
+    across = onward(across, 2)
+    cut_next = onward(sides[0], 1)
+    cut_last = onward(sides[2], 3)
+    down_next = onward(sides[1], 1)
+    down_last = onward(sides[3], 3)
+    stream, outgoing = call(
         stream_rows,
-        out_shape=[pltpu.VMEM((seq_count, quarter), BF16), pltpu.VMEM((slots, quarter), BF16)],
-        in_specs=[VMEM] * 3 + [anywhere],
-        out_specs=[VMEM] * 2,
-        scratch_shapes=[pltpu.VMEM(output_weight.shape, BF16), pltpu.SemaphoreType.DMA],
-    )(near(mixer_parts), tokens, route_ids.T, output_weight)
+        [pltpu.VMEM((seq_count, quarter), BF16), pltpu.VMEM((slots, quarter), BF16)],
+        near(mixer_parts),
+        near(output_near),
+        near(tokens_near),
+        near(dispatch),
+    )
 
     outgoing = outgoing.reshape(experts, CAPACITY, quarter)
     arrived = lax.all_to_all(outgoing, "ep", 0, 0, tiled=True)
     arrived = arrived.reshape(slots, quarter)
-    products, down = call(
+    own, across = near(own), near(across)
+    products = call(
         first_products,
-        [
-            pltpu.VMEM((members, slots + SUM_ROWS, 2 * units), BF16),
-            pltpu.VMEM((members, units, quarter), BF16),
-        ],
+        pltpu.VMEM((members, slots + SUM_ROWS, 2 * units), BF16),
         near(arrived),
-        gain_part,
-        near(own_piece),
-        *[near(w) for w in weights],
+        near(gain_part),
+        own,
+        near(cut_next),
+        across,
+        near(cut_last),
         scalar=place,
     )
     products = lax.all_to_all(products, "tp", 0, 0, tiled=True)
     hidden = call(hidden_units, pltpu.VMEM((members, slots, units), BF16), near(products))
+    hidden, down_next, down_last = lax.optimization_barrier((hidden, down_next, down_last))
     hidden = lax.all_to_all(hidden, "tp", 0, 0, tiled=True)
     answer = call(
-        last_product, pltpu.VMEM((slots, quarter), BF16), near(hidden), near(down)
+        last_product,
+        pltpu.VMEM((slots, quarter), BF16),
+        near(hidden),
+        own,
+        near(down_next),
+        across,
+        near(down_last),
+        scalar=place,
     )
     returned = lax.all_to_all(answer, "ep", 0, 0, tiled=True)
-    routed = dot(combine_high, returned) + dot(combine_low, returned)
+    routed = dot_on(combine_high, returned, 0, 0) + dot_on(combine_low, returned, 0, 0)
     result = (stream.astype(F32) + routed).astype(BF16)
     return (result, new_state, jnp.swapaxes(window, 0, 1))
 

time: 136 us -> 132 us (0.971)
  blocking collectives: 69.4 us -> 45.9 us
  starting transfers between devices: 34.6 us -> 48.6 us
  waiting for transfers between devices: 11.3 us -> 22.2 us
  local copies, waits for them, and re-layouts: 6.75 us -> 2.62 us
    all_to_all x2 -> x0, blocking collectives: 20.3 us -> none  [the longest x1 13.3 us: body(): products = lax.all_to_all(products, 'tp', 0, 0, tiled=True)]
    ppermute x3 -> x5, starting transfers between devices: 8.43 us -> 15.5 us  [onward(): return lax.ppermute(value, 'tp', ring)]
    all_to_all x0 -> x2, starting transfers between devices: none -> 6.91 us  [the longest x1 3.6 us: body(): products = lax.all_to_all(products, 'tp', 0, 0, tiled=True)]
    all_to_all x0 -> x2, waiting for transfers between devices: none -> 6.43 us  [the longest x1 3.34 us: body(): mixer_parts = lax.all_to_all(copies, 'tp', 0, 0, tiled=True)]
    all_to_all x1, waiting for transfers between devices: 8.16 us -> 11.8 us  [body(): arrived = lax.all_to_all(outgoing, 'ep', 0, 0, tiled=True)]
    all_to_all x1, blocking collectives: 41.2 us -> 37.8 us  [body(): returned = lax.all_to_all(answer, 'ep', 0, 0, tiled=True)]
    unnamed x12 -> x10, local copies, waits for them, and re-layouts: 2.07 us -> 0.02 us
    pallas_call x4 -> x5, Pallas kernels: 3.25 us -> 3.92 us  [call(): pl.pallas_call(kernel, out_shape=outs, in_specs=[SMEM] * len(scalars) + [...]
  transfers between devices with their start and end apart: 5 -> 9, of which waited for: 3 -> 5; matrix products, arithmetic and copies ran while one was open for 3% -> 0% of each run, Pallas kernels for 4% -> 5%
where the time goes in v5:
time: 132 us; the launch traced here: 131 us
  starting transfers between devices  48.6 us (37%)
  blocking collectives  45.9 us (35%)
  waiting for transfers between devices  22.2 us (17%)
  Pallas kernels  10.4 us (8%)
  local copies, waits for them, and re-layouts  2.62 us (2%)
    all_to_all x1, blocking collectives, body(): returned = lax.all_to_all(answer, 'ep', 0, 0, tiled=True)  37.8 us
    all_to_all x1, starting transfers between devices, body(): arrived = lax.all_to_all(outgoing, 'ep', 0, 0, tiled=True)  22 us
    ppermute x5, starting transfers between devices, onward(): return lax.ppermute(value, 'tp', ring)  15.5 us
    all_to_all x1, waiting for transfers between devices, body(): arrived = lax.all_to_all(outgoing, 'ep', 0, 0, tiled=True)  11.8 us
    all_to_all x1, blocking collectives, body(): hidden = lax.all_to_all(hidden, 'tp', 0, 0, tiled=True)  8.03 us
    all_to_all x1, starting transfers between devices, body(): lax.all_to_all(jnp.broadcast_to(tokens[None], (members, *tokens.shape)),...  4.18 us
    pallas_call x5, Pallas kernels, call(): pl.pallas_call(kernel, out_shape=outs, in_specs=[SMEM] * len(scalars) + [...  3.92 us
    all_to_all x1, starting transfers between devices, body(): products = lax.all_to_all(products, 'tp', 0, 0, tiled=True)  3.6 us
  transfers between devices with their start and end apart: 9, of which 5 were waited for; matrix products, arithmetic and copies ran while one was open for 0% of the time, Pallas kernels for 5%

profile of v5, /device:TPU:33, one launch (start us, length us, event | category | flops | bytes accessed | tf_op | source)
XLA Modules:
  0.0 131.4 jit_solution(11034948223989206882)
XLA Ops:
  0.6 1.5 %broadcast_in_dim.30 = bf16[4,48,512]{2,1,0:T(8,128)(2,1)} broadcast(bf16[48,512]{1,0:T(8,128)(2,1)} %tokens_ref.1), dimensions={1,2} | broadcast | bytes 245760 | tf_op jit(solution)/shard_map/broadcast_in_dim | solution.py:321
  2.1 4.2 %all-to-all-start = ((bf16[4,48,512]{2,1,0:T(8,128)(2,1)}), bf16[4,48,512]{2,1,0:T(8,128)(2,1)S(1)}, u32[]{:S(2)}, u32[]{:S(2)}) async-start(bf16[4,48,512]{2,1,0:T(8,128)(2,1)} %broadcast_in_dim.30), calls=%async_computation | async-start | bytes 393216 | tf_op jit(solution)/shard_map/all_to_all | solution.py:320
  6.3 3.5 %shard_map.220 = (bf16[384,512]{1,0:T(8,128)(2,1)}, bf16[384,512]{1,0:T(8,128)(2,1)}, bf16[256,512]{1,0:T(8,128)(2,1)}, bf16[128,512]{1,0:T(8,128)(2,1)}, bf16[2...) custom-call(s32[1]{0:T(128)} %bitcast.member_ref, ...), custom_call_target="tpu_custom_call" | custom-call | tf_op jit(solution)/shard_map/pallas_call | solution.py:353
  9.8 1.7 %all-to-all-done.parts_ref = bf16[4,48,512]{2,1,0:T(8,128)(2,1)S(1)} async-done(((bf16[4,48,512]{2,1,0:T(8,128)(2,1)}), bf16[4,48,512]{2,1,0:T(8,128)(2,1)S(1)}, u32[]{:S(2)}, u32[]{:S(2)}) %all-to-all-start) | async-done | bytes 196640 | tf_op jit(solution)/shard_map/all_to_all | solution.py:320
  11.5 1.4 %shard_map.221 = (bf16[4,48,256]{2,1,0:T(8,128)(2,1)}, f32[48,256]{1,0:T(8,128)}, bf16[3,48,256]{2,1,0:T(8,128)(2,1)}) custom-call(bf16[4,48,512]{2,1,0:T(8,128)(2,1)S(1)} %all-to-all-done.parts_ref, f32[1,2048]{1,0:T(1,128)S(1)} %get-tuple-element.36.gain_ref, bf16[2048,256]{1,0:T(8,128)(2,1)S(1)} %get-tuple-element.37.input_ref, ...), custom_call_target="tpu_custom_call" | custom-call | tf_op jit(solution)/shard_map/pallas_call | solution.py:26
  12.9 3.3 %all-to-all-start.1 = ((bf16[4,48,256]{2,1,0:T(8,128)(2,1)}), bf16[4,48,256]{2,1,0:T(8,128)(2,1)S(1)}, u32[]{:S(2)}, u32[]{:S(2)}) async-start(bf16[4,48,256]{2,1,0:T(8,128)(2,1)} %get-tuple-element.48), calls=%async_computation.1 | async-start | bytes 196608 | tf_op jit(solution)/shard_map/all_to_all | solution.py:385
  16.2 1.3 shard_map.222
  17.5 3.3 %all-to-all-done.1.parts_ref = bf16[4,48,256]{2,1,0:T(8,128)(2,1)S(1)} async-done(((bf16[4,48,256]{2,1,0:T(8,128)(2,1)}), bf16[4,48,256]{2,1,0:T(8,128)(2,1)S(1)}, u32[]{:S(2)}, u32[]{:S(2)}) %all-to-all-start.1) | async-done | bytes 98336 | tf_op jit(solution)/shard_map/all_to_all | solution.py:385
  20.8 0.5 shard_map.223
  21.3 0.0 copy-start.2
  21.3 0.0 copy-start.1
  21.3 0.8 reshape.15
  22.1 0.0 copy-start
  22.1 22.0 %all-to-all-start.2 = ((bf16[128,2,512]{2,1,0:T(2,128)(2,1)}), bf16[128,2,512]{2,1,0:T(2,128)(2,1)S(1)}, u32[]{:S(2)}, u32[]{:S(2)}) async-start(bf16[128,2,512]{2,1,0:T(2,128)(2,1)} %reshape.15), calls=%async_computation.2 | async-start | bytes 524288 | tf_op jit(solution)/shard_map/all_to_all | solution.py:406
  44.1 0.0 copy-done
  44.1 2.5 %collective-permute-start.1 = (bf16[384,512]{1,0:T(8,128)(2,1)S(1)}, bf16[384,512]{1,0:T(8,128)(2,1)S(1)}, u32[]{:S(2)}, u32[]{:S(2)}) collective-permute-start(bf16[384,512]{1,0:T(8,128)(2,1)S(1)} %copy-done), channel_id=1, source_target_pairs={{0,2},{1,3},{2,0},{3,1},{4,6},{5,7},{6,4},{7,5},{8,10},{9,11},{10,... | collective-permute-start | bytes 1179656 | tf_op jit(solution)/shard_map/ppermute | solution.py:389
  46.7 0.0 copy-done.2
  46.7 2.7 %collective-permute-start = (bf16[256,512]{1,0:T(8,128)(2,1)S(1)}, bf16[256,512]{1,0:T(8,128)(2,1)S(1)}, u32[]{:S(2)}, u32[]{:S(2)}) collective-permute-start(bf16[256,512]{1,0:T(8,128)(2,1)S(1)} %copy-done.2), channel_id=1, source_target_pairs={{0,1},{1,2},{2,3},{3,0},{4,5},{5,6},{6,7},{7,4},{8,9},{9,10},{10,1... | collective-permute-start | bytes 786440 | tf_op jit(solution)/shard_map/ppermute | solution.py:389
  49.4 0.0 copy-done.1
  49.5 3.8 %collective-permute-start.2 = (bf16[256,512]{1,0:T(8,128)(2,1)S(1)}, bf16[256,512]{1,0:T(8,128)(2,1)S(1)}, u32[]{:S(2)}, u32[]{:S(2)}) collective-permute-start(bf16[256,512]{1,0:T(8,128)(2,1)S(1)} %copy-done.1), channel_id=1, source_target_pairs={{0,3},{1,0},{2,1},{3,2},{4,7},{5,4},{6,5},{7,6},{8,11},{9,8},{10,9... | collective-permute-start | bytes 786440 | tf_op jit(solution)/shard_map/ppermute | solution.py:389
  53.2 1.7 %shard_map.224 = (bf16[256,48]{1,0:T(8,128)(2,1)S(1)}, bf16[256,48]{1,0:T(8,128)(2,1)S(1)}, bf16[384,512]{1,0:T(8,128)(2,1)S(1)}, f32[1,512]{1,0:T(1,128)S(1)}) custom-call(s32[1]{0:T(128)} %bitcast.member_ref, s32[2,48]{1,0:T(2,128)} %bitcast.20, f32[2,48]{1,0:T(2,128)} %bitcast.21, f32[1,48]{1,0:T(1,128)} %bitcast.26, ...), custom_call_target="tpu_custom_call" | custom-call | tf_op jit(solution)/shard_map/pallas_call | solution.py:368
  54.9 11.8 %all-to-all-done.2 = bf16[128,2,512]{2,1,0:T(2,128)(2,1)S(1)} async-done(((bf16[128,2,512]{2,1,0:T(2,128)(2,1)}), bf16[128,2,512]{2,1,0:T(2,128)(2,1)S(1)}, u32[]{:S(2)}, u32[]{:S(2)}) %all-to-all-start.2) | async-done | bytes 262176 | tf_op jit(solution)/shard_map/all_to_all | solution.py:406
  66.7 0.1 reshape.16.rows_ref
  66.8 0.0 collective-permute-done.refs_1_
  66.8 0.0 collective-permute-done.2.refs_3_
  66.8 0.0 collective-permute-done.1.refs_2_
  66.9 1.4 %shard_map.225 = bf16[4,272,256]{2,1,0:T(8,128)(2,1)} custom-call(s32[1]{0:T(128)} %bitcast.member_ref, bf16[256,512]{1,0:T(8,128)(2,1)S(1)} %reshape.16.rows_ref, f32[1,512]{1,0:T(1,128)S(1)} %get-tuple-element.56.gain_ref, bf16[384,512]{1,0:T(8,128)(2,1)S(1)} %get-tuple-element.57.refs_0_, bf16[256,512]{1,0:T(8,128)(2,1)S(1)} %collective-permute-done.refs_1_, ...), custom_call_target="tpu_custom_call" | custom-call | tf_op jit(solution)/shard_map/pallas_call | solution.py:26
  68.2 0.0 copy-start.4
  68.2 0.0 copy-start.3
  68.2 3.6 %all-to-all-start.3 = ((bf16[4,272,256]{2,1,0:T(8,128)(2,1)}), bf16[4,272,256]{2,1,0:T(8,128)(2,1)S(1)}, u32[]{:S(2)}, u32[]{:S(2)}) async-start(bf16[4,272,256]{2,1,0:T(8,128)(2,1)} %shard_map.225), calls=%async_computation.3 | async-start | bytes 1114112 | tf_op jit(solution)/shard_map/all_to_all | solution.py:420
  71.9 0.0 copy-done.4
  71.9 3.3 %collective-permute-start.3 = (bf16[128,512]{1,0:T(8,128)(2,1)S(1)}, bf16[128,512]{1,0:T(8,128)(2,1)S(1)}, u32[]{:S(2)}, u32[]{:S(2)}) collective-permute-start(bf16[128,512]{1,0:T(8,128)(2,1)S(1)} %copy-done.4), channel_id=1, source_target_pairs={{0,1},{1,2},{2,3},{3,0},{4,5},{5,6},{6,7},{7,4},{8,9},{9,10},{10,1... | collective-permute-start | bytes 393224 | tf_op jit(solution)/shard_map/ppermute | solution.py:389
  75.2 0.0 copy-done.3
  75.2 3.2 %collective-permute-start.4 = (bf16[128,512]{1,0:T(8,128)(2,1)S(1)}, bf16[128,512]{1,0:T(8,128)(2,1)S(1)}, u32[]{:S(2)}, u32[]{:S(2)}) collective-permute-start(bf16[128,512]{1,0:T(8,128)(2,1)S(1)} %copy-done.3), channel_id=1, source_target_pairs={{0,3},{1,0},{2,1},{3,2},{4,7},{5,4},{6,5},{7,6},{8,11},{9,8},{10,9... | collective-permute-start | bytes 393224 | tf_op jit(solution)/shard_map/ppermute | solution.py:389
  78.4 3.1 %all-to-all-done.3.parts_ref = bf16[4,272,256]{2,1,0:T(8,128)(2,1)S(1)} async-done(((bf16[4,272,256]{2,1,0:T(8,128)(2,1)}), bf16[4,272,256]{2,1,0:T(8,128)(2,1)S(1)}, u32[]{:S(2)}, u32[]{:S(2)}) %all-to-all-start.3) | async-done | bytes 557088 | tf_op jit(solution)/shard_map/all_to_all | solution.py:420
  81.5 0.2 shard_map.226
  81.7 2.2 %collective-permute-done.3.refs_1_ = bf16[128,512]{1,0:T(8,128)(2,1)S(1)} collective-permute-done((bf16[128,512]{1,0:T(8,128)(2,1)S(1)}, bf16[128,512]{1,0:T(8,128)(2,1)S(1)}, u32[]{:S(2)}, u32[]{:S(2)}) %collective-permute-start.3) | collective-permute-done | bytes 131104 | tf_op jit(solution)/shard_map/ppermute | solution.py:389
  84.0 0.0 collective-permute-done.4.refs_3_
  84.0 8.0 %all_to_all.37.hidden_ref = bf16[4,256,128]{2,1,0:T(8,128)(2,1)S(1)} all-to-all(bf16[4,256,128]{2,1,0:T(8,128)(2,1)S(1)} %shard_map.226), channel_id=1, replica_groups=mesh['ep'=128,'tp'=4] {'tp'}, dimensions={0} | all-to-all | bytes 524288 | tf_op jit(solution)/shard_map/all_to_all | solution.py:423
  92.0 0.4 shard_map.227
  92.4 0.1 all_to_all.28
  92.5 37.8 %all_to_all.38 = bf16[128,2,512]{2,1,0:T(2,128)(2,1)S(1)} all-to-all(bf16[128,2,512]{2,1,0:T(2,128)(2,1)S(1)} %all_to_all.28), channel_id=1, replica_groups=mesh['ep'=128,'tp'=4] {'ep'}, dimensions={0} | all-to-all | bytes 524288 | tf_op jit(solution)/shard_map/all_to_all | solution.py:434
  130.3 0.1 all_to_all.30
  130.4 0.2 fusion.2
  130.6 0.8 fusion.1
Async XLA Ops:
  2.1 9.4 %all-to-all-start = ((bf16[4,48,512]{2,1,0:T(8,128)(2,1)}), bf16[4,48,512]{2,1,0:T(8,128)(2,1)S(1)}, u32[]{:S(2)}, u32[]{:S(2)}) async-start(bf16[4,48,512]{2,1,0:T(8,128)(2,1)} %broadcast_in_dim.30), calls=%async_computation | async-start | bytes 393216 | tf_op jit(solution)/shard_map/all_to_all | solution.py:320
  12.9 7.9 %all-to-all-start.1 = ((bf16[4,48,256]{2,1,0:T(8,128)(2,1)}), bf16[4,48,256]{2,1,0:T(8,128)(2,1)S(1)}, u32[]{:S(2)}, u32[]{:S(2)}) async-start(bf16[4,48,256]{2,1,0:T(8,128)(2,1)} %get-tuple-element.48), calls=%async_computation.1 | async-start | bytes 196608 | tf_op jit(solution)/shard_map/all_to_all | solution.py:385
  21.3 25.4 %copy-start.2 = (bf16[256,512]{1,0:T(8,128)(2,1)S(1)}, bf16[256,512]{1,0:T(8,128)(2,1)}, u32[]{:S(2)}) copy-start(bf16[256,512]{1,0:T(8,128)(2,1)} %get-tuple-element.58) | copy-start | bytes 786436
  21.3 28.1 %copy-start.1 = (bf16[256,512]{1,0:T(8,128)(2,1)S(1)}, bf16[256,512]{1,0:T(8,128)(2,1)}, u32[]{:S(2)}) copy-start(bf16[256,512]{1,0:T(8,128)(2,1)} %get-tuple-element.60) | copy-start | bytes 786436
  22.1 22.0 %copy-start = (bf16[384,512]{1,0:T(8,128)(2,1)S(1)}, bf16[384,512]{1,0:T(8,128)(2,1)}, u32[]{:S(2)}) copy-start(bf16[384,512]{1,0:T(8,128)(2,1)} %get-tuple-element.59) | copy-start | bytes 1179652
  22.1 44.6 %all-to-all-start.2 = ((bf16[128,2,512]{2,1,0:T(2,128)(2,1)}), bf16[128,2,512]{2,1,0:T(2,128)(2,1)S(1)}, u32[]{:S(2)}, u32[]{:S(2)}) async-start(bf16[128,2,512]{2,1,0:T(2,128)(2,1)} %reshape.15), calls=%async_computation.2 | async-start | bytes 524288 | tf_op jit(solution)/shard_map/all_to_all | solution.py:406
  44.1 22.7 %collective-permute-start.1 = (bf16[384,512]{1,0:T(8,128)(2,1)S(1)}, bf16[384,512]{1,0:T(8,128)(2,1)S(1)}, u32[]{:S(2)}, u32[]{:S(2)}) collective-permute-start(bf16[384,512]{1,0:T(8,128)(2,1)S(1)} %copy-done), channel_id=1, source_target_pairs={{0,2},{1,3},{2,0},{3,1},{4,6},{5,7},{6,4},{7,5},{8,10},{9,11},{10,... | collective-permute-start | bytes 1179656 | tf_op jit(solution)/shard_map/ppermute | solution.py:389
  46.7 20.1 %collective-permute-start = (bf16[256,512]{1,0:T(8,128)(2,1)S(1)}, bf16[256,512]{1,0:T(8,128)(2,1)S(1)}, u32[]{:S(2)}, u32[]{:S(2)}) collective-permute-start(bf16[256,512]{1,0:T(8,128)(2,1)S(1)} %copy-done.2), channel_id=1, source_target_pairs={{0,1},{1,2},{2,3},{3,0},{4,5},{5,6},{6,7},{7,4},{8,9},{9,10},{10,1... | collective-permute-start | bytes 786440 | tf_op jit(solution)/shard_map/ppermute | solution.py:389
  49.5 17.4 %collective-permute-start.2 = (bf16[256,512]{1,0:T(8,128)(2,1)S(1)}, bf16[256,512]{1,0:T(8,128)(2,1)S(1)}, u32[]{:S(2)}, u32[]{:S(2)}) collective-permute-start(bf16[256,512]{1,0:T(8,128)(2,1)S(1)} %copy-done.1), channel_id=1, source_target_pairs={{0,3},{1,0},{2,1},{3,2},{4,7},{5,4},{6,5},{7,6},{8,11},{9,8},{10,9... | collective-permute-start | bytes 786440 | tf_op jit(solution)/shard_map/ppermute | solution.py:389
  68.2 3.6 %copy-start.4 = (bf16[128,512]{1,0:T(8,128)(2,1)S(1)}, bf16[128,512]{1,0:T(8,128)(2,1)}, u32[]{:S(2)}) copy-start(bf16[128,512]{1,0:T(8,128)(2,1)} %get-tuple-element.61) | copy-start | bytes 393220
  68.2 6.9 %copy-start.3 = (bf16[128,512]{1,0:T(8,128)(2,1)S(1)}, bf16[128,512]{1,0:T(8,128)(2,1)}, u32[]{:S(2)}) copy-start(bf16[128,512]{1,0:T(8,128)(2,1)} %get-tuple-element.62) | copy-start | bytes 393220
  68.2 13.2 %all-to-all-start.3 = ((bf16[4,272,256]{2,1,0:T(8,128)(2,1)}), bf16[4,272,256]{2,1,0:T(8,128)(2,1)S(1)}, u32[]{:S(2)}, u32[]{:S(2)}) async-start(bf16[4,272,256]{2,1,0:T(8,128)(2,1)} %shard_map.225), calls=%async_computation.3 | async-start | bytes 1114112 | tf_op jit(solution)/shard_map/all_to_all | solution.py:420
  71.9 12.1 %collective-permute-start.3 = (bf16[128,512]{1,0:T(8,128)(2,1)S(1)}, bf16[128,512]{1,0:T(8,128)(2,1)S(1)}, u32[]{:S(2)}, u32[]{:S(2)}) collective-permute-start(bf16[128,512]{1,0:T(8,128)(2,1)S(1)} %copy-done.4), channel_id=1, source_target_pairs={{0,1},{1,2},{2,3},{3,0},{4,5},{5,6},{6,7},{7,4},{8,9},{9,10},{10,1... | collective-permute-start | bytes 393224 | tf_op jit(solution)/shard_map/ppermute | solution.py:389
  75.2 8.8 %collective-permute-start.4 = (bf16[128,512]{1,0:T(8,128)(2,1)S(1)}, bf16[128,512]{1,0:T(8,128)(2,1)S(1)}, u32[]{:S(2)}, u32[]{:S(2)}) collective-permute-start(bf16[128,512]{1,0:T(8,128)(2,1)S(1)} %copy-done.3), channel_id=1, source_target_pairs={{0,3},{1,0},{2,1},{3,2},{4,7},{5,4},{6,5},{7,6},{8,11},{9,8},{10,9... | collective-permute-start | bytes 393224 | tf_op jit(solution)/shard_map/ppermute | solution.py:389

commit v6 on v5

--- a/solution.py
+++ b/solution.py
@@ -60,17 +60,28 @@
 
 
 def dispatch_table(
-    ids_ref, weight_ref, tokens_ref, out_ref, weight_near_ref, tokens_near_ref, ids_near_ref, done
+    member_ref,
+    ids_ref,
+    weight_ref,
+    tokens_ref,
+    gain_ref,
+    out_ref,
+    weight_near_ref,
+    tokens_near_ref,
+    gain_near_ref,
+    ids_near_ref,
+    done,
 ):
+    quarter = gain_near_ref.shape[1]
+    own = pl.multiple_of(member_ref[0] * quarter, quarter)
+    pairs = [
+        (ids_ref, ids_near_ref),
+        (weight_ref, weight_near_ref),
+        (tokens_ref, tokens_near_ref),
+        (gain_ref.at[:, pl.ds(own, quarter)], gain_near_ref),
+    ]
     copies = [
-        pltpu.make_async_copy(source, into, done.at[j])
-        for j, (source, into) in enumerate(
-            [
-                (ids_ref, ids_near_ref),
-                (weight_ref, weight_near_ref),
-                (tokens_ref, tokens_near_ref),
-            ]
-        )
+        pltpu.make_async_copy(source, into, done.at[j]) for j, (source, into) in enumerate(pairs)
     ]
     for copy in copies:
         copy.start()
@@ -80,35 +91,13 @@
         copy.wait()
 
 
-def combine_tables(
-    member_ref,
-    ids_ref,
-    logits_ref,
-    group_ref,
-    piece_ref,
-    gain_ref,
-    high_ref,
-    low_ref,
-    piece_near_ref,
-    gain_near_ref,
-    done,
-):
-    quarter = gain_near_ref.shape[1]
-    own = pl.multiple_of(member_ref[0] * quarter, quarter)
-    copies = [
-        pltpu.make_async_copy(piece_ref, piece_near_ref, done.at[0]),
-        pltpu.make_async_copy(gain_ref.at[:, pl.ds(own, quarter)], gain_near_ref, done.at[1]),
-    ]
-    for copy in copies:
-        copy.start()
+def combine_tables(ids_ref, logits_ref, group_ref, high_ref, low_ref):
     hit, first = places(ids_ref, high_ref.shape[0])
     raised = jnp.exp(logits_ref[...])
     weight = group_ref[...] * raised / (raised[0:1] + raised[1:2])
     high, low = halves(hit * jnp.where(first, weight[0:1], weight[1:2]))
     high_ref[...] = high
     low_ref[...] = low
-    for copy in copies:
-        copy.wait()
 
 
 def cut_weights(member_ref, gate_ref, up_ref, down_ref, *refs, members):
@@ -355,23 +344,24 @@
     operands = [near(value) for value in loaded[len(cuts) :]]
     table = pltpu.VMEM((slots, seq_count), BF16)
     ids = route_ids.T
-    dispatch, output_near, tokens_near = pl.pallas_call(
+    dispatch, output_near, tokens_near, gain_part = pl.pallas_call(
         dispatch_table,
-        out_shape=[table, pltpu.VMEM(output_weight.shape, BF16), pltpu.VMEM(tokens.shape, BF16)],
-        in_specs=[anywhere] * 3,
-        out_specs=[VMEM] * 3,
+        out_shape=[
+            table,
+            pltpu.VMEM(output_weight.shape, BF16),
+            pltpu.VMEM(tokens.shape, BF16),
+            pltpu.VMEM((1, quarter), F32),
+        ],
+        in_specs=[SMEM] + [anywhere] * 4,
+        out_specs=[VMEM] * 4,
         scratch_shapes=[
             pltpu.VMEM(ids.shape, ids.dtype),
-            pltpu.SemaphoreType.DMA((3,)),
+            pltpu.SemaphoreType.DMA((4,)),
         ],
-    )(ids, output_weight, tokens)
-    combine_high, combine_low, own, gain_part = pl.pallas_call(
-        combine_tables,
-        out_shape=[table, table, pltpu.VMEM(whole, BF16), pltpu.VMEM((1, quarter), F32)],
-        in_specs=[SMEM] + [VMEM] * 3 + [anywhere] * 2,
-        out_specs=[VMEM] * 4,
-        scratch_shapes=[pltpu.SemaphoreType.DMA((2,))],
-    )(place, ids, route_logits.T, group_weight[None], own, moe_gain[None])
+    )(place, ids, output_weight, tokens, moe_gain[None])
+    combine_high, combine_low = call(
+        combine_tables, [table] * 2, ids, route_logits.T, group_weight[None]
+    )
     copies, new_state, window = call(
         mixer,
         [

time: 132 us -> 133 us (level)
  blocking collectives: 45.9 us -> 8.03 us
  waiting for transfers between devices: 22.2 us -> 45.4 us
  starting transfers between devices: 48.6 us -> 64.3 us
    all_to_all x1 -> x0, blocking collectives: 37.8 us -> none  [body(): returned = lax.all_to_all(answer, 'ep', 0, 0, tiled=True)]
    all_to_all x0 -> x1, waiting for transfers between devices: none -> 21.7 us  [body(): returned = lax.all_to_all(answer, 'ep', 0, 0, tiled=True)]
    all_to_all x0 -> x1, starting transfers between devices: none -> 15.6 us  [body(): returned = lax.all_to_all(answer, 'ep', 0, 0, tiled=True)]
    pallas_call x1 -> x0, Pallas kernels: 1.72 us -> none  [body(): pl.pallas_call(combine_tables, out_shape=[table, table, pltpu.VMEM(whole,...]
    all_to_all x1, waiting for transfers between devices: 11.8 us -> 13.3 us  [body(): arrived = lax.all_to_all(outgoing, 'ep', 0, 0, tiled=True)]
    pallas_call x5 -> x6, Pallas kernels: 3.92 us -> 4.78 us  [call(): pl.pallas_call(kernel, out_shape=outs, in_specs=[SMEM] * len(scalars) + [...]
  transfers between devices with their start and end apart: 9 -> 10, of which waited for: 5 -> 6; matrix products, arithmetic and copies ran while one was open for 0% -> 0% of each run, Pallas kernels for 5% -> 4%
where the time goes in v6:
time: 133 us; the launch traced here: 132 us
  starting transfers between devices  64.3 us (48%)
  waiting for transfers between devices  45.4 us (34%)
  Pallas kernels  9.52 us (7%)
  blocking collectives  8.03 us (6%)
  local copies, waits for them, and re-layouts  3.32 us (2%)
    all_to_all x1, starting transfers between devices, body(): arrived = lax.all_to_all(outgoing, 'ep', 0, 0, tiled=True)  22 us
    all_to_all x1, waiting for transfers between devices, body(): returned = lax.all_to_all(answer, 'ep', 0, 0, tiled=True)  21.7 us
    ppermute x5, starting transfers between devices, onward(): return lax.ppermute(value, 'tp', ring)  15.7 us
    all_to_all x1, starting transfers between devices, body(): returned = lax.all_to_all(answer, 'ep', 0, 0, tiled=True)  15.6 us
    all_to_all x1, waiting for transfers between devices, body(): arrived = lax.all_to_all(outgoing, 'ep', 0, 0, tiled=True)  13.3 us
    all_to_all x1, blocking collectives, body(): hidden = lax.all_to_all(hidden, 'tp', 0, 0, tiled=True)  8.03 us
    pallas_call x6, Pallas kernels, call(): pl.pallas_call(kernel, out_shape=outs, in_specs=[SMEM] * len(scalars) + [...  4.78 us
    all_to_all x1, starting transfers between devices, body(): lax.all_to_all(jnp.broadcast_to(tokens[None], (members, *tokens.shape)),...  4.18 us
  transfers between devices with their start and end apart: 10, of which 6 were waited for; matrix products, arithmetic and copies ran while one was open for 0% of the time, Pallas kernels for 4%

profile of v6, /device:TPU:33, one launch (start us, length us, event | category | flops | bytes accessed | tf_op | source)
XLA Modules:
  0.0 132.5 jit_solution(11191011740381600612)
XLA Ops:
  0.6 1.5 %broadcast_in_dim.30 = bf16[4,48,512]{2,1,0:T(8,128)(2,1)} broadcast(bf16[48,512]{1,0:T(8,128)(2,1)} %tokens_ref.1), dimensions={1,2} | broadcast | bytes 245760 | tf_op jit(solution)/shard_map/broadcast_in_dim | solution.py:310
  2.1 4.2 %all-to-all-start = ((bf16[4,48,512]{2,1,0:T(8,128)(2,1)}), bf16[4,48,512]{2,1,0:T(8,128)(2,1)S(1)}, u32[]{:S(2)}, u32[]{:S(2)}) async-start(bf16[4,48,512]{2,1,0:T(8,128)(2,1)} %broadcast_in_dim.30), calls=%async_computation | async-start | bytes 393216 | tf_op jit(solution)/shard_map/all_to_all | solution.py:309
  6.3 3.5 %shard_map.220 = (bf16[384,512]{1,0:T(8,128)(2,1)}, bf16[384,512]{1,0:T(8,128)(2,1)}, bf16[256,512]{1,0:T(8,128)(2,1)}, bf16[128,512]{1,0:T(8,128)(2,1)}, bf16[2...) custom-call(s32[1]{0:T(128)} %bitcast.member_ref, ...), custom_call_target="tpu_custom_call" | custom-call | tf_op jit(solution)/shard_map/pallas_call | solution.py:342
  9.8 1.7 %all-to-all-done.parts_ref = bf16[4,48,512]{2,1,0:T(8,128)(2,1)S(1)} async-done(((bf16[4,48,512]{2,1,0:T(8,128)(2,1)}), bf16[4,48,512]{2,1,0:T(8,128)(2,1)S(1)}, u32[]{:S(2)}, u32[]{:S(2)}) %all-to-all-start) | async-done | bytes 196640 | tf_op jit(solution)/shard_map/all_to_all | solution.py:309
  11.5 1.4 %shard_map.221 = (bf16[4,48,256]{2,1,0:T(8,128)(2,1)}, f32[48,256]{1,0:T(8,128)}, bf16[3,48,256]{2,1,0:T(8,128)(2,1)}) custom-call(bf16[4,48,512]{2,1,0:T(8,128)(2,1)S(1)} %all-to-all-done.parts_ref, f32[1,2048]{1,0:T(1,128)S(1)} %get-tuple-element.35.gain_ref, bf16[2048,256]{1,0:T(8,128)(2,1)S(1)} %get-tuple-element.36.input_ref, ...), custom_call_target="tpu_custom_call" | custom-call | tf_op jit(solution)/shard_map/pallas_call | solution.py:26
  12.9 3.3 %all-to-all-start.1 = ((bf16[4,48,256]{2,1,0:T(8,128)(2,1)}), bf16[4,48,256]{2,1,0:T(8,128)(2,1)S(1)}, u32[]{:S(2)}, u32[]{:S(2)}) async-start(bf16[4,48,256]{2,1,0:T(8,128)(2,1)} %get-tuple-element.47), calls=%async_computation.1 | async-start | bytes 196608 | tf_op jit(solution)/shard_map/all_to_all | solution.py:375
  16.2 1.3 shard_map.222
  17.5 3.3 %all-to-all-done.1.parts_ref = bf16[4,48,256]{2,1,0:T(8,128)(2,1)S(1)} async-done(((bf16[4,48,256]{2,1,0:T(8,128)(2,1)}), bf16[4,48,256]{2,1,0:T(8,128)(2,1)S(1)}, u32[]{:S(2)}, u32[]{:S(2)}) %all-to-all-start.1) | async-done | bytes 98336 | tf_op jit(solution)/shard_map/all_to_all | solution.py:375
  20.8 0.5 shard_map.223
  21.3 0.0 copy-start.3
  21.3 0.0 copy-start.2
  21.3 0.8 reshape.15
  22.1 0.0 copy-start.1
  22.1 22.0 %all-to-all-start.2 = ((bf16[128,2,512]{2,1,0:T(2,128)(2,1)}), bf16[128,2,512]{2,1,0:T(2,128)(2,1)S(1)}, u32[]{:S(2)}, u32[]{:S(2)}) async-start(bf16[128,2,512]{2,1,0:T(2,128)(2,1)} %reshape.15), calls=%async_computation.2 | async-start | bytes 524288 | tf_op jit(solution)/shard_map/all_to_all | solution.py:396
  44.1 0.0 copy-start
  44.1 0.0 copy-done.1
  44.1 2.7 %collective-permute-start.1 = (bf16[384,512]{1,0:T(8,128)(2,1)S(1)}, bf16[384,512]{1,0:T(8,128)(2,1)S(1)}, u32[]{:S(2)}, u32[]{:S(2)}) collective-permute-start(bf16[384,512]{1,0:T(8,128)(2,1)S(1)} %copy-done.1), channel_id=1, source_target_pairs={{0,2},{1,3},{2,0},{3,1},{4,6},{5,7},{6,4},{7,5},{8,10},{9,11},{10,... | collective-permute-start | bytes 1179656 | tf_op jit(solution)/shard_map/ppermute | solution.py:379
  46.8 0.0 copy-done.3
  46.8 2.7 %collective-permute-start = (bf16[256,512]{1,0:T(8,128)(2,1)S(1)}, bf16[256,512]{1,0:T(8,128)(2,1)S(1)}, u32[]{:S(2)}, u32[]{:S(2)}) collective-permute-start(bf16[256,512]{1,0:T(8,128)(2,1)S(1)} %copy-done.3), channel_id=1, source_target_pairs={{0,1},{1,2},{2,3},{3,0},{4,5},{5,6},{6,7},{7,4},{8,9},{9,10},{10,1... | collective-permute-start | bytes 786440 | tf_op jit(solution)/shard_map/ppermute | solution.py:379
  49.6 0.0 copy-done.2
  49.6 3.7 %collective-permute-start.2 = (bf16[256,512]{1,0:T(8,128)(2,1)S(1)}, bf16[256,512]{1,0:T(8,128)(2,1)S(1)}, u32[]{:S(2)}, u32[]{:S(2)}) collective-permute-start(bf16[256,512]{1,0:T(8,128)(2,1)S(1)} %copy-done.2), channel_id=1, source_target_pairs={{0,3},{1,0},{2,1},{3,2},{4,7},{5,4},{6,5},{7,6},{8,11},{9,8},{10,9... | collective-permute-start | bytes 786440 | tf_op jit(solution)/shard_map/ppermute | solution.py:379
  53.4 13.3 %all-to-all-done.2 = bf16[128,2,512]{2,1,0:T(2,128)(2,1)S(1)} async-done(((bf16[128,2,512]{2,1,0:T(2,128)(2,1)}), bf16[128,2,512]{2,1,0:T(2,128)(2,1)S(1)}, u32[]{:S(2)}, u32[]{:S(2)}) %all-to-all-start.2) | async-done | bytes 262176 | tf_op jit(solution)/shard_map/all_to_all | solution.py:396
  66.7 0.1 reshape.16.rows_ref
  66.8 0.0 collective-permute-done.refs_1_
  66.8 0.0 collective-permute-done.2.refs_3_
  66.8 0.0 collective-permute-done.1.refs_2_
  66.8 0.0 copy-done
  66.8 1.4 %shard_map.225 = bf16[4,272,256]{2,1,0:T(8,128)(2,1)} custom-call(s32[1]{0:T(128)} %bitcast.member_ref, bf16[256,512]{1,0:T(8,128)(2,1)S(1)} %reshape.16.rows_ref, f32[1,512]{1,0:T(1,128)S(1)} %get-tuple-element.54.gain_ref, bf16[384,512]{1,0:T(8,128)(2,1)S(1)} %copy-done, bf16[256,512]{1,0:T(8,128)(2,1)S(1)} %collective-permute-done.refs_1_, ...), custom_call_target="tpu_custom_call" | custom-call | tf_op jit(solution)/shard_map/pallas_call | solution.py:26
  68.2 0.0 copy-start.5
  68.2 0.0 copy-start.4
  68.2 3.6 %all-to-all-start.3 = ((bf16[4,272,256]{2,1,0:T(8,128)(2,1)}), bf16[4,272,256]{2,1,0:T(8,128)(2,1)S(1)}, u32[]{:S(2)}, u32[]{:S(2)}) async-start(bf16[4,272,256]{2,1,0:T(8,128)(2,1)} %shard_map.225), calls=%async_computation.3 | async-start | bytes 1114112 | tf_op jit(solution)/shard_map/all_to_all | solution.py:410
  71.9 0.0 copy-done.5
  71.9 3.3 %collective-permute-start.3 = (bf16[128,512]{1,0:T(8,128)(2,1)S(1)}, bf16[128,512]{1,0:T(8,128)(2,1)S(1)}, u32[]{:S(2)}, u32[]{:S(2)}) collective-permute-start(bf16[128,512]{1,0:T(8,128)(2,1)S(1)} %copy-done.5), channel_id=1, source_target_pairs={{0,1},{1,2},{2,3},{3,0},{4,5},{5,6},{6,7},{7,4},{8,9},{9,10},{10,1... | collective-permute-start | bytes 393224 | tf_op jit(solution)/shard_map/ppermute | solution.py:379
  75.2 0.0 copy-done.4
  75.2 3.2 %collective-permute-start.4 = (bf16[128,512]{1,0:T(8,128)(2,1)S(1)}, bf16[128,512]{1,0:T(8,128)(2,1)S(1)}, u32[]{:S(2)}, u32[]{:S(2)}) collective-permute-start(bf16[128,512]{1,0:T(8,128)(2,1)S(1)} %copy-done.4), channel_id=1, source_target_pairs={{0,3},{1,0},{2,1},{3,2},{4,7},{5,4},{6,5},{7,6},{8,11},{9,8},{10,9... | collective-permute-start | bytes 393224 | tf_op jit(solution)/shard_map/ppermute | solution.py:379
  78.4 3.1 %all-to-all-done.3.parts_ref = bf16[4,272,256]{2,1,0:T(8,128)(2,1)S(1)} async-done(((bf16[4,272,256]{2,1,0:T(8,128)(2,1)}), bf16[4,272,256]{2,1,0:T(8,128)(2,1)S(1)}, u32[]{:S(2)}, u32[]{:S(2)}) %all-to-all-start.3) | async-done | bytes 557088 | tf_op jit(solution)/shard_map/all_to_all | solution.py:410
  81.5 0.2 shard_map.226
  81.7 2.2 %collective-permute-done.3.refs_1_ = bf16[128,512]{1,0:T(8,128)(2,1)S(1)} collective-permute-done((bf16[128,512]{1,0:T(8,128)(2,1)S(1)}, bf16[128,512]{1,0:T(8,128)(2,1)S(1)}, u32[]{:S(2)}, u32[]{:S(2)}) %collective-permute-start.3) | collective-permute-done | bytes 131104 | tf_op jit(solution)/shard_map/ppermute | solution.py:379
  84.0 0.0 collective-permute-done.4.refs_3_
  84.0 8.0 %all_to_all.37.hidden_ref = bf16[4,256,128]{2,1,0:T(8,128)(2,1)S(1)} all-to-all(bf16[4,256,128]{2,1,0:T(8,128)(2,1)S(1)} %shard_map.226), channel_id=1, replica_groups=mesh['ep'=128,'tp'=4] {'tp'}, dimensions={0} | all-to-all | bytes 524288 | tf_op jit(solution)/shard_map/all_to_all | solution.py:413
  92.0 0.4 shard_map.227
  92.4 0.8 all_to_all.28
  93.2 15.6 %all-to-all-start.5 = ((bf16[128,2,512]{2,1,0:T(2,128)(2,1)}), bf16[128,2,512]{2,1,0:T(2,128)(2,1)S(1)}, u32[]{:S(2)}, u32[]{:S(2)}) async-start(bf16[128,2,512]{2,1,0:T(2,128)(2,1)} %all_to_all.28), calls=%async_computation.5 | async-start | bytes 524288 | tf_op jit(solution)/shard_map/all_to_all | solution.py:424
  108.8 0.9 shard_map.224
  109.7 21.7 %all-to-all-done.5 = bf16[128,2,512]{2,1,0:T(2,128)(2,1)S(1)} async-done(((bf16[128,2,512]{2,1,0:T(2,128)(2,1)}), bf16[128,2,512]{2,1,0:T(2,128)(2,1)S(1)}, u32[]{:S(2)}, u32[]{:S(2)}) %all-to-all-start.5) | async-done | bytes 262176 | tf_op jit(solution)/shard_map/all_to_all | solution.py:424
  131.4 0.1 all_to_all.30
  131.5 0.2 fusion.2
  131.6 0.8 fusion.1
Async XLA Ops:
  2.1 9.4 %all-to-all-start = ((bf16[4,48,512]{2,1,0:T(8,128)(2,1)}), bf16[4,48,512]{2,1,0:T(8,128)(2,1)S(1)}, u32[]{:S(2)}, u32[]{:S(2)}) async-start(bf16[4,48,512]{2,1,0:T(8,128)(2,1)} %broadcast_in_dim.30), calls=%async_computation | async-start | bytes 393216 | tf_op jit(solution)/shard_map/all_to_all | solution.py:309
  12.9 7.9 %all-to-all-start.1 = ((bf16[4,48,256]{2,1,0:T(8,128)(2,1)}), bf16[4,48,256]{2,1,0:T(8,128)(2,1)S(1)}, u32[]{:S(2)}, u32[]{:S(2)}) async-start(bf16[4,48,256]{2,1,0:T(8,128)(2,1)} %get-tuple-element.47), calls=%async_computation.1 | async-start | bytes 196608 | tf_op jit(solution)/shard_map/all_to_all | solution.py:375
  21.3 25.5 %copy-start.3 = (bf16[256,512]{1,0:T(8,128)(2,1)S(1)}, bf16[256,512]{1,0:T(8,128)(2,1)}, u32[]{:S(2)}) copy-start(bf16[256,512]{1,0:T(8,128)(2,1)} %get-tuple-element.56) | copy-start | bytes 786436
  21.3 28.3 %copy-start.2 = (bf16[256,512]{1,0:T(8,128)(2,1)S(1)}, bf16[256,512]{1,0:T(8,128)(2,1)}, u32[]{:S(2)}) copy-start(bf16[256,512]{1,0:T(8,128)(2,1)} %get-tuple-element.58) | copy-start | bytes 786436
  22.1 22.0 %copy-start.1 = (bf16[384,512]{1,0:T(8,128)(2,1)S(1)}, bf16[384,512]{1,0:T(8,128)(2,1)}, u32[]{:S(2)}) copy-start(bf16[384,512]{1,0:T(8,128)(2,1)} %get-tuple-element.57) | copy-start | bytes 1179652
  22.1 44.6 %all-to-all-start.2 = ((bf16[128,2,512]{2,1,0:T(2,128)(2,1)}), bf16[128,2,512]{2,1,0:T(2,128)(2,1)S(1)}, u32[]{:S(2)}, u32[]{:S(2)}) async-start(bf16[128,2,512]{2,1,0:T(2,128)(2,1)} %reshape.15), calls=%async_computation.2 | async-start | bytes 524288 | tf_op jit(solution)/shard_map/all_to_all | solution.py:396
  44.1 22.7 %copy-start = (bf16[384,512]{1,0:T(8,128)(2,1)S(1)}, bf16[384,512]{1,0:T(8,128)(2,1)}, u32[]{:S(2)}) copy-start(bf16[384,512]{1,0:T(8,128)(2,1)} %get-tuple-element.55.refs_0_) | copy-start | bytes 1179652
  44.1 22.7 %collective-permute-start.1 = (bf16[384,512]{1,0:T(8,128)(2,1)S(1)}, bf16[384,512]{1,0:T(8,128)(2,1)S(1)}, u32[]{:S(2)}, u32[]{:S(2)}) collective-permute-start(bf16[384,512]{1,0:T(8,128)(2,1)S(1)} %copy-done.1), channel_id=1, source_target_pairs={{0,2},{1,3},{2,0},{3,1},{4,6},{5,7},{6,4},{7,5},{8,10},{9,11},{10,... | collective-permute-start | bytes 1179656 | tf_op jit(solution)/shard_map/ppermute | solution.py:379
  46.8 20.0 %collective-permute-start = (bf16[256,512]{1,0:T(8,128)(2,1)S(1)}, bf16[256,512]{1,0:T(8,128)(2,1)S(1)}, u32[]{:S(2)}, u32[]{:S(2)}) collective-permute-start(bf16[256,512]{1,0:T(8,128)(2,1)S(1)} %copy-done.3), channel_id=1, source_target_pairs={{0,1},{1,2},{2,3},{3,0},{4,5},{5,6},{6,7},{7,4},{8,9},{9,10},{10,1... | collective-permute-start | bytes 786440 | tf_op jit(solution)/shard_map/ppermute | solution.py:379
  49.6 17.2 %collective-permute-start.2 = (bf16[256,512]{1,0:T(8,128)(2,1)S(1)}, bf16[256,512]{1,0:T(8,128)(2,1)S(1)}, u32[]{:S(2)}, u32[]{:S(2)}) collective-permute-start(bf16[256,512]{1,0:T(8,128)(2,1)S(1)} %copy-done.2), channel_id=1, source_target_pairs={{0,3},{1,0},{2,1},{3,2},{4,7},{5,4},{6,5},{7,6},{8,11},{9,8},{10,9... | collective-permute-start | bytes 786440 | tf_op jit(solution)/shard_map/ppermute | solution.py:379
  68.2 3.6 %copy-start.5 = (bf16[128,512]{1,0:T(8,128)(2,1)S(1)}, bf16[128,512]{1,0:T(8,128)(2,1)}, u32[]{:S(2)}) copy-start(bf16[128,512]{1,0:T(8,128)(2,1)} %get-tuple-element.59) | copy-start | bytes 393220
  68.2 6.9 %copy-start.4 = (bf16[128,512]{1,0:T(8,128)(2,1)S(1)}, bf16[128,512]{1,0:T(8,128)(2,1)}, u32[]{:S(2)}) copy-start(bf16[128,512]{1,0:T(8,128)(2,1)} %get-tuple-element.60) | copy-start | bytes 393220
  68.2 13.2 %all-to-all-start.3 = ((bf16[4,272,256]{2,1,0:T(8,128)(2,1)}), bf16[4,272,256]{2,1,0:T(8,128)(2,1)S(1)}, u32[]{:S(2)}, u32[]{:S(2)}) async-start(bf16[4,272,256]{2,1,0:T(8,128)(2,1)} %shard_map.225), calls=%async_computation.3 | async-start | bytes 1114112 | tf_op jit(solution)/shard_map/all_to_all | solution.py:410
  71.9 12.1 %collective-permute-start.3 = (bf16[128,512]{1,0:T(8,128)(2,1)S(1)}, bf16[128,512]{1,0:T(8,128)(2,1)S(1)}, u32[]{:S(2)}, u32[]{:S(2)}) collective-permute-start(bf16[128,512]{1,0:T(8,128)(2,1)S(1)} %copy-done.5), channel_id=1, source_target_pairs={{0,1},{1,2},{2,3},{3,0},{4,5},{5,6},{6,7},{7,4},{8,9},{9,10},{10,1... | collective-permute-start | bytes 393224 | tf_op jit(solution)/shard_map/ppermute | solution.py:379
  75.2 8.8 %collective-permute-start.4 = (bf16[128,512]{1,0:T(8,128)(2,1)S(1)}, bf16[128,512]{1,0:T(8,128)(2,1)S(1)}, u32[]{:S(2)}, u32[]{:S(2)}) collective-permute-start(bf16[128,512]{1,0:T(8,128)(2,1)S(1)} %copy-done.4), channel_id=1, source_target_pairs={{0,3},{1,0},{2,1},{3,2},{4,7},{5,4},{6,5},{7,6},{8,11},{9,8},{10,9... | collective-permute-start | bytes 393224 | tf_op jit(solution)/shard_map/ppermute | solution.py:379
  93.2 38.2 %all-to-all-start.5 = ((bf16[128,2,512]{2,1,0:T(2,128)(2,1)}), bf16[128,2,512]{2,1,0:T(2,128)(2,1)S(1)}, u32[]{:S(2)}, u32[]{:S(2)}) async-start(bf16[128,2,512]{2,1,0:T(2,128)(2,1)} %all_to_all.28), calls=%async_computation.5 | async-start | bytes 524288 | tf_op jit(solution)/shard_map/all_to_all | solution.py:424

commit v7 on v6

--- a/solution.py
+++ b/solution.py
@@ -219,7 +219,7 @@
         mixed = mixed + dot(parts_ref[m], weight_ref[m * width : (m + 1) * width, :])
     stream = (tokens_ref[...].astype(F32) + mixed).astype(BF16)
     stream_ref[...] = stream
-    out_ref[...] = dot(dispatch_ref[...], stream).astype(BF16)
+    out_ref[...] = dot(dispatch_ref[...], stream).astype(BF16).reshape(out_ref.shape)
 
 
 def first_products(member_ref, rows_ref, gain_ref, *refs):
@@ -267,11 +267,17 @@
 def last_product(member_ref, hidden_ref, *refs):
     *weight_refs, out_ref = refs
     members, _, width = hidden_ref.shape
-    total = jnp.zeros(out_ref.shape, F32)
+    total = jnp.zeros((hidden_ref.shape[1], out_ref.shape[-1]), F32)
     for k, weight_ref in enumerate(weight_refs):
         owner = lax.rem(member_ref[0] + (members - k), members)
         total = total + dot(hidden_ref[owner], weight_ref[weight_ref.shape[0] - width :, :])
-    out_ref[...] = total.astype(BF16)
+    out_ref[...] = total.astype(BF16).reshape(out_ref.shape)
+
+
+def add_routed(back_ref, high_ref, low_ref, stream_ref, out_ref):
+    back = back_ref[...].reshape(high_ref.shape[0], -1)
+    routed = dot_on(high_ref[...], back, 0, 0) + dot_on(low_ref[...], back, 0, 0)
+    out_ref[...] = (stream_ref[...].astype(F32) + routed).astype(BF16)
 
 
 def body(
@@ -385,14 +391,16 @@
     down_last = onward(sides[3], 3)
     stream, outgoing = call(
         stream_rows,
-        [pltpu.VMEM((seq_count, quarter), BF16), pltpu.VMEM((slots, quarter), BF16)],
+        [
+            pltpu.VMEM((seq_count, quarter), BF16),
+            jax.ShapeDtypeStruct((experts, CAPACITY, quarter), BF16),
+        ],
         near(mixer_parts),
         near(output_near),
         near(tokens_near),
         near(dispatch),
     )
 
-    outgoing = outgoing.reshape(experts, CAPACITY, quarter)
     arrived = lax.all_to_all(outgoing, "ep", 0, 0, tiled=True)
     arrived = arrived.reshape(slots, quarter)
     own, across = near(own), near(across)
@@ -413,7 +421,7 @@
     hidden = lax.all_to_all(hidden, "tp", 0, 0, tiled=True)
     answer = call(
         last_product,
-        pltpu.VMEM((slots, quarter), BF16),
+        pltpu.VMEM((experts, CAPACITY, quarter), BF16),
         near(hidden),
         own,
         near(down_next),
@@ -422,8 +430,14 @@
         scalar=place,
     )
     returned = lax.all_to_all(answer, "ep", 0, 0, tiled=True)
-    routed = dot_on(combine_high, returned, 0, 0) + dot_on(combine_low, returned, 0, 0)
-    result = (stream.astype(F32) + routed).astype(BF16)
+    result = call(
+        add_routed,
+        jax.ShapeDtypeStruct((seq_count, quarter), BF16),
+        near(returned),
+        near(combine_high),
+        near(combine_low),
+        near(stream),
+    )
     return (result, new_state, jnp.swapaxes(window, 0, 1))
 
 

time: 133 us -> 133 us (level)
  Pallas kernels: 9.52 us -> 11.8 us
  local copies, waits for them, and re-layouts: 3.32 us -> 1.62 us
    pallas_call x6 -> x7, Pallas kernels: 4.78 us -> 7.04 us  [call(): pl.pallas_call(kernel, out_shape=outs, in_specs=[SMEM] * len(scalars) + [...]
where the time goes in v7:
time: 133 us; the launch traced here: 132 us
  starting transfers between devices  64.3 us (48%)
  waiting for transfers between devices  45.4 us (34%)
  Pallas kernels  11.8 us (9%)
  blocking collectives  8.03 us (6%)
  local copies, waits for them, and re-layouts  1.62 us (1%)
    all_to_all x1, starting transfers between devices, body(): arrived = lax.all_to_all(outgoing, 'ep', 0, 0, tiled=True)  22 us
    all_to_all x1, waiting for transfers between devices, body(): returned = lax.all_to_all(answer, 'ep', 0, 0, tiled=True)  21.7 us
    ppermute x5, starting transfers between devices, onward(): return lax.ppermute(value, 'tp', ring)  15.6 us
    all_to_all x1, starting transfers between devices, body(): returned = lax.all_to_all(answer, 'ep', 0, 0, tiled=True)  15.6 us
    all_to_all x1, waiting for transfers between devices, body(): arrived = lax.all_to_all(outgoing, 'ep', 0, 0, tiled=True)  13.4 us
    all_to_all x1, blocking collectives, body(): hidden = lax.all_to_all(hidden, 'tp', 0, 0, tiled=True)  8.03 us
    pallas_call x7, Pallas kernels, call(): pl.pallas_call(kernel, out_shape=outs, in_specs=[SMEM] * len(scalars) + [...  7.04 us
    all_to_all x1, starting transfers between devices, body(): lax.all_to_all(jnp.broadcast_to(tokens[None], (members, *tokens.shape)),...  4.18 us
  transfers between devices with their start and end apart: 10, of which 6 were waited for; matrix products, arithmetic and copies ran while one was open for 0% of the time, Pallas kernels for 4%

profile of v7, /device:TPU:33, one launch (start us, length us, event | category | flops | bytes accessed | tf_op | source)
XLA Modules:
  0.0 132.0 jit_solution(18363467098878848957)
XLA Ops:
  0.6 1.5 %broadcast_in_dim.31 = bf16[4,48,512]{2,1,0:T(8,128)(2,1)} broadcast(bf16[48,512]{1,0:T(8,128)(2,1)} %tokens_ref.1), dimensions={1,2} | broadcast | bytes 245760 | tf_op jit(solution)/shard_map/broadcast_in_dim | solution.py:316
  2.1 4.2 %all-to-all-start = ((bf16[4,48,512]{2,1,0:T(8,128)(2,1)}), bf16[4,48,512]{2,1,0:T(8,128)(2,1)S(1)}, u32[]{:S(2)}, u32[]{:S(2)}) async-start(bf16[4,48,512]{2,1,0:T(8,128)(2,1)} %broadcast_in_dim.31), calls=%async_computation | async-start | bytes 393216 | tf_op jit(solution)/shard_map/all_to_all | solution.py:315
  6.3 3.5 %shard_map.220 = (bf16[384,512]{1,0:T(8,128)(2,1)}, bf16[384,512]{1,0:T(8,128)(2,1)}, bf16[256,512]{1,0:T(8,128)(2,1)}, bf16[128,512]{1,0:T(8,128)(2,1)}, bf16[2...) custom-call(s32[1]{0:T(128)} %bitcast.member_ref, ...), custom_call_target="tpu_custom_call" | custom-call | tf_op jit(solution)/shard_map/pallas_call | solution.py:348
  9.8 1.7 %all-to-all-done.parts_ref = bf16[4,48,512]{2,1,0:T(8,128)(2,1)S(1)} async-done(((bf16[4,48,512]{2,1,0:T(8,128)(2,1)}), bf16[4,48,512]{2,1,0:T(8,128)(2,1)S(1)}, u32[]{:S(2)}, u32[]{:S(2)}) %all-to-all-start) | async-done | bytes 196640 | tf_op jit(solution)/shard_map/all_to_all | solution.py:315
  11.5 1.4 %shard_map.221 = (bf16[4,48,256]{2,1,0:T(8,128)(2,1)}, f32[48,256]{1,0:T(8,128)}, bf16[3,48,256]{2,1,0:T(8,128)(2,1)}) custom-call(bf16[4,48,512]{2,1,0:T(8,128)(2,1)S(1)} %all-to-all-done.parts_ref, f32[1,2048]{1,0:T(1,128)S(1)} %get-tuple-element.35.gain_ref, bf16[2048,256]{1,0:T(8,128)(2,1)S(1)} %get-tuple-element.36.input_ref, ...), custom_call_target="tpu_custom_call" | custom-call | tf_op jit(solution)/shard_map/pallas_call | solution.py:26
  12.9 3.3 %all-to-all-start.1 = ((bf16[4,48,256]{2,1,0:T(8,128)(2,1)}), bf16[4,48,256]{2,1,0:T(8,128)(2,1)S(1)}, u32[]{:S(2)}, u32[]{:S(2)}) async-start(bf16[4,48,256]{2,1,0:T(8,128)(2,1)} %get-tuple-element.47), calls=%async_computation.1 | async-start | bytes 196608 | tf_op jit(solution)/shard_map/all_to_all | solution.py:381
  16.2 1.3 shard_map.222
  17.5 3.3 %all-to-all-done.1.parts_ref = bf16[4,48,256]{2,1,0:T(8,128)(2,1)S(1)} async-done(((bf16[4,48,256]{2,1,0:T(8,128)(2,1)}), bf16[4,48,256]{2,1,0:T(8,128)(2,1)S(1)}, u32[]{:S(2)}, u32[]{:S(2)}) %all-to-all-start.1) | async-done | bytes 98336 | tf_op jit(solution)/shard_map/all_to_all | solution.py:381
  20.8 0.0 copy-start.3
  20.8 0.0 copy-start.2
  20.8 1.2 shard_map.223
  22.0 0.0 copy-start.1
  22.0 22.0 %all-to-all-start.2 = ((bf16[128,2,512]{2,1,0:T(2,128)(2,1)}), bf16[128,2,512]{2,1,0:T(2,128)(2,1)S(1)}, u32[]{:S(2)}, u32[]{:S(2)}) async-start(bf16[128,2,512]{2,1,0:T(2,128)(2,1)} %get-tuple-element.51), calls=%async_computation.2 | async-start | bytes 524288 | tf_op jit(solution)/shard_map/all_to_all | solution.py:404
  44.0 0.0 copy-start
  44.0 0.0 copy-done.1
  44.0 2.7 %collective-permute-start.1 = (bf16[384,512]{1,0:T(8,128)(2,1)S(1)}, bf16[384,512]{1,0:T(8,128)(2,1)S(1)}, u32[]{:S(2)}, u32[]{:S(2)}) collective-permute-start(bf16[384,512]{1,0:T(8,128)(2,1)S(1)} %copy-done.1), channel_id=1, source_target_pairs={{0,2},{1,3},{2,0},{3,1},{4,6},{5,7},{6,4},{7,5},{8,10},{9,11},{10,... | collective-permute-start | bytes 1179656 | tf_op jit(solution)/shard_map/ppermute | solution.py:385
  46.7 0.0 copy-done.3
  46.7 2.7 %collective-permute-start = (bf16[256,512]{1,0:T(8,128)(2,1)S(1)}, bf16[256,512]{1,0:T(8,128)(2,1)S(1)}, u32[]{:S(2)}, u32[]{:S(2)}) collective-permute-start(bf16[256,512]{1,0:T(8,128)(2,1)S(1)} %copy-done.3), channel_id=1, source_target_pairs={{0,1},{1,2},{2,3},{3,0},{4,5},{5,6},{6,7},{7,4},{8,9},{9,10},{10,1... | collective-permute-start | bytes 786440 | tf_op jit(solution)/shard_map/ppermute | solution.py:385
  49.5 0.0 copy-done.2
  49.5 3.7 %collective-permute-start.2 = (bf16[256,512]{1,0:T(8,128)(2,1)S(1)}, bf16[256,512]{1,0:T(8,128)(2,1)S(1)}, u32[]{:S(2)}, u32[]{:S(2)}) collective-permute-start(bf16[256,512]{1,0:T(8,128)(2,1)S(1)} %copy-done.2), channel_id=1, source_target_pairs={{0,3},{1,0},{2,1},{3,2},{4,7},{5,4},{6,5},{7,6},{8,11},{9,8},{10,9... | collective-permute-start | bytes 786440 | tf_op jit(solution)/shard_map/ppermute | solution.py:385
  53.2 13.4 %all-to-all-done.2 = bf16[128,2,512]{2,1,0:T(2,128)(2,1)S(1)} async-done(((bf16[128,2,512]{2,1,0:T(2,128)(2,1)}), bf16[128,2,512]{2,1,0:T(2,128)(2,1)S(1)}, u32[]{:S(2)}, u32[]{:S(2)}) %all-to-all-start.2) | async-done | bytes 262176 | tf_op jit(solution)/shard_map/all_to_all | solution.py:404
  66.6 0.1 reshape.10.rows_ref
  66.7 0.0 collective-permute-done.refs_1_
  66.7 0.0 collective-permute-done.2.refs_3_
  66.7 0.0 collective-permute-done.1.refs_2_
  66.7 0.0 copy-done
  66.7 1.4 %shard_map.224 = bf16[4,272,256]{2,1,0:T(8,128)(2,1)} custom-call(s32[1]{0:T(128)} %bitcast.member_ref, bf16[256,512]{1,0:T(8,128)(2,1)S(1)} %reshape.10.rows_ref, f32[1,512]{1,0:T(1,128)S(1)} %get-tuple-element.52.gain_ref, bf16[384,512]{1,0:T(8,128)(2,1)S(1)} %copy-done, bf16[256,512]{1,0:T(8,128)(2,1)S(1)} %collective-permute-done.refs_1_, ...), custom_call_target="tpu_custom_call" | custom-call | tf_op jit(solution)/shard_map/pallas_call | solution.py:26
  68.1 0.0 copy-start.5
  68.1 0.0 copy-start.4
  68.1 3.6 %all-to-all-start.3 = ((bf16[4,272,256]{2,1,0:T(8,128)(2,1)}), bf16[4,272,256]{2,1,0:T(8,128)(2,1)S(1)}, u32[]{:S(2)}, u32[]{:S(2)}) async-start(bf16[4,272,256]{2,1,0:T(8,128)(2,1)} %shard_map.224), calls=%async_computation.3 | async-start | bytes 1114112 | tf_op jit(solution)/shard_map/all_to_all | solution.py:418
  71.8 0.0 copy-done.5
  71.8 3.3 %collective-permute-start.3 = (bf16[128,512]{1,0:T(8,128)(2,1)S(1)}, bf16[128,512]{1,0:T(8,128)(2,1)S(1)}, u32[]{:S(2)}, u32[]{:S(2)}) collective-permute-start(bf16[128,512]{1,0:T(8,128)(2,1)S(1)} %copy-done.5), channel_id=1, source_target_pairs={{0,1},{1,2},{2,3},{3,0},{4,5},{5,6},{6,7},{7,4},{8,9},{9,10},{10,1... | collective-permute-start | bytes 393224 | tf_op jit(solution)/shard_map/ppermute | solution.py:385
  75.1 0.0 copy-done.4
  75.1 3.2 %collective-permute-start.4 = (bf16[128,512]{1,0:T(8,128)(2,1)S(1)}, bf16[128,512]{1,0:T(8,128)(2,1)S(1)}, u32[]{:S(2)}, u32[]{:S(2)}) collective-permute-start(bf16[128,512]{1,0:T(8,128)(2,1)S(1)} %copy-done.4), channel_id=1, source_target_pairs={{0,3},{1,0},{2,1},{3,2},{4,7},{5,4},{6,5},{7,6},{8,11},{9,8},{10,9... | collective-permute-start | bytes 393224 | tf_op jit(solution)/shard_map/ppermute | solution.py:385
  78.3 3.1 %all-to-all-done.3.parts_ref = bf16[4,272,256]{2,1,0:T(8,128)(2,1)S(1)} async-done(((bf16[4,272,256]{2,1,0:T(8,128)(2,1)}), bf16[4,272,256]{2,1,0:T(8,128)(2,1)S(1)}, u32[]{:S(2)}, u32[]{:S(2)}) %all-to-all-start.3) | async-done | bytes 557088 | tf_op jit(solution)/shard_map/all_to_all | solution.py:418
  81.4 0.2 shard_map.225
  81.6 2.2 %collective-permute-done.3.refs_1_ = bf16[128,512]{1,0:T(8,128)(2,1)S(1)} collective-permute-done((bf16[128,512]{1,0:T(8,128)(2,1)S(1)}, bf16[128,512]{1,0:T(8,128)(2,1)S(1)}, u32[]{:S(2)}, u32[]{:S(2)}) %collective-permute-start.3) | collective-permute-done | bytes 131104 | tf_op jit(solution)/shard_map/ppermute | solution.py:385
  83.8 0.0 collective-permute-done.4.refs_3_
  83.8 8.0 %all_to_all.30.hidden_ref = bf16[4,256,128]{2,1,0:T(8,128)(2,1)S(1)} all-to-all(bf16[4,256,128]{2,1,0:T(8,128)(2,1)S(1)} %shard_map.225), channel_id=1, replica_groups=mesh['ep'=128,'tp'=4] {'tp'}, dimensions={0} | all-to-all | bytes 524288 | tf_op jit(solution)/shard_map/all_to_all | solution.py:421
  91.9 1.1 shard_map.226
  93.0 15.6 %all-to-all-start.5 = ((bf16[128,2,512]{2,1,0:T(2,128)(2,1)}), bf16[128,2,512]{2,1,0:T(2,128)(2,1)S(1)}, u32[]{:S(2)}, u32[]{:S(2)}) async-start(bf16[128,2,512]{2,1,0:T(2,128)(2,1)} %shard_map.226), calls=%async_computation.5 | async-start | bytes 524288 | tf_op jit(solution)/shard_map/all_to_all | solution.py:432
  108.6 0.9 shard_map.227
  109.5 21.7 %all-to-all-done.5.back_ref = bf16[128,2,512]{2,1,0:T(2,128)(2,1)S(1)} async-done(((bf16[128,2,512]{2,1,0:T(2,128)(2,1)}), bf16[128,2,512]{2,1,0:T(2,128)(2,1)S(1)}, u32[]{:S(2)}, u32[]{:S(2)}) %all-to-all-start.5) | async-done | bytes 262176 | tf_op jit(solution)/shard_map/all_to_all | solution.py:432
  131.2 0.8 shard_map.228
Async XLA Ops:
  2.1 9.4 %all-to-all-start = ((bf16[4,48,512]{2,1,0:T(8,128)(2,1)}), bf16[4,48,512]{2,1,0:T(8,128)(2,1)S(1)}, u32[]{:S(2)}, u32[]{:S(2)}) async-start(bf16[4,48,512]{2,1,0:T(8,128)(2,1)} %broadcast_in_dim.31), calls=%async_computation | async-start | bytes 393216 | tf_op jit(solution)/shard_map/all_to_all | solution.py:315
  12.9 7.9 %all-to-all-start.1 = ((bf16[4,48,256]{2,1,0:T(8,128)(2,1)}), bf16[4,48,256]{2,1,0:T(8,128)(2,1)S(1)}, u32[]{:S(2)}, u32[]{:S(2)}) async-start(bf16[4,48,256]{2,1,0:T(8,128)(2,1)} %get-tuple-element.47), calls=%async_computation.1 | async-start | bytes 196608 | tf_op jit(solution)/shard_map/all_to_all | solution.py:381
  20.8 25.9 %copy-start.3 = (bf16[256,512]{1,0:T(8,128)(2,1)S(1)}, bf16[256,512]{1,0:T(8,128)(2,1)}, u32[]{:S(2)}) copy-start(bf16[256,512]{1,0:T(8,128)(2,1)} %get-tuple-element.54) | copy-start | bytes 786436
  20.8 28.7 %copy-start.2 = (bf16[256,512]{1,0:T(8,128)(2,1)S(1)}, bf16[256,512]{1,0:T(8,128)(2,1)}, u32[]{:S(2)}) copy-start(bf16[256,512]{1,0:T(8,128)(2,1)} %get-tuple-element.56) | copy-start | bytes 786436
  22.0 22.0 %copy-start.1 = (bf16[384,512]{1,0:T(8,128)(2,1)S(1)}, bf16[384,512]{1,0:T(8,128)(2,1)}, u32[]{:S(2)}) copy-start(bf16[384,512]{1,0:T(8,128)(2,1)} %get-tuple-element.55) | copy-start | bytes 1179652
  22.0 44.6 %all-to-all-start.2 = ((bf16[128,2,512]{2,1,0:T(2,128)(2,1)}), bf16[128,2,512]{2,1,0:T(2,128)(2,1)S(1)}, u32[]{:S(2)}, u32[]{:S(2)}) async-start(bf16[128,2,512]{2,1,0:T(2,128)(2,1)} %get-tuple-element.51), calls=%async_computation.2 | async-start | bytes 524288 | tf_op jit(solution)/shard_map/all_to_all | solution.py:404
  44.0 22.7 %copy-start = (bf16[384,512]{1,0:T(8,128)(2,1)S(1)}, bf16[384,512]{1,0:T(8,128)(2,1)}, u32[]{:S(2)}) copy-start(bf16[384,512]{1,0:T(8,128)(2,1)} %get-tuple-element.53.refs_0_) | copy-start | bytes 1179652
  44.0 22.7 %collective-permute-start.1 = (bf16[384,512]{1,0:T(8,128)(2,1)S(1)}, bf16[384,512]{1,0:T(8,128)(2,1)S(1)}, u32[]{:S(2)}, u32[]{:S(2)}) collective-permute-start(bf16[384,512]{1,0:T(8,128)(2,1)S(1)} %copy-done.1), channel_id=1, source_target_pairs={{0,2},{1,3},{2,0},{3,1},{4,6},{5,7},{6,4},{7,5},{8,10},{9,11},{10,... | collective-permute-start | bytes 1179656 | tf_op jit(solution)/shard_map/ppermute | solution.py:385
  46.7 20.0 %collective-permute-start = (bf16[256,512]{1,0:T(8,128)(2,1)S(1)}, bf16[256,512]{1,0:T(8,128)(2,1)S(1)}, u32[]{:S(2)}, u32[]{:S(2)}) collective-permute-start(bf16[256,512]{1,0:T(8,128)(2,1)S(1)} %copy-done.3), channel_id=1, source_target_pairs={{0,1},{1,2},{2,3},{3,0},{4,5},{5,6},{6,7},{7,4},{8,9},{9,10},{10,1... | collective-permute-start | bytes 786440 | tf_op jit(solution)/shard_map/ppermute | solution.py:385
  49.5 17.2 %collective-permute-start.2 = (bf16[256,512]{1,0:T(8,128)(2,1)S(1)}, bf16[256,512]{1,0:T(8,128)(2,1)S(1)}, u32[]{:S(2)}, u32[]{:S(2)}) collective-permute-start(bf16[256,512]{1,0:T(8,128)(2,1)S(1)} %copy-done.2), channel_id=1, source_target_pairs={{0,3},{1,0},{2,1},{3,2},{4,7},{5,4},{6,5},{7,6},{8,11},{9,8},{10,9... | collective-permute-start | bytes 786440 | tf_op jit(solution)/shard_map/ppermute | solution.py:385
  68.1 3.6 %copy-start.5 = (bf16[128,512]{1,0:T(8,128)(2,1)S(1)}, bf16[128,512]{1,0:T(8,128)(2,1)}, u32[]{:S(2)}) copy-start(bf16[128,512]{1,0:T(8,128)(2,1)} %get-tuple-element.57) | copy-start | bytes 393220
  68.1 6.9 %copy-start.4 = (bf16[128,512]{1,0:T(8,128)(2,1)S(1)}, bf16[128,512]{1,0:T(8,128)(2,1)}, u32[]{:S(2)}) copy-start(bf16[128,512]{1,0:T(8,128)(2,1)} %get-tuple-element.58) | copy-start | bytes 393220
  68.1 13.2 %all-to-all-start.3 = ((bf16[4,272,256]{2,1,0:T(8,128)(2,1)}), bf16[4,272,256]{2,1,0:T(8,128)(2,1)S(1)}, u32[]{:S(2)}, u32[]{:S(2)}) async-start(bf16[4,272,256]{2,1,0:T(8,128)(2,1)} %shard_map.224), calls=%async_computation.3 | async-start | bytes 1114112 | tf_op jit(solution)/shard_map/all_to_all | solution.py:418
  71.8 12.1 %collective-permute-start.3 = (bf16[128,512]{1,0:T(8,128)(2,1)S(1)}, bf16[128,512]{1,0:T(8,128)(2,1)S(1)}, u32[]{:S(2)}, u32[]{:S(2)}) collective-permute-start(bf16[128,512]{1,0:T(8,128)(2,1)S(1)} %copy-done.5), channel_id=1, source_target_pairs={{0,1},{1,2},{2,3},{3,0},{4,5},{5,6},{6,7},{7,4},{8,9},{9,10},{10,1... | collective-permute-start | bytes 393224 | tf_op jit(solution)/shard_map/ppermute | solution.py:385
  75.1 8.8 %collective-permute-start.4 = (bf16[128,512]{1,0:T(8,128)(2,1)S(1)}, bf16[128,512]{1,0:T(8,128)(2,1)S(1)}, u32[]{:S(2)}, u32[]{:S(2)}) collective-permute-start(bf16[128,512]{1,0:T(8,128)(2,1)S(1)} %copy-done.4), channel_id=1, source_target_pairs={{0,3},{1,0},{2,1},{3,2},{4,7},{5,4},{6,5},{7,6},{8,11},{9,8},{10,9... | collective-permute-start | bytes 393224 | tf_op jit(solution)/shard_map/ppermute | solution.py:385
  93.0 38.2 %all-to-all-start.5 = ((bf16[128,2,512]{2,1,0:T(2,128)(2,1)}), bf16[128,2,512]{2,1,0:T(2,128)(2,1)S(1)}, u32[]{:S(2)}, u32[]{:S(2)}) async-start(bf16[128,2,512]{2,1,0:T(2,128)(2,1)} %shard_map.226), calls=%async_computation.5 | async-start | bytes 524288 | tf_op jit(solution)/shard_map/all_to_all | solution.py:432

commit v8 on v7

--- a/solution.py
+++ b/solution.py
@@ -5,12 +5,15 @@
 from jax import lax
 from jax.experimental import pallas as pl
 from jax.experimental.pallas import tpu as pltpu
+from jax.sharding import Mesh
 from jax.sharding import PartitionSpec as P
 
 EPS = 1e-06
 RATE = 8.0
 CAPACITY = 2
 SUM_ROWS = 16
+CORES = 2
+EP = ("z", "x", "core")
 F32 = jnp.float32
 BF16 = jnp.bfloat16
 VMEM = pl.BlockSpec(memory_space=pltpu.VMEM)
@@ -225,10 +228,18 @@
 def first_products(member_ref, rows_ref, gain_ref, *refs):
     *weight_refs, out_ref = refs
     members = len(weight_refs)
-    count, width = rows_ref.shape
+    width = rows_ref.shape[-1]
+    count = out_ref.shape[1] - SUM_ROWS
     half = width // 2
+    shape = (count, count * CORES)
+    row = lax.broadcasted_iota(jnp.int32, shape, 0)
+    column = lax.broadcasted_iota(jnp.int32, shape, 1)
+    chip = lax.div(row, CORES * CAPACITY)
+    sender = lax.rem(lax.div(row, CAPACITY), CORES)
+    source = sender * count + (chip * CORES + member_ref[1]) * CAPACITY + lax.rem(row, CAPACITY)
+    choice = jnp.where(column == source, 1.0, 0.0).astype(BF16)
     owners = [lax.rem(member_ref[0] + (members - k), members) for k in range(members)]
-    rows = rows_ref[...].astype(F32)
+    rows = dot(choice, rows_ref[...].reshape(count * CORES, width))
     scaled = (rows * gain_ref[...]).astype(BF16)
     squares = rows * rows
     high, low = halves(squares)
@@ -306,7 +317,8 @@
     seq_count, quarter = tokens.shape
     channels = lru_state.shape[1]
     members = lax.axis_size("tp")
-    experts = lax.axis_size("ep")
+    experts = lax.axis_size("z") * lax.axis_size("x") * CORES
+    core = lax.axis_index("core").astype(jnp.int32)
     member = lax.axis_index("tp")
     place = member.astype(jnp.int32)[None]
     slots = experts * CAPACITY
@@ -393,7 +405,7 @@
         stream_rows,
         [
             pltpu.VMEM((seq_count, quarter), BF16),
-            jax.ShapeDtypeStruct((experts, CAPACITY, quarter), BF16),
+            jax.ShapeDtypeStruct((experts // CORES, CORES * CAPACITY, quarter), BF16),
         ],
         near(mixer_parts),
         near(output_near),
@@ -401,8 +413,8 @@
         near(dispatch),
     )
 
-    arrived = lax.all_to_all(outgoing, "ep", 0, 0, tiled=True)
-    arrived = arrived.reshape(slots, quarter)
+    arrived = lax.all_to_all(outgoing, ("z", "x"), 0, 0, tiled=True)
+    arrived = lax.all_gather(arrived, "core", axis=0, tiled=True)
     own, across = near(own), near(across)
     products = call(
         first_products,
@@ -413,7 +425,7 @@
         near(cut_next),
         across,
         near(cut_last),
-        scalar=place,
+        scalar=jnp.stack([place[0], core]),
     )
     products = lax.all_to_all(products, "tp", 0, 0, tiled=True)
     hidden = call(hidden_units, pltpu.VMEM((members, slots, units), BF16), near(products))
@@ -429,7 +441,7 @@
         near(down_last),
         scalar=place,
     )
-    returned = lax.all_to_all(answer, "ep", 0, 0, tiled=True)
+    returned = lax.all_to_all(answer, EP, 0, 0, tiled=True)
     result = call(
         add_routed,
         jax.ShapeDtypeStruct((seq_count, quarter), BF16),
@@ -443,9 +455,9 @@
 
 def solution(mesh):
     in_specs = (
-        P("ep", "tp"),
-        P("ep", None, "tp"),
-        P("ep", "tp"),
+        P(EP, "tp"),
+        P(EP, None, "tp"),
+        P(EP, "tp"),
         P(),
         P(None, "tp"),
         P(None, "tp"),
@@ -458,12 +470,21 @@
         P("tp"),
         P(None, "tp"),
         P(),
-        P("ep", None),
-        P("ep", None),
-        P("ep"),
-        P("ep", None, "tp"),
-        P("ep", None, "tp"),
-        P("ep", "tp", None),
-    )
-    out_specs = (P("ep", "tp"), P("ep", "tp"), P("ep", None, "tp"))
-    return jax.shard_map(body, mesh=mesh, in_specs=in_specs, out_specs=out_specs, check_vma=False)
+        P(EP, None),
+        P(EP, None),
+        P(EP),
+        P(EP, None, "tp"),
+        P(EP, None, "tp"),
+        P(EP, "tp", None),
+    )
+    out_specs = (P(EP, "tp"), P(EP, "tp"), P(EP, None, "tp"))
+    members = mesh.shape["tp"]
+    _, members = mesh.devices.shape
+    chips = mesh.devices.reshape(-1, 4, CORES, members)
+    return jax.shard_map(
+        body,
+        mesh=Mesh(chips, (*EP, "tp")),
+        in_specs=in_specs,
+        out_specs=out_specs,
+        check_vma=False,
+    )

time: 133 us -> 128 us (0.962)
  starting transfers between devices: 64.3 us -> 56.6 us
  blocking collectives: 8.03 us -> 15.7 us
  waiting for transfers between devices: 45.4 us -> 39.5 us
    all_gather x0 -> x1, blocking collectives: none -> 7.67 us  [body(): arrived = lax.all_gather(arrived, 'core', axis=0, tiled=True)]
    all_to_all x2, starting transfers between devices: 37.6 us -> 30 us  [the longest x1 17.8 us: body(): arrived = lax.all_to_all(outgoing, ('z', 'x'), 0, 0, tiled=True)]
    all_to_all x2, waiting for transfers between devices: 35.1 us -> 29.2 us  [the longest x1 21.7 us: body(): returned = lax.all_to_all(answer, EP, 0, 0, tiled=True)]
  transfers between devices with their start and end apart: 10 -> 10, of which waited for: 6 -> 6; matrix products, arithmetic and copies ran while one was open for 0% -> 1% of each run, Pallas kernels for 4% -> 5%
where the time goes in v8:
time: 128 us
  starting transfers between devices  56.6 us (44%)
  waiting for transfers between devices  39.5 us (31%)
  blocking collectives  15.7 us (12%)
  Pallas kernels  12.7 us (10%)
  local copies, waits for them, and re-layouts  1.51 us (1%)
    all_to_all x1, waiting for transfers between devices, body(): returned = lax.all_to_all(answer, EP, 0, 0, tiled=True)  21.7 us
    all_to_all x1, starting transfers between devices, body(): arrived = lax.all_to_all(outgoing, ('z', 'x'), 0, 0, tiled=True)  17.8 us
    ppermute x5, starting transfers between devices, onward(): return lax.ppermute(value, 'tp', ring)  15.5 us
    all_to_all x1, starting transfers between devices, body(): returned = lax.all_to_all(answer, EP, 0, 0, tiled=True)  12.2 us
    all_to_all x1, blocking collectives, body(): hidden = lax.all_to_all(hidden, 'tp', 0, 0, tiled=True)  8.05 us
    pallas_call x7, Pallas kernels, call(): pl.pallas_call(kernel, out_shape=outs, in_specs=[SMEM] * len(scalars) + [...  7.99 us
    all_gather x1, blocking collectives, body(): arrived = lax.all_gather(arrived, 'core', axis=0, tiled=True)  7.67 us
    all_to_all x1, waiting for transfers between devices, body(): arrived = lax.all_to_all(outgoing, ('z', 'x'), 0, 0, tiled=True)  7.46 us
  transfers between devices with their start and end apart: 10, of which 6 were waited for; matrix products, arithmetic and copies ran while one was open for 1% of the time, Pallas kernels for 5%

profile of v8, /device:TPU:33, one launch (start us, length us, event | category | flops | bytes accessed | tf_op | source)
XLA Modules:
  0.0 127.5 jit_solution(18270386406688063357)
XLA Ops:
  0.6 1.5 %broadcast_in_dim.31 = bf16[4,48,512]{2,1,0:T(8,128)(2,1)} broadcast(bf16[48,512]{1,0:T(8,128)(2,1)} %tokens_ref.1), dimensions={1,2} | broadcast | bytes 245760 | tf_op jit(solution)/shard_map/broadcast_in_dim | solution.py:328
  2.1 4.2 %all-to-all-start = ((bf16[4,48,512]{2,1,0:T(8,128)(2,1)}), bf16[4,48,512]{2,1,0:T(8,128)(2,1)S(1)}, u32[]{:S(2)}, u32[]{:S(2)}) async-start(bf16[4,48,512]{2,1,0:T(8,128)(2,1)} %broadcast_in_dim.31), calls=%async_computation | async-start | bytes 393216 | tf_op jit(solution)/shard_map/all_to_all | solution.py:327
  6.3 3.5 %shard_map.220 = (bf16[384,512]{1,0:T(8,128)(2,1)}, bf16[384,512]{1,0:T(8,128)(2,1)}, bf16[256,512]{1,0:T(8,128)(2,1)}, bf16[128,512]{1,0:T(8,128)(2,1)}, bf16[2...) custom-call(s32[1]{0:T(128)} %bitcast.member_ref, ...), custom_call_target="tpu_custom_call" | custom-call | tf_op jit(solution)/shard_map/pallas_call | solution.py:360
  9.8 1.7 %all-to-all-done.parts_ref = bf16[4,48,512]{2,1,0:T(8,128)(2,1)S(1)} async-done(((bf16[4,48,512]{2,1,0:T(8,128)(2,1)}), bf16[4,48,512]{2,1,0:T(8,128)(2,1)S(1)}, u32[]{:S(2)}, u32[]{:S(2)}) %all-to-all-start) | async-done | bytes 196640 | tf_op jit(solution)/shard_map/all_to_all | solution.py:327
  11.5 1.4 %shard_map.221 = (bf16[4,48,256]{2,1,0:T(8,128)(2,1)}, f32[48,256]{1,0:T(8,128)}, bf16[3,48,256]{2,1,0:T(8,128)(2,1)}) custom-call(bf16[4,48,512]{2,1,0:T(8,128)(2,1)S(1)} %all-to-all-done.parts_ref, f32[1,2048]{1,0:T(1,128)S(1)} %get-tuple-element.35.gain_ref, bf16[2048,256]{1,0:T(8,128)(2,1)S(1)} %get-tuple-element.36.input_ref, ...), custom_call_target="tpu_custom_call" | custom-call | tf_op jit(solution)/shard_map/pallas_call | solution.py:29
  12.9 3.3 %all-to-all-start.1 = ((bf16[4,48,256]{2,1,0:T(8,128)(2,1)}), bf16[4,48,256]{2,1,0:T(8,128)(2,1)S(1)}, u32[]{:S(2)}, u32[]{:S(2)}) async-start(bf16[4,48,256]{2,1,0:T(8,128)(2,1)} %get-tuple-element.47), calls=%async_computation.1 | async-start | bytes 196608 | tf_op jit(solution)/shard_map/all_to_all | solution.py:393
  16.2 1.3 %shard_map.222 = (bf16[256,48]{1,0:T(8,128)(2,1)S(1)}, bf16[1024,512]{1,0:T(8,128)(2,1)S(1)}, bf16[48,512]{1,0:T(8,128)(2,1)S(1)}, f32[1,512]{1,0:T(1,128)S(1)}) custom-call(s32[1]{0:T(128)} %bitcast.member_ref, s32[2,48]{1,0:T(2,128)} %bitcast.16, bf16[1024,512]{1,0:T(8,128)(2,1)} %weight_ref.1, bf16[48,512]{1,0:T(8,128)(2,1)} %tokens_ref.1, f32[1,2048]{1,0:T(1,128)} %bitcast.15), custom_call_target="tpu_custom_call" | custom-call | tf_op jit(solution)/shard_map/pallas_call | solution.py:365
  17.5 3.3 %all-to-all-done.1.parts_ref = bf16[4,48,256]{2,1,0:T(8,128)(2,1)S(1)} async-done(((bf16[4,48,256]{2,1,0:T(8,128)(2,1)}), bf16[4,48,256]{2,1,0:T(8,128)(2,1)S(1)}, u32[]{:S(2)}, u32[]{:S(2)}) %all-to-all-start.1) | async-done | bytes 98336 | tf_op jit(solution)/shard_map/all_to_all | solution.py:393
  20.8 0.0 copy-start.3
  20.8 0.0 copy-start.2
  20.8 1.2 shard_map.223
  22.0 0.0 copy-start.1
  22.0 17.8 %all-to-all-start.2 = ((bf16[64,4,512]{2,1,0:T(4,128)(2,1)}), bf16[64,4,512]{2,1,0:T(4,128)(2,1)S(1)}, u32[]{:S(2)}, u32[]{:S(2)}) async-start(bf16[64,4,512]{2,1,0:T(4,128)(2,1)} %get-tuple-element.51), calls=%async_computation.2 | async-start | bytes 524288 | tf_op jit(solution)/shard_map/all_to_all | solution.py:416
  39.8 0.0 copy-done.1
  39.8 2.5 %collective-permute-start.1 = (bf16[384,512]{1,0:T(8,128)(2,1)S(1)}, bf16[384,512]{1,0:T(8,128)(2,1)S(1)}, u32[]{:S(2)}, u32[]{:S(2)}) collective-permute-start(bf16[384,512]{1,0:T(8,128)(2,1)S(1)} %copy-done.1), channel_id=1, source_target_pairs={{0,2},{1,3},{2,0},{3,1},{4,6},{5,7},{6,4},{7,5},{8,10},{9,11},{10,... | collective-permute-start | bytes 1179656 | tf_op jit(solution)/shard_map/ppermute | solution.py:397
  42.3 0.0 copy-done.3
  42.4 2.7 %collective-permute-start = (bf16[256,512]{1,0:T(8,128)(2,1)S(1)}, bf16[256,512]{1,0:T(8,128)(2,1)S(1)}, u32[]{:S(2)}, u32[]{:S(2)}) collective-permute-start(bf16[256,512]{1,0:T(8,128)(2,1)S(1)} %copy-done.3), channel_id=1, source_target_pairs={{0,1},{1,2},{2,3},{3,0},{4,5},{5,6},{6,7},{7,4},{8,9},{9,10},{10,1... | collective-permute-start | bytes 786440 | tf_op jit(solution)/shard_map/ppermute | solution.py:397
  45.1 0.0 copy-done.2
  45.1 3.8 %collective-permute-start.2 = (bf16[256,512]{1,0:T(8,128)(2,1)S(1)}, bf16[256,512]{1,0:T(8,128)(2,1)S(1)}, u32[]{:S(2)}, u32[]{:S(2)}) collective-permute-start(bf16[256,512]{1,0:T(8,128)(2,1)S(1)} %copy-done.2), channel_id=1, source_target_pairs={{0,3},{1,0},{2,1},{3,2},{4,7},{5,4},{6,5},{7,6},{8,11},{9,8},{10,9... | collective-permute-start | bytes 786440 | tf_op jit(solution)/shard_map/ppermute | solution.py:397
  48.9 0.7 pad_add_fusion.member_ref
  49.5 0.0 copy-start
  49.5 7.5 %all-to-all-done.2 = bf16[64,4,512]{2,1,0:T(4,128)(2,1)S(1)} async-done(((bf16[64,4,512]{2,1,0:T(4,128)(2,1)}), bf16[64,4,512]{2,1,0:T(4,128)(2,1)S(1)}, u32[]{:S(2)}, u32[]{:S(2)}) %all-to-all-start.2) | async-done | bytes 262176 | tf_op jit(solution)/shard_map/all_to_all | solution.py:416
  57.0 7.7 %all_gather.3.rows_ref = bf16[128,4,512]{2,1,0:T(4,128)(2,1)S(1)} all-gather(bf16[64,4,512]{2,1,0:T(4,128)(2,1)S(1)} %all-to-all-done.2), channel_id=1, replica_groups=mesh['z'=16,'x'=4,'core'=2,'tp'=4] {'core'}, dimensions={0}, use_global_device_ids=true | all-gather | bytes 786432 | tf_op jit(solution)/shard_map/all_gather | solution.py:417
  64.7 0.0 collective-permute-done.refs_1_
  64.7 0.0 collective-permute-done.2.refs_3_
  64.7 0.0 collective-permute-done.1.refs_2_
  64.7 0.0 copy-done
  64.7 2.4 %shard_map.224 = bf16[4,272,256]{2,1,0:T(8,128)(2,1)} custom-call(s32[2]{0:T(128)} %pad_add_fusion.member_ref, bf16[128,4,512]{2,1,0:T(4,128)(2,1)S(1)} %all_gather.3.rows_ref, f32[1,512]{1,0:T(1,128)S(1)} %get-tuple-element.52.gain_ref, bf16[384,512]{1,0:T(8,128)(2,1)S(1)} %copy-done, bf16[256,512]{1,0:T(8,128)(2,1)S(1)} %collective-permute-done.refs_1_, ...), custom_call_target="tpu_custom_call" | custom-call | tf_op jit(solution)/shard_map/pallas_call | solution.py:29
  67.0 0.0 copy-start.5
  67.0 0.0 copy-start.4
  67.0 3.6 %all-to-all-start.3 = ((bf16[4,272,256]{2,1,0:T(8,128)(2,1)}), bf16[4,272,256]{2,1,0:T(8,128)(2,1)S(1)}, u32[]{:S(2)}, u32[]{:S(2)}) async-start(bf16[4,272,256]{2,1,0:T(8,128)(2,1)} %shard_map.224), calls=%async_computation.3 | async-start | bytes 1114112 | tf_op jit(solution)/shard_map/all_to_all | solution.py:430
  70.7 0.0 copy-done.5
  70.7 3.3 %collective-permute-start.3 = (bf16[128,512]{1,0:T(8,128)(2,1)S(1)}, bf16[128,512]{1,0:T(8,128)(2,1)S(1)}, u32[]{:S(2)}, u32[]{:S(2)}) collective-permute-start(bf16[128,512]{1,0:T(8,128)(2,1)S(1)} %copy-done.5), channel_id=1, source_target_pairs={{0,1},{1,2},{2,3},{3,0},{4,5},{5,6},{6,7},{7,4},{8,9},{9,10},{10,1... | collective-permute-start | bytes 393224 | tf_op jit(solution)/shard_map/ppermute | solution.py:397
  74.0 0.0 copy-done.4
  74.0 3.2 %collective-permute-start.4 = (bf16[128,512]{1,0:T(8,128)(2,1)S(1)}, bf16[128,512]{1,0:T(8,128)(2,1)S(1)}, u32[]{:S(2)}, u32[]{:S(2)}) collective-permute-start(bf16[128,512]{1,0:T(8,128)(2,1)S(1)} %copy-done.4), channel_id=1, source_target_pairs={{0,3},{1,0},{2,1},{3,2},{4,7},{5,4},{6,5},{7,6},{8,11},{9,8},{10,9... | collective-permute-start | bytes 393224 | tf_op jit(solution)/shard_map/ppermute | solution.py:397
  77.2 3.0 %all-to-all-done.3.parts_ref = bf16[4,272,256]{2,1,0:T(8,128)(2,1)S(1)} async-done(((bf16[4,272,256]{2,1,0:T(8,128)(2,1)}), bf16[4,272,256]{2,1,0:T(8,128)(2,1)S(1)}, u32[]{:S(2)}, u32[]{:S(2)}) %all-to-all-start.3) | async-done | bytes 557088 | tf_op jit(solution)/shard_map/all_to_all | solution.py:430
  80.2 0.2 shard_map.225
  80.4 2.2 %collective-permute-done.3.refs_1_ = bf16[128,512]{1,0:T(8,128)(2,1)S(1)} collective-permute-done((bf16[128,512]{1,0:T(8,128)(2,1)S(1)}, bf16[128,512]{1,0:T(8,128)(2,1)S(1)}, u32[]{:S(2)}, u32[]{:S(2)}) %collective-permute-start.3) | collective-permute-done | bytes 131104 | tf_op jit(solution)/shard_map/ppermute | solution.py:397
  82.7 0.0 collective-permute-done.4.refs_3_
  82.7 8.0 %all_to_all.30.hidden_ref = bf16[4,256,128]{2,1,0:T(8,128)(2,1)S(1)} all-to-all(bf16[4,256,128]{2,1,0:T(8,128)(2,1)S(1)} %shard_map.225), channel_id=1, replica_groups=mesh['z'=16,'x'=4,'core'=2,'tp'=4] {'tp'}, dimensions={0} | all-to-all | bytes 524288 | tf_op jit(solution)/shard_map/all_to_all | solution.py:433
  90.7 1.1 shard_map.226
  91.9 12.2 %all-to-all-start.5 = ((bf16[128,2,512]{2,1,0:T(2,128)(2,1)}), bf16[128,2,512]{2,1,0:T(2,128)(2,1)S(1)}, u32[]{:S(2)}, u32[]{:S(2)}) async-start(bf16[128,2,512]{2,1,0:T(2,128)(2,1)} %shard_map.226), calls=%async_computation.5 | async-start | bytes 524288 | tf_op jit(solution)/shard_map/all_to_all | solution.py:444
  104.1 0.9 shard_map.227
  105.0 21.7 %all-to-all-done.5.back_ref = bf16[128,2,512]{2,1,0:T(2,128)(2,1)S(1)} async-done(((bf16[128,2,512]{2,1,0:T(2,128)(2,1)}), bf16[128,2,512]{2,1,0:T(2,128)(2,1)S(1)}, u32[]{:S(2)}, u32[]{:S(2)}) %all-to-all-start.5) | async-done | bytes 262176 | tf_op jit(solution)/shard_map/all_to_all | solution.py:444
  126.7 0.8 shard_map.228
Async XLA Ops:
  2.1 9.4 %all-to-all-start = ((bf16[4,48,512]{2,1,0:T(8,128)(2,1)}), bf16[4,48,512]{2,1,0:T(8,128)(2,1)S(1)}, u32[]{:S(2)}, u32[]{:S(2)}) async-start(bf16[4,48,512]{2,1,0:T(8,128)(2,1)} %broadcast_in_dim.31), calls=%async_computation | async-start | bytes 393216 | tf_op jit(solution)/shard_map/all_to_all | solution.py:327
  12.9 7.9 %all-to-all-start.1 = ((bf16[4,48,256]{2,1,0:T(8,128)(2,1)}), bf16[4,48,256]{2,1,0:T(8,128)(2,1)S(1)}, u32[]{:S(2)}, u32[]{:S(2)}) async-start(bf16[4,48,256]{2,1,0:T(8,128)(2,1)} %get-tuple-element.47), calls=%async_computation.1 | async-start | bytes 196608 | tf_op jit(solution)/shard_map/all_to_all | solution.py:393
  20.8 21.5 %copy-start.3 = (bf16[256,512]{1,0:T(8,128)(2,1)S(1)}, bf16[256,512]{1,0:T(8,128)(2,1)}, u32[]{:S(2)}) copy-start(bf16[256,512]{1,0:T(8,128)(2,1)} %get-tuple-element.54) | copy-start | bytes 786436
  20.8 24.3 %copy-start.2 = (bf16[256,512]{1,0:T(8,128)(2,1)S(1)}, bf16[256,512]{1,0:T(8,128)(2,1)}, u32[]{:S(2)}) copy-start(bf16[256,512]{1,0:T(8,128)(2,1)} %get-tuple-element.56) | copy-start | bytes 786436
  22.0 17.8 %copy-start.1 = (bf16[384,512]{1,0:T(8,128)(2,1)S(1)}, bf16[384,512]{1,0:T(8,128)(2,1)}, u32[]{:S(2)}) copy-start(bf16[384,512]{1,0:T(8,128)(2,1)} %get-tuple-element.55) | copy-start | bytes 1179652
  22.0 35.0 %all-to-all-start.2 = ((bf16[64,4,512]{2,1,0:T(4,128)(2,1)}), bf16[64,4,512]{2,1,0:T(4,128)(2,1)S(1)}, u32[]{:S(2)}, u32[]{:S(2)}) async-start(bf16[64,4,512]{2,1,0:T(4,128)(2,1)} %get-tuple-element.51), calls=%async_computation.2 | async-start | bytes 524288 | tf_op jit(solution)/shard_map/all_to_all | solution.py:416
  39.8 24.9 %collective-permute-start.1 = (bf16[384,512]{1,0:T(8,128)(2,1)S(1)}, bf16[384,512]{1,0:T(8,128)(2,1)S(1)}, u32[]{:S(2)}, u32[]{:S(2)}) collective-permute-start(bf16[384,512]{1,0:T(8,128)(2,1)S(1)} %copy-done.1), channel_id=1, source_target_pairs={{0,2},{1,3},{2,0},{3,1},{4,6},{5,7},{6,4},{7,5},{8,10},{9,11},{10,... | collective-permute-start | bytes 1179656 | tf_op jit(solution)/shard_map/ppermute | solution.py:397
  42.4 22.3 %collective-permute-start = (bf16[256,512]{1,0:T(8,128)(2,1)S(1)}, bf16[256,512]{1,0:T(8,128)(2,1)S(1)}, u32[]{:S(2)}, u32[]{:S(2)}) collective-permute-start(bf16[256,512]{1,0:T(8,128)(2,1)S(1)} %copy-done.3), channel_id=1, source_target_pairs={{0,1},{1,2},{2,3},{3,0},{4,5},{5,6},{6,7},{7,4},{8,9},{9,10},{10,1... | collective-permute-start | bytes 786440 | tf_op jit(solution)/shard_map/ppermute | solution.py:397
  45.1 19.6 %collective-permute-start.2 = (bf16[256,512]{1,0:T(8,128)(2,1)S(1)}, bf16[256,512]{1,0:T(8,128)(2,1)S(1)}, u32[]{:S(2)}, u32[]{:S(2)}) collective-permute-start(bf16[256,512]{1,0:T(8,128)(2,1)S(1)} %copy-done.2), channel_id=1, source_target_pairs={{0,3},{1,0},{2,1},{3,2},{4,7},{5,4},{6,5},{7,6},{8,11},{9,8},{10,9... | collective-permute-start | bytes 786440 | tf_op jit(solution)/shard_map/ppermute | solution.py:397
  49.5 15.1 %copy-start = (bf16[384,512]{1,0:T(8,128)(2,1)S(1)}, bf16[384,512]{1,0:T(8,128)(2,1)}, u32[]{:S(2)}) copy-start(bf16[384,512]{1,0:T(8,128)(2,1)} %get-tuple-element.53.refs_0_) | copy-start | bytes 1179652
  67.0 3.6 %copy-start.5 = (bf16[128,512]{1,0:T(8,128)(2,1)S(1)}, bf16[128,512]{1,0:T(8,128)(2,1)}, u32[]{:S(2)}) copy-start(bf16[128,512]{1,0:T(8,128)(2,1)} %get-tuple-element.57) | copy-start | bytes 393220
  67.0 6.9 %copy-start.4 = (bf16[128,512]{1,0:T(8,128)(2,1)S(1)}, bf16[128,512]{1,0:T(8,128)(2,1)}, u32[]{:S(2)}) copy-start(bf16[128,512]{1,0:T(8,128)(2,1)} %get-tuple-element.58) | copy-start | bytes 393220
  67.0 13.2 %all-to-all-start.3 = ((bf16[4,272,256]{2,1,0:T(8,128)(2,1)}), bf16[4,272,256]{2,1,0:T(8,128)(2,1)S(1)}, u32[]{:S(2)}, u32[]{:S(2)}) async-start(bf16[4,272,256]{2,1,0:T(8,128)(2,1)} %shard_map.224), calls=%async_computation.3 | async-start | bytes 1114112 | tf_op jit(solution)/shard_map/all_to_all | solution.py:430
  70.7 12.0 %collective-permute-start.3 = (bf16[128,512]{1,0:T(8,128)(2,1)S(1)}, bf16[128,512]{1,0:T(8,128)(2,1)S(1)}, u32[]{:S(2)}, u32[]{:S(2)}) collective-permute-start(bf16[128,512]{1,0:T(8,128)(2,1)S(1)} %copy-done.5), channel_id=1, source_target_pairs={{0,1},{1,2},{2,3},{3,0},{4,5},{5,6},{6,7},{7,4},{8,9},{9,10},{10,1... | collective-permute-start | bytes 393224 | tf_op jit(solution)/shard_map/ppermute | solution.py:397
  74.0 8.7 %collective-permute-start.4 = (bf16[128,512]{1,0:T(8,128)(2,1)S(1)}, bf16[128,512]{1,0:T(8,128)(2,1)S(1)}, u32[]{:S(2)}, u32[]{:S(2)}) collective-permute-start(bf16[128,512]{1,0:T(8,128)(2,1)S(1)} %copy-done.4), channel_id=1, source_target_pairs={{0,3},{1,0},{2,1},{3,2},{4,7},{5,4},{6,5},{7,6},{8,11},{9,8},{10,9... | collective-permute-start | bytes 393224 | tf_op jit(solution)/shard_map/ppermute | solution.py:397
  91.9 34.8 %all-to-all-start.5 = ((bf16[128,2,512]{2,1,0:T(2,128)(2,1)}), bf16[128,2,512]{2,1,0:T(2,128)(2,1)S(1)}, u32[]{:S(2)}, u32[]{:S(2)}) async-start(bf16[128,2,512]{2,1,0:T(2,128)(2,1)} %shard_map.226), calls=%async_computation.5 | async-start | bytes 524288 | tf_op jit(solution)/shard_map/all_to_all | solution.py:444

commit v9 on v7

--- a/solution.py
+++ b/solution.py
@@ -59,49 +59,24 @@
     return jnp.where(earlier == place.astype(F32), named, 0.0), first
 
 
-def dispatch_table(
-    member_ref,
-    ids_ref,
-    weight_ref,
-    tokens_ref,
-    gain_ref,
-    out_ref,
-    weight_near_ref,
-    tokens_near_ref,
-    gain_near_ref,
-    ids_near_ref,
-    done,
+def combine_tables(
+    feature_ref, ids_ref, logits_ref, group_ref, gain_ref, high_ref, low_ref, gain_near_ref, done
 ):
-    quarter = gain_near_ref.shape[1]
-    own = pl.multiple_of(member_ref[0] * quarter, quarter)
-    pairs = [
-        (ids_ref, ids_near_ref),
-        (weight_ref, weight_near_ref),
-        (tokens_ref, tokens_near_ref),
-        (gain_ref.at[:, pl.ds(own, quarter)], gain_near_ref),
-    ]
-    copies = [
-        pltpu.make_async_copy(source, into, done.at[j]) for j, (source, into) in enumerate(pairs)
-    ]
-    for copy in copies:
-        copy.start()
-    copies[0].wait()
-    out_ref[...] = places(ids_near_ref, out_ref.shape[0])[0].astype(BF16)
-    for copy in copies[1:]:
-        copy.wait()
-
-
-def combine_tables(ids_ref, logits_ref, group_ref, high_ref, low_ref):
+    width = gain_near_ref.shape[1]
+    own = pl.multiple_of(feature_ref[0], width)
+    copy = pltpu.make_async_copy(gain_ref.at[:, pl.ds(own, width)], gain_near_ref, done)
+    copy.start()
     hit, first = places(ids_ref, high_ref.shape[0])
     raised = jnp.exp(logits_ref[...])
     weight = group_ref[...] * raised / (raised[0:1] + raised[1:2])
     high, low = halves(hit * jnp.where(first, weight[0:1], weight[1:2]))
     high_ref[...] = high
     low_ref[...] = low
-
-
-def cut_weights(member_ref, gate_ref, up_ref, down_ref, *refs, members):
-    *rest, piece_ref, reads, writes, loads = refs
+    copy.wait()
+
+
+def cut_weights(member_ref, ids_ref, gate_ref, up_ref, down_ref, *refs, members):
+    *rest, table_ref, piece_ref, ids_near_ref, reads, writes, loads = refs
     pieces = 2 * members - 2
     count = (len(rest) - pieces) // 2
     far_refs, rest = rest[:count], rest[count:]
@@ -110,6 +85,8 @@
     half = quarter // 2
     width = gate_ref.shape[2]
     order = (2, 1, 3, 0)
+    ids_copy = pltpu.make_async_copy(ids_ref, ids_near_ref, loads.at[count])
+    ids_copy.start()
     copies = {}
     for k in order:
         target = lax.rem(member_ref[0] + k, members)
@@ -137,6 +114,8 @@
     parts = [(0, whole), (2, whole)]
     for k in (1, 3):
         parts += [(k, pl.ds(0, half)), (k, pl.ds(half, width))]
+    ids_copy.wait()
+    table_ref[...] = places(ids_near_ref, table_ref.shape[0])[0].astype(BF16)
     out_copies = []
     for k in order:
         for copy in copies[k]:
@@ -212,12 +191,27 @@
         copies_ref[m] = out
 
 
-def stream_rows(parts_ref, weight_ref, tokens_ref, dispatch_ref, stream_ref, out_ref):
+def stream_rows(
+    parts_ref, dispatch_ref, weight_ref, tokens_ref, stream_ref, out_ref, near_ref, tokens_near_ref, done
+):
     members, _, width = parts_ref.shape
-    mixed = dot(parts_ref[0], weight_ref[:width, :])
-    for m in range(1, members):
-        mixed = mixed + dot(parts_ref[m], weight_ref[m * width : (m + 1) * width, :])
-    stream = (tokens_ref[...].astype(F32) + mixed).astype(BF16)
+    copies = [
+        pltpu.make_async_copy(
+            weight_ref.at[pl.ds(m * width, width), :],
+            near_ref.at[pl.ds(m * width, width), :],
+            done.at[m],
+        )
+        for m in range(members)
+    ]
+    copies.append(pltpu.make_async_copy(tokens_ref, tokens_near_ref, done.at[members]))
+    for copy in copies:
+        copy.start()
+    mixed = jnp.zeros(stream_ref.shape, F32)
+    for m in range(members):
+        copies[m].wait()
+        mixed = mixed + dot(parts_ref[m], near_ref[m * width : (m + 1) * width, :])
+    copies[members].wait()
+    stream = (tokens_near_ref[...].astype(F32) + mixed).astype(BF16)
     stream_ref[...] = stream
     out_ref[...] = dot(dispatch_ref[...], stream).astype(BF16).reshape(out_ref.shape)
 
@@ -332,42 +326,34 @@
     ]
     half, whole = (quarter // 2, quarter), (quarter // 2 + units, quarter)
     cuts = [whole, whole, half, (units, quarter), half, (units, quarter)]
+    ids = route_ids.T
+    table = pltpu.VMEM((slots, seq_count), BF16)
     cutting = pl.pallas_call(
         functools.partial(cut_weights, members=members),
         out_shape=[jax.ShapeDtypeStruct(shape, BF16) for shape in cuts]
-        + [pltpu.VMEM(value.shape, value.dtype) for value in operands],
-        in_specs=[SMEM] + [anywhere] * (3 + len(operands)),
-        out_specs=[anywhere] * len(cuts) + [VMEM] * len(operands),
+        + [pltpu.VMEM(value.shape, value.dtype) for value in operands]
+        + [table],
+        in_specs=[SMEM] + [anywhere] * (4 + len(operands)),
+        out_specs=[anywhere] * len(cuts) + [VMEM] * (1 + len(operands)),
         scratch_shapes=[
             pltpu.VMEM((members, *whole), BF16),
+            pltpu.VMEM(ids.shape, ids.dtype),
             pltpu.SemaphoreType.DMA((members, 5)),
             pltpu.SemaphoreType.DMA((len(cuts),)),
-            pltpu.SemaphoreType.DMA((len(operands),)),
+            pltpu.SemaphoreType.DMA((1 + len(operands),)),
         ],
     )
-    loaded = cutting(place, expert_gate, expert_up, expert_down, *operands)
+    loaded = cutting(place, ids, expert_gate, expert_up, expert_down, *operands)
     own, across, *sides = loaded[: len(cuts)]
-    operands = [near(value) for value in loaded[len(cuts) :]]
-    table = pltpu.VMEM((slots, seq_count), BF16)
-    ids = route_ids.T
-    dispatch, output_near, tokens_near, gain_part = pl.pallas_call(
-        dispatch_table,
-        out_shape=[
-            table,
-            pltpu.VMEM(output_weight.shape, BF16),
-            pltpu.VMEM(tokens.shape, BF16),
-            pltpu.VMEM((1, quarter), F32),
-        ],
-        in_specs=[SMEM] + [anywhere] * 4,
-        out_specs=[VMEM] * 4,
-        scratch_shapes=[
-            pltpu.VMEM(ids.shape, ids.dtype),
-            pltpu.SemaphoreType.DMA((4,)),
-        ],
-    )(place, ids, output_weight, tokens, moe_gain[None])
-    combine_high, combine_low = call(
-        combine_tables, [table] * 2, ids, route_logits.T, group_weight[None]
-    )
+    *operands, dispatch = [near(value) for value in loaded[len(cuts) :]]
+    feature = member.astype(jnp.int32) * quarter
+    combine_high, combine_low, gain_part = pl.pallas_call(
+        combine_tables,
+        out_shape=[table, table, pltpu.VMEM((1, quarter), F32)],
+        in_specs=[SMEM] + [VMEM] * 3 + [anywhere],
+        out_specs=[VMEM] * 3,
+        scratch_shapes=[pltpu.SemaphoreType.DMA],
+    )(feature[None], ids, route_logits.T, group_weight[None], moe_gain[None])
     copies, new_state, window = call(
         mixer,
         [
@@ -389,17 +375,20 @@
     cut_last = onward(sides[2], 3)
     down_next = onward(sides[1], 1)
     down_last = onward(sides[3], 3)
-    stream, outgoing = call(
+    stream, outgoing = pl.pallas_call(
         stream_rows,
-        [
+        out_shape=[
             pltpu.VMEM((seq_count, quarter), BF16),
             jax.ShapeDtypeStruct((experts, CAPACITY, quarter), BF16),
         ],
-        near(mixer_parts),
-        near(output_near),
-        near(tokens_near),
-        near(dispatch),
-    )
+        in_specs=[VMEM] * 2 + [anywhere] * 2,
+        out_specs=[VMEM] * 2,
+        scratch_shapes=[
+            pltpu.VMEM(output_weight.shape, BF16),
+            pltpu.VMEM(tokens.shape, BF16),
+            pltpu.SemaphoreType.DMA((members + 1,)),
+        ],
+    )(near(mixer_parts), dispatch, output_weight, tokens)
 
     arrived = lax.all_to_all(outgoing, "ep", 0, 0, tiled=True)
     arrived = arrived.reshape(slots, quarter)

time: 133 us -> 132 us (level)
  blocking collectives: 8.03 us -> 53 us
  waiting for transfers between devices: 45.4 us -> 19 us
  starting transfers between devices: 64.3 us -> 45.4 us
    all_to_all x0 -> x2, blocking collectives: none -> 45 us  [the longest x1 38 us: body(): returned = lax.all_to_all(answer, 'ep', 0, 0, tiled=True)]
    all_to_all x2 -> x0, waiting for transfers between devices: 25 us -> none  [the longest x1 21.7 us: body(): returned = lax.all_to_all(answer, 'ep', 0, 0, tiled=True)]
    all_to_all x2 -> x0, starting transfers between devices: 18.9 us -> none  [the longest x1 15.6 us: body(): returned = lax.all_to_all(answer, 'ep', 0, 0, tiled=True)]
    pallas_call x7 -> x5, Pallas kernels: 7.04 us -> 4.21 us  [call(): pl.pallas_call(kernel, out_shape=outs, in_specs=[SMEM] * len(scalars) + [...]
    pallas_call x2 -> x3, Pallas kernels: 4.74 us -> 7.24 us  [the longest x1 3.49 us: body(): loaded = cutting(place, ids, expert_gate, expert_up, expert_down, *operands)]
    all_to_all x1, waiting for transfers between devices: 13.4 us -> 11.9 us  [body(): arrived = lax.all_to_all(outgoing, 'ep', 0, 0, tiled=True)]
  transfers between devices with their start and end apart: 10 -> 8, of which waited for: 6 -> 4; matrix products, arithmetic and copies ran while one was open for 0% -> 0% of each run, Pallas kernels for 4% -> 4%
where the time goes in v9:
time: 132 us; the launch traced here: 131 us
  blocking collectives  53 us (40%)
  starting transfers between devices  45.4 us (34%)
  waiting for transfers between devices  19 us (14%)
  Pallas kernels  11.4 us (9%)
  local copies, waits for them, and re-layouts  1.63 us (1%)
    all_to_all x1, blocking collectives, body(): returned = lax.all_to_all(answer, 'ep', 0, 0, tiled=True)  38 us
    all_to_all x1, starting transfers between devices, body(): arrived = lax.all_to_all(outgoing, 'ep', 0, 0, tiled=True)  22 us
    ppermute x5, starting transfers between devices, onward(): return lax.ppermute(value, 'tp', ring)  15.7 us
    all_to_all x1, waiting for transfers between devices, body(): arrived = lax.all_to_all(outgoing, 'ep', 0, 0, tiled=True)  11.9 us
    all_to_all x1, blocking collectives, body(): hidden = lax.all_to_all(hidden, 'tp', 0, 0, tiled=True)  8.03 us
    all_to_all x1, blocking collectives, body(): mixer_parts = lax.all_to_all(copies, 'tp', 0, 0, tiled=True)  7.01 us
    pallas_call x5, Pallas kernels, call(): pl.pallas_call(kernel, out_shape=outs, in_specs=[SMEM] * len(scalars) + [...  4.21 us
    all_to_all x1, starting transfers between devices, body(): lax.all_to_all(jnp.broadcast_to(tokens[None], (members, *tokens.shape)),...  4.18 us
  transfers between devices with their start and end apart: 8, of which 4 were waited for; matrix products, arithmetic and copies ran while one was open for 0% of the time, Pallas kernels for 4%

profile of v9, /device:TPU:33, one launch (start us, length us, event | category | flops | bytes accessed | tf_op | source)
XLA Modules:
  0.0 131.3 jit_solution(6573595927037699944)
XLA Ops:
  0.6 1.5 %broadcast_in_dim.34 = bf16[4,48,512]{2,1,0:T(8,128)(2,1)} broadcast(bf16[48,512]{1,0:T(8,128)(2,1)} %tokens_ref.1), dimensions={1,2} | broadcast | bytes 245760 | tf_op jit(solution)/shard_map/broadcast_in_dim | solution.py:310
  2.1 4.2 %all-to-all-start = ((bf16[4,48,512]{2,1,0:T(8,128)(2,1)}), bf16[4,48,512]{2,1,0:T(8,128)(2,1)S(1)}, u32[]{:S(2)}, u32[]{:S(2)}) async-start(bf16[4,48,512]{2,1,0:T(8,128)(2,1)} %broadcast_in_dim.34), calls=%async_computation | async-start | bytes 393216 | tf_op jit(solution)/shard_map/all_to_all | solution.py:309
  6.3 3.5 %shard_map.220 = (bf16[384,512]{1,0:T(8,128)(2,1)}, bf16[384,512]{1,0:T(8,128)(2,1)}, bf16[256,512]{1,0:T(8,128)(2,1)}, bf16[128,512]{1,0:T(8,128)(2,1)}, bf16[2...) custom-call(s32[1]{0:T(128)} %bitcast.member_ref, ...), custom_call_target="tpu_custom_call" | custom-call | tf_op jit(solution)/shard_map/pallas_call | solution.py:346
  9.8 1.7 %all-to-all-done.parts_ref = bf16[4,48,512]{2,1,0:T(8,128)(2,1)S(1)} async-done(((bf16[4,48,512]{2,1,0:T(8,128)(2,1)}), bf16[4,48,512]{2,1,0:T(8,128)(2,1)S(1)}, u32[]{:S(2)}, u32[]{:S(2)}) %all-to-all-start) | async-done | bytes 196640 | tf_op jit(solution)/shard_map/all_to_all | solution.py:309
  11.5 1.3 %shard_map.221 = (bf16[4,48,256]{2,1,0:T(8,128)(2,1)S(1)}, f32[48,256]{1,0:T(8,128)}, bf16[3,48,256]{2,1,0:T(8,128)(2,1)}) custom-call(bf16[4,48,512]{2,1,0:T(8,128)(2,1)S(1)} %all-to-all-done.parts_ref, f32[1,2048]{1,0:T(1,128)S(1)} %get-tuple-element.33.gain_ref, bf16[2048,256]{1,0:T(8,128)(2,1)S(1)} %get-tuple-element.34.input_ref, ...), custom_call_target="tpu_custom_call" | custom-call | tf_op jit(solution)/shard_map/pallas_call | solution.py:26
  12.8 7.0 %all_to_all.30.parts_ref = bf16[4,48,256]{2,1,0:T(8,128)(2,1)S(1)} all-to-all(bf16[4,48,256]{2,1,0:T(8,128)(2,1)S(1)} %get-tuple-element.45), channel_id=1, replica_groups=mesh['ep'=128,'tp'=4] {'tp'}, dimensions={0} | all-to-all | bytes 196608 | tf_op jit(solution)/shard_map/all_to_all | solution.py:367
  19.8 0.0 copy-start.3
  19.8 0.0 copy-start.2
  19.9 2.4 %shard_map.222 = (bf16[48,512]{1,0:T(8,128)(2,1)S(1)}, bf16[128,2,512]{2,1,0:T(2,128)(2,1)}) custom-call(bf16[4,48,256]{2,1,0:T(8,128)(2,1)S(1)} %all_to_all.30.parts_ref, bf16[256,48]{1,0:T(8,128)(2,1)S(1)} %get-tuple-element.46.dispatch_ref, bf16[1024,512]{1,0:T(8,128)(2,1)} %weight_ref.1, bf16[48,512]{1,0:T(8,128)(2,1)} %tokens_ref.1), custom_call_target="tpu_custom_call" | custom-call | tf_op jit(solution)/shard_map/pallas_call | solution.py:378
  22.2 0.0 copy-start.1
  22.2 22.0 %all-to-all-start.2 = ((bf16[128,2,512]{2,1,0:T(2,128)(2,1)}), bf16[128,2,512]{2,1,0:T(2,128)(2,1)S(1)}, u32[]{:S(2)}, u32[]{:S(2)}) async-start(bf16[128,2,512]{2,1,0:T(2,128)(2,1)} %get-tuple-element.47), calls=%async_computation.2 | async-start | bytes 524288 | tf_op jit(solution)/shard_map/all_to_all | solution.py:393
  44.2 0.0 copy-start
  44.2 0.0 copy-done.1
  44.3 2.7 %collective-permute-start.1 = (bf16[384,512]{1,0:T(8,128)(2,1)S(1)}, bf16[384,512]{1,0:T(8,128)(2,1)S(1)}, u32[]{:S(2)}, u32[]{:S(2)}) collective-permute-start(bf16[384,512]{1,0:T(8,128)(2,1)S(1)} %copy-done.1), channel_id=1, source_target_pairs={{0,2},{1,3},{2,0},{3,1},{4,6},{5,7},{6,4},{7,5},{8,10},{9,11},{10,... | collective-permute-start | bytes 1179656 | tf_op jit(solution)/shard_map/ppermute | solution.py:371
  46.9 0.0 copy-done.3
  46.9 2.7 %collective-permute-start = (bf16[256,512]{1,0:T(8,128)(2,1)S(1)}, bf16[256,512]{1,0:T(8,128)(2,1)S(1)}, u32[]{:S(2)}, u32[]{:S(2)}) collective-permute-start(bf16[256,512]{1,0:T(8,128)(2,1)S(1)} %copy-done.3), channel_id=1, source_target_pairs={{0,1},{1,2},{2,3},{3,0},{4,5},{5,6},{6,7},{7,4},{8,9},{9,10},{10,1... | collective-permute-start | bytes 786440 | tf_op jit(solution)/shard_map/ppermute | solution.py:371
  49.7 0.0 copy-done.2
  49.7 3.8 %collective-permute-start.2 = (bf16[256,512]{1,0:T(8,128)(2,1)S(1)}, bf16[256,512]{1,0:T(8,128)(2,1)S(1)}, u32[]{:S(2)}, u32[]{:S(2)}) collective-permute-start(bf16[256,512]{1,0:T(8,128)(2,1)S(1)} %copy-done.2), channel_id=1, source_target_pairs={{0,3},{1,0},{2,1},{3,2},{4,7},{5,4},{6,5},{7,6},{8,11},{9,8},{10,9... | collective-permute-start | bytes 786440 | tf_op jit(solution)/shard_map/ppermute | solution.py:371
  53.5 1.4 %shard_map.223 = (bf16[256,48]{1,0:T(8,128)(2,1)S(1)}, bf16[256,48]{1,0:T(8,128)(2,1)S(1)}, f32[1,512]{1,0:T(1,128)S(1)}) custom-call(s32[1]{0:T(128)} %bitcast.8.feature_ref, s32[2,48]{1,0:T(2,128)} %bitcast.17, f32[2,48]{1,0:T(2,128)} %bitcast.22, f32[1,48]{1,0:T(1,128)} %bitcast.23, f32[1,2048]{1,0:T(1,128)} %bitcast.15), custom_call_target="tpu_custom_call" | custom-call | tf_op jit(solution)/shard_map/pallas_call | solution.py:350
  54.9 11.9 %all-to-all-done.2 = bf16[128,2,512]{2,1,0:T(2,128)(2,1)S(1)} async-done(((bf16[128,2,512]{2,1,0:T(2,128)(2,1)}), bf16[128,2,512]{2,1,0:T(2,128)(2,1)S(1)}, u32[]{:S(2)}, u32[]{:S(2)}) %all-to-all-start.2) | async-done | bytes 262176 | tf_op jit(solution)/shard_map/all_to_all | solution.py:393
  66.8 0.1 reshape.10.rows_ref
  66.9 0.0 collective-permute-done.refs_1_
  66.9 0.0 collective-permute-done.2.refs_3_
  66.9 0.0 collective-permute-done.1.refs_2_
  67.0 0.0 copy-done
  67.0 1.4 %shard_map.224 = bf16[4,272,256]{2,1,0:T(8,128)(2,1)} custom-call(s32[1]{0:T(128)} %bitcast.member_ref, bf16[256,512]{1,0:T(8,128)(2,1)S(1)} %reshape.10.rows_ref, f32[1,512]{1,0:T(1,128)S(1)} %get-tuple-element.48.gain_ref, bf16[384,512]{1,0:T(8,128)(2,1)S(1)} %copy-done, bf16[256,512]{1,0:T(8,128)(2,1)S(1)} %collective-permute-done.refs_1_, ...), custom_call_target="tpu_custom_call" | custom-call | tf_op jit(solution)/shard_map/pallas_call | solution.py:26
  68.4 0.0 copy-start.5
  68.4 0.0 copy-start.4
  68.4 3.6 %all-to-all-start.3 = ((bf16[4,272,256]{2,1,0:T(8,128)(2,1)}), bf16[4,272,256]{2,1,0:T(8,128)(2,1)S(1)}, u32[]{:S(2)}, u32[]{:S(2)}) async-start(bf16[4,272,256]{2,1,0:T(8,128)(2,1)} %shard_map.224), calls=%async_computation.3 | async-start | bytes 1114112 | tf_op jit(solution)/shard_map/all_to_all | solution.py:407
  72.0 0.0 copy-done.5
  72.0 3.3 %collective-permute-start.3 = (bf16[128,512]{1,0:T(8,128)(2,1)S(1)}, bf16[128,512]{1,0:T(8,128)(2,1)S(1)}, u32[]{:S(2)}, u32[]{:S(2)}) collective-permute-start(bf16[128,512]{1,0:T(8,128)(2,1)S(1)} %copy-done.5), channel_id=1, source_target_pairs={{0,1},{1,2},{2,3},{3,0},{4,5},{5,6},{6,7},{7,4},{8,9},{9,10},{10,1... | collective-permute-start | bytes 393224 | tf_op jit(solution)/shard_map/ppermute | solution.py:371
  75.3 0.0 copy-done.4
  75.3 3.2 %collective-permute-start.4 = (bf16[128,512]{1,0:T(8,128)(2,1)S(1)}, bf16[128,512]{1,0:T(8,128)(2,1)S(1)}, u32[]{:S(2)}, u32[]{:S(2)}) collective-permute-start(bf16[128,512]{1,0:T(8,128)(2,1)S(1)} %copy-done.4), channel_id=1, source_target_pairs={{0,3},{1,0},{2,1},{3,2},{4,7},{5,4},{6,5},{7,6},{8,11},{9,8},{10,9... | collective-permute-start | bytes 393224 | tf_op jit(solution)/shard_map/ppermute | solution.py:371
  78.5 3.1 %all-to-all-done.3.parts_ref = bf16[4,272,256]{2,1,0:T(8,128)(2,1)S(1)} async-done(((bf16[4,272,256]{2,1,0:T(8,128)(2,1)}), bf16[4,272,256]{2,1,0:T(8,128)(2,1)S(1)}, u32[]{:S(2)}, u32[]{:S(2)}) %all-to-all-start.3) | async-done | bytes 557088 | tf_op jit(solution)/shard_map/all_to_all | solution.py:407
  81.6 0.2 shard_map.225
  81.8 2.2 %collective-permute-done.3.refs_1_ = bf16[128,512]{1,0:T(8,128)(2,1)S(1)} collective-permute-done((bf16[128,512]{1,0:T(8,128)(2,1)S(1)}, bf16[128,512]{1,0:T(8,128)(2,1)S(1)}, u32[]{:S(2)}, u32[]{:S(2)}) %collective-permute-start.3) | collective-permute-done | bytes 131104 | tf_op jit(solution)/shard_map/ppermute | solution.py:371
  84.1 0.0 collective-permute-done.4.refs_3_
  84.1 8.0 %all_to_all.31.hidden_ref = bf16[4,256,128]{2,1,0:T(8,128)(2,1)S(1)} all-to-all(bf16[4,256,128]{2,1,0:T(8,128)(2,1)S(1)} %shard_map.225), channel_id=1, replica_groups=mesh['ep'=128,'tp'=4] {'tp'}, dimensions={0} | all-to-all | bytes 524288 | tf_op jit(solution)/shard_map/all_to_all | solution.py:410
  92.1 0.4 shard_map.226
  92.5 38.0 %all_to_all.32.back_ref = bf16[128,2,512]{2,1,0:T(2,128)(2,1)S(1)} all-to-all(bf16[128,2,512]{2,1,0:T(2,128)(2,1)S(1)} %shard_map.226), channel_id=1, replica_groups=mesh['ep'=128,'tp'=4] {'ep'}, dimensions={0} | all-to-all | bytes 524288 | tf_op jit(solution)/shard_map/all_to_all | solution.py:421
  130.5 0.8 shard_map.227
Async XLA Ops:
  2.1 9.4 %all-to-all-start = ((bf16[4,48,512]{2,1,0:T(8,128)(2,1)}), bf16[4,48,512]{2,1,0:T(8,128)(2,1)S(1)}, u32[]{:S(2)}, u32[]{:S(2)}) async-start(bf16[4,48,512]{2,1,0:T(8,128)(2,1)} %broadcast_in_dim.34), calls=%async_computation | async-start | bytes 393216 | tf_op jit(solution)/shard_map/all_to_all | solution.py:309
  19.8 27.1 %copy-start.3 = (bf16[256,512]{1,0:T(8,128)(2,1)S(1)}, bf16[256,512]{1,0:T(8,128)(2,1)}, u32[]{:S(2)}) copy-start(bf16[256,512]{1,0:T(8,128)(2,1)} %get-tuple-element.50) | copy-start | bytes 786436
  19.8 29.8 %copy-start.2 = (bf16[256,512]{1,0:T(8,128)(2,1)S(1)}, bf16[256,512]{1,0:T(8,128)(2,1)}, u32[]{:S(2)}) copy-start(bf16[256,512]{1,0:T(8,128)(2,1)} %get-tuple-element.52) | copy-start | bytes 786436
  22.2 22.0 %copy-start.1 = (bf16[384,512]{1,0:T(8,128)(2,1)S(1)}, bf16[384,512]{1,0:T(8,128)(2,1)}, u32[]{:S(2)}) copy-start(bf16[384,512]{1,0:T(8,128)(2,1)} %get-tuple-element.51) | copy-start | bytes 1179652
  22.2 44.6 %all-to-all-start.2 = ((bf16[128,2,512]{2,1,0:T(2,128)(2,1)}), bf16[128,2,512]{2,1,0:T(2,128)(2,1)S(1)}, u32[]{:S(2)}, u32[]{:S(2)}) async-start(bf16[128,2,512]{2,1,0:T(2,128)(2,1)} %get-tuple-element.47), calls=%async_computation.2 | async-start | bytes 524288 | tf_op jit(solution)/shard_map/all_to_all | solution.py:393
  44.2 22.7 %copy-start = (bf16[384,512]{1,0:T(8,128)(2,1)S(1)}, bf16[384,512]{1,0:T(8,128)(2,1)}, u32[]{:S(2)}) copy-start(bf16[384,512]{1,0:T(8,128)(2,1)} %get-tuple-element.49.refs_0_) | copy-start | bytes 1179652
  44.3 22.7 %collective-permute-start.1 = (bf16[384,512]{1,0:T(8,128)(2,1)S(1)}, bf16[384,512]{1,0:T(8,128)(2,1)S(1)}, u32[]{:S(2)}, u32[]{:S(2)}) collective-permute-start(bf16[384,512]{1,0:T(8,128)(2,1)S(1)} %copy-done.1), channel_id=1, source_target_pairs={{0,2},{1,3},{2,0},{3,1},{4,6},{5,7},{6,4},{7,5},{8,10},{9,11},{10,... | collective-permute-start | bytes 1179656 | tf_op jit(solution)/shard_map/ppermute | solution.py:371
  46.9 20.0 %collective-permute-start = (bf16[256,512]{1,0:T(8,128)(2,1)S(1)}, bf16[256,512]{1,0:T(8,128)(2,1)S(1)}, u32[]{:S(2)}, u32[]{:S(2)}) collective-permute-start(bf16[256,512]{1,0:T(8,128)(2,1)S(1)} %copy-done.3), channel_id=1, source_target_pairs={{0,1},{1,2},{2,3},{3,0},{4,5},{5,6},{6,7},{7,4},{8,9},{9,10},{10,1... | collective-permute-start | bytes 786440 | tf_op jit(solution)/shard_map/ppermute | solution.py:371
  49.7 17.2 %collective-permute-start.2 = (bf16[256,512]{1,0:T(8,128)(2,1)S(1)}, bf16[256,512]{1,0:T(8,128)(2,1)S(1)}, u32[]{:S(2)}, u32[]{:S(2)}) collective-permute-start(bf16[256,512]{1,0:T(8,128)(2,1)S(1)} %copy-done.2), channel_id=1, source_target_pairs={{0,3},{1,0},{2,1},{3,2},{4,7},{5,4},{6,5},{7,6},{8,11},{9,8},{10,9... | collective-permute-start | bytes 786440 | tf_op jit(solution)/shard_map/ppermute | solution.py:371
  68.4 3.6 %copy-start.5 = (bf16[128,512]{1,0:T(8,128)(2,1)S(1)}, bf16[128,512]{1,0:T(8,128)(2,1)}, u32[]{:S(2)}) copy-start(bf16[128,512]{1,0:T(8,128)(2,1)} %get-tuple-element.53) | copy-start | bytes 393220
  68.4 6.9 %copy-start.4 = (bf16[128,512]{1,0:T(8,128)(2,1)S(1)}, bf16[128,512]{1,0:T(8,128)(2,1)}, u32[]{:S(2)}) copy-start(bf16[128,512]{1,0:T(8,128)(2,1)} %get-tuple-element.54) | copy-start | bytes 393220
  68.4 13.2 %all-to-all-start.3 = ((bf16[4,272,256]{2,1,0:T(8,128)(2,1)}), bf16[4,272,256]{2,1,0:T(8,128)(2,1)S(1)}, u32[]{:S(2)}, u32[]{:S(2)}) async-start(bf16[4,272,256]{2,1,0:T(8,128)(2,1)} %shard_map.224), calls=%async_computation.3 | async-start | bytes 1114112 | tf_op jit(solution)/shard_map/all_to_all | solution.py:407
  72.0 12.1 %collective-permute-start.3 = (bf16[128,512]{1,0:T(8,128)(2,1)S(1)}, bf16[128,512]{1,0:T(8,128)(2,1)S(1)}, u32[]{:S(2)}, u32[]{:S(2)}) collective-permute-start(bf16[128,512]{1,0:T(8,128)(2,1)S(1)} %copy-done.5), channel_id=1, source_target_pairs={{0,1},{1,2},{2,3},{3,0},{4,5},{5,6},{6,7},{7,4},{8,9},{9,10},{10,1... | collective-permute-start | bytes 393224 | tf_op jit(solution)/shard_map/ppermute | solution.py:371
  75.3 8.8 %collective-permute-start.4 = (bf16[128,512]{1,0:T(8,128)(2,1)S(1)}, bf16[128,512]{1,0:T(8,128)(2,1)S(1)}, u32[]{:S(2)}, u32[]{:S(2)}) collective-permute-start(bf16[128,512]{1,0:T(8,128)(2,1)S(1)} %copy-done.4), channel_id=1, source_target_pairs={{0,3},{1,0},{2,1},{3,2},{4,7},{5,4},{6,5},{7,6},{8,11},{9,8},{10,9... | collective-permute-start | bytes 393224 | tf_op jit(solution)/shard_map/ppermute | solution.py:371
